TPU v7x, 512 devices: a whole 4x4x16 slice. The times are simulated.
512 devices in a mesh: sp: 64 (over z, y), tp: 8 (over x, core).
Axes of the slice: x: 4, y: 4, z: 16, core: 2. Of those that a mesh axis runs over, the one named last changes fastest.
Arguments:
- stream_in: bfloat16 [16384, 2048], P('sp'), may hold values from -6 to 6
- norm_gain: float32 [2, 2048], replicated, may hold values from 0.1 to 1.9
- value_weight: bfloat16 [2, 2048, 2048], P(None, 'sp', 'tp'), may hold values from -0.125 to 0.125
- gate_weight: bfloat16 [2, 2048, 2048], P(None, 'sp', 'tp'), may hold values from -0.125 to 0.125
- conv_taps: float32 [2, 31, 2048], P(None, None, 'tp'), may hold values from -5 to 5
- channel_gain: float32 [2, 2048], P(None, 'tp'), may hold values from 0.1 to 1.9
- out_weight: bfloat16 [2, 2048, 2048], P(None, 'tp', 'sp'), may hold values from -0.125 to 0.125
Outputs:
- stream_out: bfloat16 [16384, 2048], P('sp')
All inputs are finite; a program needn't handle non-finite values.
Results may differ from a plain program's by a relative error of at most 0.015.
Values may be sent and summed in bfloat16 or wider, within the bound.
No kernel may reach another device: no remote copies, remote signals or barrier semaphores. Data moves between devices by JAX's collectives and lax.ppermute only.
A program may use at most 64 MiB of HBM per device.

v0:
```python
import jax
import jax.numpy as jnp
from jax import lax
from jax.sharding import Mesh
from jax.sharding import PartitionSpec as P

LAYERS = 2
SP = ("sp_0", "sp_1")


epsilon = 1e-05


def side_by_side(arrays, axis, dim, along):
    widths = [a.shape[along] for a in arrays]
    both = jnp.concatenate(arrays, axis=along)
    out = lax.all_gather(both, axis, axis=dim, tiled=True)
    return tuple(jnp.split(out, [sum(widths[:k]) for k in range(1, len(widths))], axis=along))


def passed_along(value, axis, steps):
    count = lax.axis_size(axis)
    leading, last = (max(0, -steps), min(count, count - steps))
    return lax.ppermute(value, axis, [(source, source + steps) for source in range(leading, last)])


def sent_to_all(shard, axis):
    copies = jnp.broadcast_to(shard, (lax.axis_size(axis), *shard.shape))
    return lax.all_to_all(copies, axis, split_axis=0, concat_axis=0, tiled=True)


def over_copies(shard, axis):
    return sent_to_all(shard, axis).sum(axis=0)


def together(arrays, axis):
    ends = [0]
    for a in arrays:
        ends.append(ends[-1] + a.size)
    total = over_copies(jnp.concatenate([a.ravel() for a in arrays]), axis)
    return tuple((total[b:e].reshape(a.shape) for a, b, e in zip(arrays, ends, ends[1:])))


def gathered_by_axis(shard, axes, dim):
    if not axes:
        return shard
    nearer = lax.all_gather(shard, axes[-1], axis=dim, tiled=True)
    return gathered_by_axis(nearer, axes[:-1], dim)


def in_blocks(shard, dim, peers):
    before, after = (shard.shape[:dim], shard.shape[dim + 1 :])
    return jnp.moveaxis(shard.reshape(*before, peers, -1, *after), dim, 0)


def summed_on_arrival(shard, axis, dim):
    peers = lax.axis_size(axis)
    parts = lax.all_to_all(in_blocks(shard, dim, peers), axis, 0, 0, tiled=True)
    return jnp.sum(parts.astype(jnp.float32), axis=0)


def laid_out(parts, dim):
    parts = jnp.moveaxis(parts, 0, dim)
    lengths = parts.shape
    return parts.reshape(*lengths[:dim], lengths[dim] * lengths[dim + 1], *lengths[dim + 2 :])


def gather_directly(shard, axis, dim):
    return laid_out(sent_to_all(shard, axis), dim)


def body(stream_in, norm_gain, value_weight, gate_weight, conv_taps, channel_gain, out_weight):
    stream = stream_in
    tok_rows = stream_in.shape[0]
    width = stream_in.shape[1]
    kernel = conv_taps.shape[1]
    local_cols = value_weight.shape[2]
    for layer in range(LAYERS):
        wide = stream.astype(jnp.float32)
        normed = (
            wide
            * lax.rsqrt(jnp.mean(wide * wide, axis=1, keepdims=True) + epsilon)
            * norm_gain[layer]
        ).astype(jnp.bfloat16)
        full_value, full_gate = side_by_side((value_weight[layer], gate_weight[layer]), SP, 0, 1)
        value = jnp.dot(normed, full_value, preferred_element_type=jnp.float32)
        gate = jnp.dot(normed, full_gate, preferred_element_type=jnp.float32)
        gated = (value * jax.nn.sigmoid(gate)).astype(jnp.bfloat16)
        earlier = passed_along(gated[tok_rows - (kernel - 1) :], SP, 1)
        padded = jnp.concatenate([earlier, gated], axis=0).astype(jnp.float32)
        taps = conv_taps[layer]
        filtered = jnp.zeros((tok_rows, local_cols), jnp.float32)
        for tap in range(kernel):
            filtered = filtered + taps[tap] * padded[tap : tap + tok_rows]
        sum_first, sum_second = together(
            (jnp.sum(filtered, axis=1), jnp.sum(filtered * filtered, axis=1)), "tp"
        )
        mean_value = (sum_first / width)[:, None]
        variance = (sum_second / width)[:, None] - mean_value * mean_value
        activated = jax.nn.silu(
            (filtered - mean_value) * lax.rsqrt(variance + epsilon) * channel_gain[layer]
        ).astype(jnp.bfloat16)
        full_out = gathered_by_axis(out_weight[layer], SP, 1)
        share = tok_rows // lax.axis_size("tp")
        summed_rows = summed_on_arrival(
            jnp.dot(activated, full_out, preferred_element_type=jnp.float32).astype(jnp.bfloat16),
            "tp",
            0,
        )
        own_rows = lax.dynamic_slice_in_dim(wide, lax.axis_index("tp") * share, share, 0)
        stream = gather_directly((own_rows + summed_rows).astype(jnp.bfloat16), "tp", 0)
    return stream


def solution(mesh):
    finer = Mesh(mesh.devices.reshape(16, 4, mesh.shape["tp"]), ("sp_0", "sp_1", "tp"))
    placed = (
        P(SP, None),
        P(),
        P(None, SP, "tp"),
        P(None, SP, "tp"),
        P(None, None, "tp"),
        P(None, "tp"),
        P(None, "tp", SP),
    )
    return jax.shard_map(body, mesh=finer, in_specs=placed, out_specs=P(SP, None), check_vma=False)
```

profile of v0, /device:TPU:1, one launch (start us, length us, event | category | flops | bytes accessed | tf_op | source)
XLA Modules:
  0.0 482.7 jit_solution(8478346066151861120)
XLA Ops:
  8.7 11.0 %all-gather = bf16[1,256,128]{1,2,0:T(8,128)(2,1)} all-gather(bf16[1,256,32]{1,2,0:T(8,128)(2,1)S(1)} %get-tuple-element.79), channel_id=2, replica_groups=mesh['sp_0'=16,'sp_1'=4,'tp'=8] {'sp_1'}, dimensions={2}, use_global_device_ids=true | all-gather | bytes 81920 | tf_op jit(solution)/shard_map/all_gather | solution.py:47
  21.4 0.9 fusion.93
  23.1 1.5 multiply_reduce_fusion.1
  24.7 122.1 %all-gather.9.cloned.1.call-done = bf16[2048,512]{1,0:T(8,128)(2,1)} async-done(((bf16[32,512]{1,0:T(8,128)(2,1)}), bf16[2048,512]{1,0:T(8,128)(2,1)}) %all-gather.9.cloned.1.call-update) | async-done | bytes 2097168 | tf_op jit(solution)/shard_map/all_gather | solution.py:17
  146.8 2.2 fusion.14
  149.5 2.2 collective-permute-start
  152.7 1.1 fusion.89
  154.5 15.4 %all-to-all-start = ((f32[8,1,512]{2,1,0:T(1,128)}), f32[8,1,512]{2,1,0:T(1,128)S(1)}, u32[]{:S(2)}, u32[]{:S(2)}) async-start(f32[8,1,512]{2,1,0:T(1,128)} %broadcast_in_dim.8), calls=%async_computation | async-start | bytes 32768 | tf_op jit(solution)/shard_map/all_to_all | solution.py:29
  169.8 4.6 all-to-all-done
  174.5 40.2 %all-gather.13.cloned.1.call-done = bf16[1,256,2048]{1,2,0:T(8,128)(2,1)} async-done(((bf16[1,256,128]{1,2,0:T(8,128)(2,1)}), bf16[1,256,2048]{1,2,0:T(8,128)(2,1)}) %all-gather.13.cloned.1.call-update) | async-done | bytes 1048592 | tf_op jit(solution)/shard_map/all_gather | solution.py:47
  214.7 2.7 convolution_convert_fusion.1
  217.4 15.6 %all-to-all-start.1 = ((bf16[8,32,2048]{2,1,0:T(8,128)(2,1)}), bf16[8,32,2048]{2,1,0:T(8,128)(2,1)S(1)}, u32[]{:S(2)}, u32[]{:S(2)}) async-start(bf16[8,32,2048]{2,1,0:T(8,128)(2,1)} %bitcast.36), calls=%async_computation.1 | async-start | bytes 2097152 | tf_op jit(solution)/shard_map/all_to_all | solution.py:58
  233.0 1.5 convert_element_type.54
  234.6 13.4 %all-to-all-done.1 = bf16[8,32,2048]{2,1,0:T(8,128)(2,1)S(1)} async-done(((bf16[8,32,2048]{2,1,0:T(8,128)(2,1)}), bf16[8,32,2048]{2,1,0:T(8,128)(2,1)S(1)}, u32[]{:S(2)}, u32[]{:S(2)}) %all-to-all-start.1) | async-done | bytes 1048608 | tf_op jit(solution)/shard_map/all_to_all | solution.py:58
  248.2 1.0 add_convert_fusion.1
  249.2 1.1 broadcast_in_dim.9
  250.2 4.4 all-to-all-start.2
  254.7 10.6 %all-gather.2 = bf16[1,256,128]{1,2,0:T(8,128)(2,1)} all-gather(bf16[1,256,32]{1,2,0:T(8,128)(2,1)S(1)} %get-tuple-element.80), channel_id=4, replica_groups=mesh['sp_0'=16,'sp_1'=4,'tp'=8] {'sp_1'}, dimensions={2}, use_global_device_ids=true | all-gather | bytes 81920 | tf_op jit(solution)/shard_map/all_gather | solution.py:47
  265.3 4.4 all-to-all-done.2
  270.0 1.3 multiply_convert_fusion
  271.3 85.2 %all-gather.11.cloned.1.call-done = bf16[2048,512]{1,0:T(8,128)(2,1)} async-done(((bf16[32,512]{1,0:T(8,128)(2,1)}), bf16[2048,512]{1,0:T(8,128)(2,1)}) %all-gather.11.cloned.1.call-update) | async-done | bytes 2097168 | tf_op jit(solution)/shard_map/all_gather | solution.py:17
  356.6 2.0 fusion.11
  358.6 1.7 fusion.9
  360.3 2.2 collective-permute-start.1
  362.5 0.9 fusion.92
  363.4 1.2 fusion.88
  364.6 19.8 %all_to_all.32 = f32[8,1,512]{2,1,0:T(1,128)S(1)} all-to-all(f32[8,1,512]{2,1,0:T(1,128)S(1)} %broadcast_in_dim.20), channel_id=1, replica_groups=mesh['sp_0'=16,'sp_1'=4,'tp'=8] {'tp'}, dimensions={0} | all-to-all | bytes 32768 | tf_op jit(solution)/shard_map/all_to_all | solution.py:29
  384.4 40.0 %all-gather.15.cloned.1.call-done = bf16[1,256,2048]{1,2,0:T(8,128)(2,1)} async-done(((bf16[1,256,128]{1,2,0:T(8,128)(2,1)}), bf16[1,256,2048]{1,2,0:T(8,128)(2,1)}) %all-gather.15.cloned.1.call-update) | async-done | bytes 1048592 | tf_op jit(solution)/shard_map/all_gather | solution.py:47
  424.4 1.7 convolution_convert_fusion
  426.1 30.3 %all_to_all.33 = bf16[8,32,2048]{2,1,0:T(8,128)(2,1)S(1)} all-to-all(bf16[8,32,2048]{2,1,0:T(8,128)(2,1)S(1)} %bitcast.89), channel_id=1, replica_groups=mesh['sp_0'=16,'sp_1'=4,'tp'=8] {'tp'}, dimensions={0} | all-to-all | bytes 2097152 | tf_op jit(solution)/shard_map/all_to_all | solution.py:58
  456.8 18.4 %all_to_all.34 = bf16[8,32,2048]{2,1,0:T(8,128)(2,1)S(1)} all-to-all(bf16[8,32,2048]{2,1,0:T(8,128)(2,1)S(1)} %broadcast_in_dim.21), channel_id=1, replica_groups=mesh['sp_0'=16,'sp_1'=4,'tp'=8] {'tp'}, dimensions={0} | all-to-all | bytes 2097152 | tf_op jit(solution)/shard_map/all_to_all | solution.py:29
  475.2 1.0 copy.17
  (47 shorter events, 7.7 us)
Async XLA Ops:
  6.5 140.2 %all-gather.9.cloned.1.call-start = ((), (), s32[]{:S(2)}) async-start(), calls=%async_computation.6 | async-start | bytes 2129920 | tf_op jit(solution)/shard_map/all_gather | solution.py:17
  8.0 206.8 %all-gather.13.cloned.1.call-start = ((), (), s32[]{:S(2)}) async-start(), calls=%async_computation.8 | async-start | bytes 1114112 | tf_op jit(solution)/shard_map/all_gather | solution.py:47
  19.8 336.8 %all-gather.11.cloned.1.call-start = ((), (), s32[]{:S(2)}) async-start(), calls=%async_computation.7 | async-start | bytes 2129920 | tf_op jit(solution)/shard_map/all_gather | solution.py:17
  24.6 124.3 %copy-start = (bf16[256,2048]{1,0:T(8,128)(2,1)S(1)}, bf16[256,2048]{1,0:T(8,128)(2,1)}, u32[]{:S(2)}) copy-start(bf16[256,2048]{1,0:T(8,128)(2,1)} %param.7) | copy-start | bytes 3145732
  146.8 2.2 copy-start.3
  149.5 3.1 collective-permute-start
  152.7 17.2 %copy-start.2 = (f32[2,256]{1,0:T(2,128)S(1)}, f32[2,256]{1,0:T(2,128)}, u32[]{:S(2)}) copy-start(f32[2,256]{1,0:T(2,128)} %param.12) | copy-start | bytes 6148
  154.5 20.0 %all-to-all-start = ((f32[8,1,512]{2,1,0:T(1,128)}), f32[8,1,512]{2,1,0:T(1,128)S(1)}, u32[]{:S(2)}, u32[]{:S(2)}) async-start(f32[8,1,512]{2,1,0:T(1,128)} %broadcast_in_dim.8), calls=%async_computation | async-start | bytes 32768 | tf_op jit(solution)/shard_map/all_to_all | solution.py:29
  217.4 30.6 %all-to-all-start.1 = ((bf16[8,32,2048]{2,1,0:T(8,128)(2,1)}), bf16[8,32,2048]{2,1,0:T(8,128)(2,1)S(1)}, u32[]{:S(2)}, u32[]{:S(2)}) async-start(bf16[8,32,2048]{2,1,0:T(8,128)(2,1)} %bitcast.36), calls=%async_computation.1 | async-start | bytes 2097152 | tf_op jit(solution)/shard_map/all_to_all | solution.py:58
  250.2 19.4 %all-to-all-start.2 = ((bf16[8,32,2048]{2,1,0:T(8,128)(2,1)}), bf16[8,32,2048]{2,1,0:T(8,128)(2,1)S(1)}, u32[]{:S(2)}, u32[]{:S(2)}) async-start(bf16[8,32,2048]{2,1,0:T(8,128)(2,1)} %broadcast_in_dim.9), calls=%async_computation.2 | async-start | bytes 2097152 | tf_op jit(solution)/shard_map/all_to_all | solution.py:29
  254.7 169.7 %all-gather.15.cloned.1.call-start = ((), (), s32[]{:S(2)}) async-start(), calls=%async_computation.9 | async-start | bytes 1114112 | tf_op jit(solution)/shard_map/all_gather | solution.py:47
  271.3 87.2 %copy-start.1 = (bf16[256,2048]{1,0:T(8,128)(2,1)S(1)}, bf16[256,2048]{1,0:T(8,128)(2,1)}, u32[]{:S(2)}) copy-start(bf16[256,2048]{1,0:T(8,128)(2,1)} %get-tuple-element.10) | copy-start | bytes 3145732
  360.3 3.1 collective-permute-start.1
Sparse Core Ops, SparseCore 0:
  10.3 136.4 all-gather.8
  148.8 65.8 all-gather.12
  217.7 138.8 all-gather.10
  358.5 65.8 all-gather.14
where the time goes:
time: 484 us; the launch traced here: 483 us
  waiting for transfers between devices  310 us (64%)
  blocking collectives  90.1 us (19%)
  starting transfers between devices  40 us (8%)
  between operations  13.3 us (3%)
  matrix products  10.8 us (2%)
  other arithmetic  9.64 us (2%)
  local copies, waits for them, and re-layouts  8.66 us (2%)
    all_gather x2, waiting for transfers between devices, side_by_side(): out = lax.all_gather(both, axis, axis=dim, tiled=True)  207 us
    all_gather x2, waiting for transfers between devices, gathered_by_axis(): nearer = lax.all_gather(shard, axes[-1], axis=dim, tiled=True)  80.2 us
    all_to_all x2, blocking collectives, sent_to_all(): return lax.all_to_all(copies, axis, split_axis=0, concat_axis=0, tiled=True)  38.2 us
    all_to_all x1, blocking collectives, summed_on_arrival(): parts = lax.all_to_all(in_blocks(shard, dim, peers), axis, 0, 0, tiled=True)  30.3 us
    all_gather x2, blocking collectives, gathered_by_axis(): nearer = lax.all_gather(shard, axes[-1], axis=dim, tiled=True)  21.6 us
    all_to_all x2, starting transfers between devices, sent_to_all(): return lax.all_to_all(copies, axis, split_axis=0, concat_axis=0, tiled=True)  19.8 us
    all_to_all x1, starting transfers between devices, summed_on_arrival(): parts = lax.all_to_all(in_blocks(shard, dim, peers), axis, 0, 0, tiled=True)  15.6 us
    all_to_all x1, waiting for transfers between devices, summed_on_arrival(): parts = lax.all_to_all(in_blocks(shard, dim, peers), axis, 0, 0, tiled=True)  13.4 us
  transfers between devices with their start and end apart: 9, of which 8 were waited for; matrix products, arithmetic and copies ran while one was open for 5% of the time, Pallas kernels for 0%

commit v1 on v0

v1 whole, which is shorter than its diff:
```python
import jax
import jax.numpy as jnp
from jax import lax
from jax.sharding import Mesh
from jax.sharding import PartitionSpec as P

LAYERS = 2
SP = ("z", "y")
TP = ("x", "c")
HALO = 32
epsilon = 1e-05


def shifted(value, axis, steps):
    count = lax.axis_size(axis)
    return lax.ppermute(value, axis, [(i, (i + steps) % count) for i in range(count)])


def passed_on(value, axes):
    count = lax.axis_size(axes)
    return lax.ppermute(value, axes, [(i, i + 1) for i in range(count - 1)])


def sent_to_all(shard, axis):
    copies = jnp.broadcast_to(shard, (lax.axis_size(axis), *shard.shape))
    return lax.all_to_all(copies, axis, split_axis=0, concat_axis=0, tiled=True)


def ring(block, axis):
    count = lax.axis_size(axis)
    ahead, behind = [], []
    up = down = block
    for step in range(1, count // 2 + 1):
        up = shifted(up, axis, 1)
        behind.append(up)
        if step < count - count // 2:
            down = shifted(down, axis, -1)
            ahead.append(down)
    return [block] + ahead + behind[::-1]


def body(stream_in, norm_gain, value_weight, gate_weight, conv_taps, channel_gain, out_weight):
    z, x, c = (lax.axis_index(a) for a in ("z", "x", "c"))
    width = stream_in.shape[1]
    half = stream_in.shape[0] // 2
    kernel = conv_taps.shape[1]
    cols = value_weight.shape[2]
    xs = lax.axis_size("x")
    share = half // xs

    before = passed_on(stream_in[-HALO:], SP)
    extended = jnp.concatenate([before, stream_in], axis=0)
    rows = lax.dynamic_slice_in_dim(extended, c * half, half + HALO, 0)

    raw = jnp.concatenate([value_weight, gate_weight, jnp.swapaxes(out_weight, 1, 2)], axis=2)
    near = sent_to_all(raw, "y")
    near = jnp.swapaxes(near, 0, 1).reshape(LAYERS, -1, raw.shape[2])
    pieces = ring(near, "z")

    small = jnp.concatenate([conv_taps, channel_gain[:, None]], axis=1)
    small = jnp.concatenate([small, shifted(small, "c", 1)], axis=2)

    stream = rows[HALO:]
    for layer in range(LAYERS):
        mine = jnp.concatenate([p[layer] for p in pieces], axis=0)
        other = shifted(mine, "c", 1)
        wide = rows.astype(jnp.float32)
        normed = (
            wide
            * lax.rsqrt(jnp.mean(wide * wide, axis=1, keepdims=True) + epsilon)
            * norm_gain[layer]
        ).astype(jnp.bfloat16)
        turned = lax.dynamic_slice_in_dim(
            jnp.concatenate([normed, normed], axis=1), z * (width // lax.axis_size("z")), width, 1
        )

        def product(at):
            return jnp.concatenate(
                [
                    jnp.dot(turned, w[:, at : at + cols], preferred_element_type=jnp.float32)
                    for w in (mine, other)
                ],
                axis=1,
            )

        gated = (product(0) * jax.nn.sigmoid(product(cols))).astype(jnp.bfloat16)
        if layer:
            tail = jnp.roll(gated[-HALO:], cols, axis=1)
            gated = jnp.concatenate([passed_on(tail, (*SP, "c")), gated], axis=0)
        padded = gated.astype(jnp.float32)
        taps = small[layer, :kernel]
        filtered = jnp.zeros((half, 2 * cols), jnp.float32)
        for tap in range(kernel):
            at = HALO - kernel + 1 + tap
            filtered = filtered + taps[tap] * padded[at : at + half]
        sums = jnp.stack([jnp.sum(filtered, axis=1), jnp.sum(filtered * filtered, axis=1)])
        sums = jnp.sum(sent_to_all(sums.reshape(1, -1), "x"), axis=0).reshape(2, half, 1)
        mean = sums[0] / width
        variance = sums[1] / width - mean * mean
        activated = jax.nn.silu(
            (filtered - mean) * lax.rsqrt(variance + epsilon) * small[layer, kernel]
        ).astype(jnp.bfloat16)
        out_t = jnp.concatenate([mine[:, 2 * cols :], other[:, 2 * cols :]], axis=1)
        branch = lax.dot_general(
            activated, out_t, (((1,), (1,)), ((), ())), preferred_element_type=jnp.float32
        ).astype(jnp.bfloat16)
        branch = lax.dynamic_slice_in_dim(
            jnp.concatenate([branch, branch], axis=1),
            width - z * (width // lax.axis_size("z")),
            width,
            1,
        )
        parts = lax.all_to_all(branch.reshape(xs, share, width), "x", 0, 0, tiled=True)
        own = lax.dynamic_slice_in_dim(stream, x * share, share, 0).astype(jnp.float32)
        own = (own + jnp.sum(parts.astype(jnp.float32), axis=0)).astype(jnp.bfloat16)
        stream = lax.all_gather(own, "x", axis=0, tiled=True)
        rows = stream
    sibling = shifted(stream, "c", 1)
    return jnp.where(
        c == 0,
        jnp.concatenate([stream, sibling], axis=0),
        jnp.concatenate([sibling, stream], axis=0),
    )


def solution(mesh):
    finer = Mesh(mesh.devices.reshape(16, 4, 4, 2), (*SP, *TP))
    placed = (
        P(SP, None),
        P(),
        P(None, SP, TP),
        P(None, SP, TP),
        P(None, None, TP),
        P(None, TP),
        P(None, TP, SP),
    )
    return jax.shard_map(body, mesh=finer, in_specs=placed, out_specs=P(SP, None), check_vma=False)
```

time: 484 us -> 235 us (0.49)
  the two profiles are of different devices: /device:TPU:1 before, /device:TPU:33 now
where the time goes in v1:
time: 235 us; the launch traced here: 233 us
  starting transfers between devices  97.9 us (42%)
  waiting for transfers between devices  51.4 us (22%)
  blocking collectives  42.1 us (18%)
  local copies, waits for them, and re-layouts  19.2 us (8%)
  matrix products  14 us (6%)
  other arithmetic  7.86 us (3%)
    ppermute x19, starting transfers between devices, shifted(): lax.ppermute(value, axis, [(i, (i + steps) % count) for i in range(count)])  79.5 us
    ppermute x19, waiting for transfers between devices, shifted(): lax.ppermute(value, axis, [(i, (i + steps) % count) for i in range(count)])  34.8 us
    all_gather x2, blocking collectives, body(): stream = lax.all_gather(own, 'x', axis=0, tiled=True)  21.5 us
    dot_general x8, matrix products, product(): jnp.dot(turned, w[:, at:at + cols], preferred_element_type=jnp.float32)  12.4 us
    unnamed x23, local copies, waits for them, and re-layouts  11.8 us
    all_to_all x1, blocking collectives, sent_to_all(): return lax.all_to_all(copies, axis, split_axis=0, concat_axis=0, tiled=True)  11.2 us
    all_to_all x1, blocking collectives, body(): lax.all_to_all(branch.reshape(xs, share, width), 'x', 0, 0, tiled=True)  9.44 us
    all_to_all x1, waiting for transfers between devices, body(): lax.all_to_all(branch.reshape(xs, share, width), 'x', 0, 0, tiled=True)  9.24 us
  transfers between devices with their start and end apart: 24, of which 15 were waited for; matrix products, arithmetic and copies ran while one was open for 9% of the time, Pallas kernels for 0%

profile of v1, /device:TPU:33, one launch (start us, length us, event | category | flops | bytes accessed | tf_op | source)
XLA Modules:
  0.0 233.1 jit_solution(16521013540078405230)
XLA Ops:
  0.8 11.2 %all_to_all.25 = bf16[4,2,32,768]{3,2,1,0:T(8,128)(2,1)S(1)} all-to-all(bf16[4,2,32,768]{3,2,1,0:T(8,128)(2,1)S(1)} %broadcast_in_dim.15), channel_id=1, replica_groups=mesh['z'=16,'y'=4,'x'=4,'c'=2] {'y'}, dimensions={0} | all-to-all | bytes 786432 | tf_op jit(solution)/shard_map/all_to_all | solution.py:26
  12.1 3.5 %collective-permute-start.9 = (bf16[2,128,768]{2,1,0:T(8,128)(2,1)S(1)}, bf16[2,128,768]{2,1,0:T(8,128)(2,1)S(1)}, u32[]{:S(2)}, u32[]{:S(2)}) collective-permute-start(bf16[2,128,768]{2,1,0:T(8,128)(2,1)S(1)} %bitcast.235), channel_id=1, source_target_pairs={{0,32},{32,64},{64,96},{96,128},{128,160},{160,192},{192,224},{224... | collective-permute-start | bytes 1179656 | tf_op jit(solution)/shard_map/ppermute | solution.py:16
  15.6 1.9 collective-permute-start.2
  17.5 4.7 %collective-permute-done.9 = bf16[2,128,768]{2,1,0:T(8,128)(2,1)S(1)} collective-permute-done((bf16[2,128,768]{2,1,0:T(8,128)(2,1)S(1)}, bf16[2,128,768]{2,1,0:T(8,128)(2,1)S(1)}, u32[]{:S(2)}, u32[]{:S(2)}) %collective-permute-start.9) | collective-permute-done | bytes 393248 | tf_op jit(solution)/shard_map/ppermute | solution.py:16
  22.3 4.1 %collective-permute-start.10 = (bf16[2,128,768]{2,1,0:T(8,128)(2,1)S(1)}, bf16[2,128,768]{2,1,0:T(8,128)(2,1)S(1)}, u32[]{:S(2)}, u32[]{:S(2)}) collective-permute-start(bf16[2,128,768]{2,1,0:T(8,128)(2,1)S(1)} %collective-permute-done.9), channel_id=1, source_target_pairs={{0,32},{32,64},{64,96},{96,128},{128,160},{160,192},{192,224},{224... | collective-permute-start | bytes 1179656 | tf_op jit(solution)/shard_map/ppermute | solution.py:16
  26.5 8.1 %collective-permute-start.3 = (bf16[2,128,768]{2,1,0:T(8,128)(2,1)S(1)}, bf16[2,128,768]{2,1,0:T(8,128)(2,1)S(1)}, u32[]{:S(2)}, u32[]{:S(2)}) collective-permute-start(bf16[2,128,768]{2,1,0:T(8,128)(2,1)S(1)} %collective-permute-done.2), channel_id=1, source_target_pairs={{0,480},{32,0},{64,32},{96,64},{128,96},{160,128},{192,160},{224,1... | collective-permute-start | bytes 1179656 | tf_op jit(solution)/shard_map/ppermute | solution.py:16
  34.5 5.2 %collective-permute-done.10 = bf16[2,128,768]{2,1,0:T(8,128)(2,1)S(1)} collective-permute-done((bf16[2,128,768]{2,1,0:T(8,128)(2,1)S(1)}, bf16[2,128,768]{2,1,0:T(8,128)(2,1)S(1)}, u32[]{:S(2)}, u32[]{:S(2)}) %collective-permute-start.10) | collective-permute-done | bytes 393248 | tf_op jit(solution)/shard_map/ppermute | solution.py:16
  39.7 1.9 collective-permute-start.11
  41.6 4.3 %collective-permute-start.4 = (bf16[2,128,768]{2,1,0:T(8,128)(2,1)S(1)}, bf16[2,128,768]{2,1,0:T(8,128)(2,1)S(1)}, u32[]{:S(2)}, u32[]{:S(2)}) collective-permute-start(bf16[2,128,768]{2,1,0:T(8,128)(2,1)S(1)} %collective-permute-done.3), channel_id=1, source_target_pairs={{0,480},{32,0},{64,32},{96,64},{128,96},{160,128},{192,160},{224,1... | collective-permute-start | bytes 1179656 | tf_op jit(solution)/shard_map/ppermute | solution.py:16
  45.9 4.3 %collective-permute-done.11 = bf16[2,128,768]{2,1,0:T(8,128)(2,1)S(1)} collective-permute-done((bf16[2,128,768]{2,1,0:T(8,128)(2,1)S(1)}, bf16[2,128,768]{2,1,0:T(8,128)(2,1)S(1)}, u32[]{:S(2)}, u32[]{:S(2)}) %collective-permute-start.11) | collective-permute-done | bytes 393248 | tf_op jit(solution)/shard_map/ppermute | solution.py:16
  52.1 4.3 %collective-permute-start.5 = (bf16[2,128,768]{2,1,0:T(8,128)(2,1)S(1)}, bf16[2,128,768]{2,1,0:T(8,128)(2,1)S(1)}, u32[]{:S(2)}, u32[]{:S(2)}) collective-permute-start(bf16[2,128,768]{2,1,0:T(8,128)(2,1)S(1)} %collective-permute-done.4), channel_id=1, source_target_pairs={{0,480},{32,0},{64,32},{96,64},{128,96},{160,128},{192,160},{224,1... | collective-permute-start | bytes 1179656 | tf_op jit(solution)/shard_map/ppermute | solution.py:16
  56.4 3.2 %collective-permute-done.12 = bf16[2,128,768]{2,1,0:T(8,128)(2,1)S(1)} collective-permute-done((bf16[2,128,768]{2,1,0:T(8,128)(2,1)S(1)}, bf16[2,128,768]{2,1,0:T(8,128)(2,1)S(1)}, u32[]{:S(2)}, u32[]{:S(2)}) %collective-permute-start.12) | collective-permute-done | bytes 393248 | tf_op jit(solution)/shard_map/ppermute | solution.py:16
  62.4 4.6 %collective-permute-start.6 = (bf16[2,128,768]{2,1,0:T(8,128)(2,1)S(1)}, bf16[2,128,768]{2,1,0:T(8,128)(2,1)S(1)}, u32[]{:S(2)}, u32[]{:S(2)}) collective-permute-start(bf16[2,128,768]{2,1,0:T(8,128)(2,1)S(1)} %collective-permute-done.5), channel_id=1, source_target_pairs={{0,480},{32,0},{64,32},{96,64},{128,96},{160,128},{192,160},{224,1... | collective-permute-start | bytes 1179656 | tf_op jit(solution)/shard_map/ppermute | solution.py:16
  72.1 4.6 %collective-permute-start.7 = (bf16[2,128,768]{2,1,0:T(8,128)(2,1)S(1)}, bf16[2,128,768]{2,1,0:T(8,128)(2,1)S(1)}, u32[]{:S(2)}, u32[]{:S(2)}) collective-permute-start(bf16[2,128,768]{2,1,0:T(8,128)(2,1)S(1)} %collective-permute-done.6), channel_id=1, source_target_pairs={{0,480},{32,0},{64,32},{96,64},{128,96},{160,128},{192,160},{224,1... | collective-permute-start | bytes 1179656 | tf_op jit(solution)/shard_map/ppermute | solution.py:16
  81.8 4.8 %collective-permute-start.8 = (bf16[2,128,768]{2,1,0:T(8,128)(2,1)S(1)}, bf16[2,128,768]{2,1,0:T(8,128)(2,1)S(1)}, u32[]{:S(2)}, u32[]{:S(2)}) collective-permute-start(bf16[2,128,768]{2,1,0:T(8,128)(2,1)S(1)} %collective-permute-done.7), channel_id=1, source_target_pairs={{0,480},{32,0},{64,32},{96,64},{128,96},{160,128},{192,160},{224,1... | collective-permute-start | bytes 1179656 | tf_op jit(solution)/shard_map/ppermute | solution.py:16
  87.4 2.7 %collective-permute-done.15 = bf16[2,128,768]{2,1,0:T(8,128)(2,1)S(1)} collective-permute-done((bf16[2,128,768]{2,1,0:T(8,128)(2,1)S(1)}, bf16[2,128,768]{2,1,0:T(8,128)(2,1)S(1)}, u32[]{:S(2)}, u32[]{:S(2)}) %collective-permute-start.15) | collective-permute-done | bytes 393248 | tf_op jit(solution)/shard_map/ppermute | solution.py:16
  93.6 8.7 %collective-permute-done.16 = bf16[2,128,768]{2,1,0:T(8,128)(2,1)S(1)} collective-permute-done((bf16[2,128,768]{2,1,0:T(8,128)(2,1)S(1)}, bf16[2,128,768]{2,1,0:T(8,128)(2,1)S(1)}, u32[]{:S(2)}, u32[]{:S(2)}) %collective-permute-start.16) | collective-permute-done | bytes 393248 | tf_op jit(solution)/shard_map/ppermute | solution.py:16
  108.5 11.7 %collective-permute-start.17 = (bf16[2048,768]{1,0:T(8,128)(2,1)}, bf16[2048,768]{1,0:T(8,128)(2,1)}, u32[]{:S(2)}, u32[]{:S(2)}) collective-permute-start(bf16[2048,768]{1,0:T(8,128)(2,1)} %get-tuple-element.13), channel_id=1, source_target_pairs={{0,1},{1,0},{2,3},{3,2},{4,5},{5,4},{6,7},{7,6},{8,9},{9,8},{10,11... | collective-permute-start | bytes 9437192 | tf_op jit(solution)/shard_map/ppermute | solution.py:16
  120.3 2.2 collective-permute-start
  122.6 2.2 collective-permute-start.1
  126.1 3.3 %collective-permute-done = bf16[32,2048]{1,0:T(8,128)(2,1)S(1)} collective-permute-done((bf16[32,2048]{1,0:T(8,128)(2,1)S(1)}, bf16[32,2048]{1,0:T(8,128)(2,1)S(1)}, u32[]{:S(2)}, u32[]{:S(2)}) %collective-permute-start) | collective-permute-done | bytes 131104 | tf_op jit(solution)/shard_map/ppermute | solution.py:21
  138.4 4.0 %all-to-all-start.1 = ((f32[4,1,256]{2,1,0:T(1,128)}), f32[4,1,256]{2,1,0:T(1,128)S(1)}, u32[]{:S(2)}, u32[]{:S(2)}) async-start(f32[4,1,256]{2,1,0:T(1,128)} %broadcast_in_dim.16), calls=%async_computation.1 | async-start | bytes 8192 | tf_op jit(solution)/shard_map/all_to_all | solution.py:26
  143.7 3.1 %collective-permute-start.18 = (bf16[2048,768]{1,0:T(8,128)(2,1)}, bf16[2048,768]{1,0:T(8,128)(2,1)}, u32[]{:S(2)}, u32[]{:S(2)}) collective-permute-start(bf16[2048,768]{1,0:T(8,128)(2,1)} %get-tuple-element.14), channel_id=1, source_target_pairs={{0,1},{1,0},{2,3},{3,2},{4,5},{5,4},{6,7},{7,6},{8,9},{9,8},{10,11... | collective-permute-start | bytes 9437192 | tf_op jit(solution)/shard_map/ppermute | solution.py:16
  150.0 4.5 %all-to-all-start.2 = ((bf16[4,32,2048]{2,1,0:T(8,128)(2,1)}), bf16[4,32,2048]{2,1,0:T(8,128)(2,1)S(1)}, u32[]{:S(2)}, u32[]{:S(2)}) async-start(bf16[4,32,2048]{2,1,0:T(8,128)(2,1)} %bitcast.60), calls=%async_computation.2 | async-start | bytes 1048576 | tf_op jit(solution)/shard_map/all_to_all | solution.py:113
  154.6 9.2 %all-to-all-done.2 = bf16[4,32,2048]{2,1,0:T(8,128)(2,1)S(1)} async-done(((bf16[4,32,2048]{2,1,0:T(8,128)(2,1)}), bf16[4,32,2048]{2,1,0:T(8,128)(2,1)S(1)}, u32[]{:S(2)}, u32[]{:S(2)}) %all-to-all-start.2) | async-done | bytes 524320 | tf_op jit(solution)/shard_map/all_to_all | solution.py:113
  164.0 10.2 %all_gather.6 = bf16[128,2048]{1,0:T(8,128)(2,1)S(1)} all-gather(bf16[32,2048]{1,0:T(8,128)(2,1)S(1)} %add_convert_fusion.1), channel_id=1, replica_groups=mesh['z'=16,'y'=4,'x'=4,'c'=2] {'x'}, dimensions={0}, use_global_device_ids=true | all-gather | bytes 655360 | tf_op jit(solution)/shard_map/all_gather | solution.py:116
  181.1 4.4 %collective-permute-start.19 = (bf16[32,512]{1,0:T(8,128)(2,1)S(1)}, bf16[32,512]{1,0:T(8,128)(2,1)S(1)}, u32[]{:S(2)}, u32[]{:S(2)}) collective-permute-start(bf16[32,512]{1,0:T(8,128)(2,1)S(1)} %pad_maximum_fusion.3), channel_id=1, source_target_pairs={{0,1},{1,8},{8,9},{9,16},{16,17},{17,24},{24,25},{25,32},{32,33},{... | collective-permute-start | bytes 98312 | tf_op jit(solution)/shard_map/ppermute | solution.py:21
  185.6 2.6 %collective-permute-done.19 = bf16[32,512]{1,0:T(8,128)(2,1)S(1)} collective-permute-done((bf16[32,512]{1,0:T(8,128)(2,1)S(1)}, bf16[32,512]{1,0:T(8,128)(2,1)S(1)}, u32[]{:S(2)}, u32[]{:S(2)}) %collective-permute-start.19) | collective-permute-done | bytes 32800 | tf_op jit(solution)/shard_map/ppermute | solution.py:21
  190.0 3.2 %all-to-all-start.3 = ((f32[4,1,256]{2,1,0:T(1,128)}), f32[4,1,256]{2,1,0:T(1,128)S(1)}, u32[]{:S(2)}, u32[]{:S(2)}) async-start(f32[4,1,256]{2,1,0:T(1,128)} %broadcast_in_dim.17), calls=%async_computation.3 | async-start | bytes 8192 | tf_op jit(solution)/shard_map/all_to_all | solution.py:26
  198.5 9.4 %all_to_all.26 = bf16[4,32,2048]{2,1,0:T(8,128)(2,1)S(1)} all-to-all(bf16[4,32,2048]{2,1,0:T(8,128)(2,1)S(1)} %bitcast.234), channel_id=1, replica_groups=mesh['z'=16,'y'=4,'x'=4,'c'=2] {'x'}, dimensions={0} | all-to-all | bytes 1048576 | tf_op jit(solution)/shard_map/all_to_all | solution.py:113
  208.1 11.3 %all_gather.7 = bf16[128,2048]{1,0:T(8,128)(2,1)S(1)} all-gather(bf16[32,2048]{1,0:T(8,128)(2,1)S(1)} %add_convert_fusion), channel_id=1, replica_groups=mesh['z'=16,'y'=4,'x'=4,'c'=2] {'x'}, dimensions={0}, use_global_device_ids=true | all-gather | bytes 655360 | tf_op jit(solution)/shard_map/all_gather | solution.py:116
  219.4 11.0 %collective-permute-start.20 = (bf16[128,2048]{1,0:T(8,128)(2,1)S(1)}, bf16[128,2048]{1,0:T(8,128)(2,1)S(1)}, u32[]{:S(2)}, u32[]{:S(2)}) collective-permute-start(bf16[128,2048]{1,0:T(8,128)(2,1)S(1)} %all_gather.7), channel_id=1, source_target_pairs={{0,1},{1,0},{2,3},{3,2},{4,5},{5,4},{6,7},{7,6},{8,9},{9,8},{10,11... | collective-permute-start | bytes 1572872 | tf_op jit(solution)/shard_map/ppermute | solution.py:16
  (103 shorter events, 58.1 us)
Async XLA Ops:
  12.1 10.2 %collective-permute-start.9 = (bf16[2,128,768]{2,1,0:T(8,128)(2,1)S(1)}, bf16[2,128,768]{2,1,0:T(8,128)(2,1)S(1)}, u32[]{:S(2)}, u32[]{:S(2)}) collective-permute-start(bf16[2,128,768]{2,1,0:T(8,128)(2,1)S(1)} %bitcast.235), channel_id=1, source_target_pairs={{0,32},{32,64},{64,96},{96,128},{128,160},{160,192},{192,224},{224... | collective-permute-start | bytes 1179656 | tf_op jit(solution)/shard_map/ppermute | solution.py:16
  15.6 10.8 %collective-permute-start.2 = (bf16[2,128,768]{2,1,0:T(8,128)(2,1)S(1)}, bf16[2,128,768]{2,1,0:T(8,128)(2,1)S(1)}, u32[]{:S(2)}, u32[]{:S(2)}) collective-permute-start(bf16[2,128,768]{2,1,0:T(8,128)(2,1)S(1)} %bitcast.236), channel_id=1, source_target_pairs={{0,480},{32,0},{64,32},{96,64},{128,96},{160,128},{192,160},{224,1... | collective-permute-start | bytes 1179656 | tf_op jit(solution)/shard_map/ppermute | solution.py:16
  22.3 17.4 %collective-permute-start.10 = (bf16[2,128,768]{2,1,0:T(8,128)(2,1)S(1)}, bf16[2,128,768]{2,1,0:T(8,128)(2,1)S(1)}, u32[]{:S(2)}, u32[]{:S(2)}) collective-permute-start(bf16[2,128,768]{2,1,0:T(8,128)(2,1)S(1)} %collective-permute-done.9), channel_id=1, source_target_pairs={{0,32},{32,64},{64,96},{96,128},{128,160},{160,192},{192,224},{224... | collective-permute-start | bytes 1179656 | tf_op jit(solution)/shard_map/ppermute | solution.py:16
  26.5 15.1 %collective-permute-start.3 = (bf16[2,128,768]{2,1,0:T(8,128)(2,1)S(1)}, bf16[2,128,768]{2,1,0:T(8,128)(2,1)S(1)}, u32[]{:S(2)}, u32[]{:S(2)}) collective-permute-start(bf16[2,128,768]{2,1,0:T(8,128)(2,1)S(1)} %collective-permute-done.2), channel_id=1, source_target_pairs={{0,480},{32,0},{64,32},{96,64},{128,96},{160,128},{192,160},{224,1... | collective-permute-start | bytes 1179656 | tf_op jit(solution)/shard_map/ppermute | solution.py:16
  39.7 10.5 %collective-permute-start.11 = (bf16[2,128,768]{2,1,0:T(8,128)(2,1)S(1)}, bf16[2,128,768]{2,1,0:T(8,128)(2,1)S(1)}, u32[]{:S(2)}, u32[]{:S(2)}) collective-permute-start(bf16[2,128,768]{2,1,0:T(8,128)(2,1)S(1)} %collective-permute-done.10), channel_id=1, source_target_pairs={{0,32},{32,64},{64,96},{96,128},{128,160},{160,192},{192,224},{224... | collective-permute-start | bytes 1179656 | tf_op jit(solution)/shard_map/ppermute | solution.py:16
  41.6 10.5 %collective-permute-start.4 = (bf16[2,128,768]{2,1,0:T(8,128)(2,1)S(1)}, bf16[2,128,768]{2,1,0:T(8,128)(2,1)S(1)}, u32[]{:S(2)}, u32[]{:S(2)}) collective-permute-start(bf16[2,128,768]{2,1,0:T(8,128)(2,1)S(1)} %collective-permute-done.3), channel_id=1, source_target_pairs={{0,480},{32,0},{64,32},{96,64},{128,96},{160,128},{192,160},{224,1... | collective-permute-start | bytes 1179656 | tf_op jit(solution)/shard_map/ppermute | solution.py:16
  50.2 9.4 %collective-permute-start.12 = (bf16[2,128,768]{2,1,0:T(8,128)(2,1)S(1)}, bf16[2,128,768]{2,1,0:T(8,128)(2,1)S(1)}, u32[]{:S(2)}, u32[]{:S(2)}) collective-permute-start(bf16[2,128,768]{2,1,0:T(8,128)(2,1)S(1)} %collective-permute-done.11), channel_id=1, source_target_pairs={{0,32},{32,64},{64,96},{96,128},{128,160},{160,192},{192,224},{224... | collective-permute-start | bytes 1179656 | tf_op jit(solution)/shard_map/ppermute | solution.py:16
  52.1 10.2 %collective-permute-start.5 = (bf16[2,128,768]{2,1,0:T(8,128)(2,1)S(1)}, bf16[2,128,768]{2,1,0:T(8,128)(2,1)S(1)}, u32[]{:S(2)}, u32[]{:S(2)}) collective-permute-start(bf16[2,128,768]{2,1,0:T(8,128)(2,1)S(1)} %collective-permute-done.4), channel_id=1, source_target_pairs={{0,480},{32,0},{64,32},{96,64},{128,96},{160,128},{192,160},{224,1... | collective-permute-start | bytes 1179656 | tf_op jit(solution)/shard_map/ppermute | solution.py:16
  59.7 9.7 %collective-permute-start.13 = (bf16[2,128,768]{2,1,0:T(8,128)(2,1)S(1)}, bf16[2,128,768]{2,1,0:T(8,128)(2,1)S(1)}, u32[]{:S(2)}, u32[]{:S(2)}) collective-permute-start(bf16[2,128,768]{2,1,0:T(8,128)(2,1)S(1)} %collective-permute-done.12), channel_id=1, source_target_pairs={{0,32},{32,64},{64,96},{96,128},{128,160},{160,192},{192,224},{224... | collective-permute-start | bytes 1179656 | tf_op jit(solution)/shard_map/ppermute | solution.py:16
  62.4 9.7 %collective-permute-start.6 = (bf16[2,128,768]{2,1,0:T(8,128)(2,1)S(1)}, bf16[2,128,768]{2,1,0:T(8,128)(2,1)S(1)}, u32[]{:S(2)}, u32[]{:S(2)}) collective-permute-start(bf16[2,128,768]{2,1,0:T(8,128)(2,1)S(1)} %collective-permute-done.5), channel_id=1, source_target_pairs={{0,480},{32,0},{64,32},{96,64},{128,96},{160,128},{192,160},{224,1... | collective-permute-start | bytes 1179656 | tf_op jit(solution)/shard_map/ppermute | solution.py:16
  69.4 9.7 %collective-permute-start.14 = (bf16[2,128,768]{2,1,0:T(8,128)(2,1)S(1)}, bf16[2,128,768]{2,1,0:T(8,128)(2,1)S(1)}, u32[]{:S(2)}, u32[]{:S(2)}) collective-permute-start(bf16[2,128,768]{2,1,0:T(8,128)(2,1)S(1)} %collective-permute-done.13), channel_id=1, source_target_pairs={{0,32},{32,64},{64,96},{96,128},{128,160},{160,192},{192,224},{224... | collective-permute-start | bytes 1179656 | tf_op jit(solution)/shard_map/ppermute | solution.py:16
  72.1 9.7 %collective-permute-start.7 = (bf16[2,128,768]{2,1,0:T(8,128)(2,1)S(1)}, bf16[2,128,768]{2,1,0:T(8,128)(2,1)S(1)}, u32[]{:S(2)}, u32[]{:S(2)}) collective-permute-start(bf16[2,128,768]{2,1,0:T(8,128)(2,1)S(1)} %collective-permute-done.6), channel_id=1, source_target_pairs={{0,480},{32,0},{64,32},{96,64},{128,96},{160,128},{192,160},{224,1... | collective-permute-start | bytes 1179656 | tf_op jit(solution)/shard_map/ppermute | solution.py:16
  79.1 11.0 %collective-permute-start.15 = (bf16[2,128,768]{2,1,0:T(8,128)(2,1)S(1)}, bf16[2,128,768]{2,1,0:T(8,128)(2,1)S(1)}, u32[]{:S(2)}, u32[]{:S(2)}) collective-permute-start(bf16[2,128,768]{2,1,0:T(8,128)(2,1)S(1)} %collective-permute-done.14), channel_id=1, source_target_pairs={{0,32},{32,64},{64,96},{96,128},{128,160},{160,192},{192,224},{224... | collective-permute-start | bytes 1179656 | tf_op jit(solution)/shard_map/ppermute | solution.py:16
  81.8 11.0 %collective-permute-start.8 = (bf16[2,128,768]{2,1,0:T(8,128)(2,1)S(1)}, bf16[2,128,768]{2,1,0:T(8,128)(2,1)S(1)}, u32[]{:S(2)}, u32[]{:S(2)}) collective-permute-start(bf16[2,128,768]{2,1,0:T(8,128)(2,1)S(1)} %collective-permute-done.7), channel_id=1, source_target_pairs={{0,480},{32,0},{64,32},{96,64},{128,96},{160,128},{192,160},{224,1... | collective-permute-start | bytes 1179656 | tf_op jit(solution)/shard_map/ppermute | solution.py:16
  90.1 12.2 %collective-permute-start.16 = (bf16[2,128,768]{2,1,0:T(8,128)(2,1)S(1)}, bf16[2,128,768]{2,1,0:T(8,128)(2,1)S(1)}, u32[]{:S(2)}, u32[]{:S(2)}) collective-permute-start(bf16[2,128,768]{2,1,0:T(8,128)(2,1)S(1)} %collective-permute-done.15), channel_id=1, source_target_pairs={{0,32},{32,64},{64,96},{96,128},{128,160},{160,192},{192,224},{224... | collective-permute-start | bytes 1179656 | tf_op jit(solution)/shard_map/ppermute | solution.py:16
  102.3 18.0 %copy-start = (bf16[256,2048]{1,0:T(8,128)(2,1)S(1)}, bf16[256,2048]{1,0:T(8,128)(2,1)}, u32[]{:S(2)}) copy-start(bf16[256,2048]{1,0:T(8,128)(2,1)} %param.7) | copy-start | bytes 3145732
  102.3 20.2 %copy-start.1 = (f32[2,31,256]{2,0,1:T(2,128)S(1)}, f32[2,31,256]{2,0,1:T(2,128)}, u32[]{:S(2)}) copy-start(f32[2,31,256]{2,0,1:T(2,128)} %param.11) | copy-start | bytes 190468
  102.3 20.2 %copy-start.3 = (f32[2,256]{1,0:T(2,128)S(1)}, f32[2,256]{1,0:T(2,128)}, u32[]{:S(2)}) copy-start(f32[2,256]{1,0:T(2,128)} %param.12) | copy-start | bytes 6148
  103.1 21.7 %copy-start.2 = (f32[2,2048]{1,0:T(2,128)S(1)}, f32[2,2048]{1,0:T(2,128)}, u32[]{:S(2)}) copy-start(f32[2,2048]{1,0:T(2,128)} %param.8) | copy-start | bytes 49156
  108.5 24.8 %collective-permute-start.17 = (bf16[2048,768]{1,0:T(8,128)(2,1)}, bf16[2048,768]{1,0:T(8,128)(2,1)}, u32[]{:S(2)}, u32[]{:S(2)}) collective-permute-start(bf16[2048,768]{1,0:T(8,128)(2,1)} %get-tuple-element.13), channel_id=1, source_target_pairs={{0,1},{1,0},{2,3},{3,2},{4,5},{5,4},{6,7},{7,6},{8,9},{9,8},{10,11... | collective-permute-start | bytes 9437192 | tf_op jit(solution)/shard_map/ppermute | solution.py:16
  120.3 9.0 %collective-permute-start = (bf16[32,2048]{1,0:T(8,128)(2,1)S(1)}, bf16[32,2048]{1,0:T(8,128)(2,1)S(1)}, u32[]{:S(2)}, u32[]{:S(2)}) collective-permute-start(bf16[32,2048]{1,0:T(8,128)(2,1)S(1)} %slice.677), channel_id=1, source_target_pairs={{0,8},{8,16},{16,24},{24,32},{32,40},{40,48},{48,56},{56,64},{64,7... | collective-permute-start | bytes 393224 | tf_op jit(solution)/shard_map/ppermute | solution.py:21
  122.6 3.3 %collective-permute-start.1 = (f32[2,32,256]{2,0,1:T(2,128)S(1)}, f32[2,32,256]{2,0,1:T(2,128)S(1)}, u32[]{:S(2)}, u32[]{:S(2)}) collective-permute-start(f32[2,32,256]{2,0,1:T(2,128)S(1)} %pad_maximum_fusion.2), channel_id=1, source_target_pairs={{0,1},{1,0},{2,3},{3,2},{4,5},{5,4},{6,7},{7,6},{8,9},{9,8},{10,11... | collective-permute-start | bytes 196616 | tf_op jit(solution)/shard_map/ppermute | solution.py:16
  138.4 9.7 %all-to-all-start.1 = ((f32[4,1,256]{2,1,0:T(1,128)}), f32[4,1,256]{2,1,0:T(1,128)S(1)}, u32[]{:S(2)}, u32[]{:S(2)}) async-start(f32[4,1,256]{2,1,0:T(1,128)} %broadcast_in_dim.16), calls=%async_computation.1 | async-start | bytes 8192 | tf_op jit(solution)/shard_map/all_to_all | solution.py:26
  143.7 34.2 %collective-permute-start.18 = (bf16[2048,768]{1,0:T(8,128)(2,1)}, bf16[2048,768]{1,0:T(8,128)(2,1)}, u32[]{:S(2)}, u32[]{:S(2)}) collective-permute-start(bf16[2048,768]{1,0:T(8,128)(2,1)} %get-tuple-element.14), channel_id=1, source_target_pairs={{0,1},{1,0},{2,3},{3,2},{4,5},{5,4},{6,7},{7,6},{8,9},{9,8},{10,11... | collective-permute-start | bytes 9437192 | tf_op jit(solution)/shard_map/ppermute | solution.py:16
  150.0 13.8 %all-to-all-start.2 = ((bf16[4,32,2048]{2,1,0:T(8,128)(2,1)}), bf16[4,32,2048]{2,1,0:T(8,128)(2,1)S(1)}, u32[]{:S(2)}, u32[]{:S(2)}) async-start(bf16[4,32,2048]{2,1,0:T(8,128)(2,1)} %bitcast.60), calls=%async_computation.2 | async-start | bytes 1048576 | tf_op jit(solution)/shard_map/all_to_all | solution.py:113
  181.1 7.1 %collective-permute-start.19 = (bf16[32,512]{1,0:T(8,128)(2,1)S(1)}, bf16[32,512]{1,0:T(8,128)(2,1)S(1)}, u32[]{:S(2)}, u32[]{:S(2)}) collective-permute-start(bf16[32,512]{1,0:T(8,128)(2,1)S(1)} %pad_maximum_fusion.3), channel_id=1, source_target_pairs={{0,1},{1,8},{8,9},{9,16},{16,17},{17,24},{24,25},{25,32},{32,33},{... | collective-permute-start | bytes 98312 | tf_op jit(solution)/shard_map/ppermute | solution.py:21
  190.0 7.4 %all-to-all-start.3 = ((f32[4,1,256]{2,1,0:T(1,128)}), f32[4,1,256]{2,1,0:T(1,128)S(1)}, u32[]{:S(2)}, u32[]{:S(2)}) async-start(f32[4,1,256]{2,1,0:T(1,128)} %broadcast_in_dim.17), calls=%async_computation.3 | async-start | bytes 8192 | tf_op jit(solution)/shard_map/all_to_all | solution.py:26
  219.4 12.5 %collective-permute-start.20 = (bf16[128,2048]{1,0:T(8,128)(2,1)S(1)}, bf16[128,2048]{1,0:T(8,128)(2,1)S(1)}, u32[]{:S(2)}, u32[]{:S(2)}) collective-permute-start(bf16[128,2048]{1,0:T(8,128)(2,1)S(1)} %all_gather.7), channel_id=1, source_target_pairs={{0,1},{1,0},{2,3},{3,2},{4,5},{5,4},{6,7},{7,6},{8,9},{9,8},{10,11... | collective-permute-start | bytes 1572872 | tf_op jit(solution)/shard_map/ppermute | solution.py:16

commit v2 on v1

v2 whole, which is shorter than its diff:
```python
import functools

import jax
import jax.numpy as jnp
from jax import lax
from jax.experimental import pallas as pl
from jax.experimental.pallas import tpu as pltpu
from jax.sharding import Mesh
from jax.sharding import PartitionSpec as P

SP = ("z", "y")
TP = ("x", "c")
HALO = 32
epsilon = 1e-05
F32 = jnp.float32
BF16 = jnp.bfloat16


def shifted(value, axis, steps):
    count = lax.axis_size(axis)
    return lax.ppermute(value, axis, [(i, (i + steps) % count) for i in range(count)])


def passed_on(value, axes):
    count = lax.axis_size(axes)
    return lax.ppermute(value, axes, [(i, i + 1) for i in range(count - 1)])


def sent_to_all(shard, axis):
    copies = jnp.broadcast_to(shard, (lax.axis_size(axis), *shard.shape))
    return lax.all_to_all(copies, axis, split_axis=0, concat_axis=0, tiled=True)


def in_parts(value):
    parts = []
    for _ in range(3):
        parts.append(lax.reduce_precision(value, 8, 7).astype(BF16))
        value = value - parts[-1].astype(F32)
    return jnp.stack(parts)


def call(kernel, out, *args, scratch=(), scalars=0):
    smem, vmem = pl.BlockSpec(memory_space=pltpu.SMEM), pl.BlockSpec(memory_space=pltpu.VMEM)
    return pl.pallas_call(
        kernel,
        out_shape=[jax.ShapeDtypeStruct(s, d) for s, d in out],
        in_specs=[smem] * scalars + [vmem] * (len(args) - scalars),
        out_specs=[vmem] * len(out),
        scratch_shapes=[pltpu.VMEM(s, d) for s, d in scratch],
    )(*args)


def normed(rows_ref, gain_ref, to_ref):
    count = rows_ref.shape[0]
    for at in range(0, count, HALO):
        wide = rows_ref[at : at + HALO, :].astype(F32)
        mean = jnp.mean(wide * wide, axis=1, keepdims=True)
        to_ref[at : at + HALO, :] = (wide * lax.rsqrt(mean + epsilon) * gain_ref[...]).astype(BF16)


def gate_of(a, w_ref, cols):
    value = jnp.dot(a, w_ref[:, :cols], preferred_element_type=F32)
    gate = jnp.dot(a, w_ref[:, cols : 2 * cols], preferred_element_type=F32)
    return (value * jax.nn.sigmoid(gate)).astype(BF16)


def first_kernel(cols, deep, ys, at_ref, rows_ref, gain_ref, small_ref, *refs):
    *blocks, pair_ref, keep_ref, send_ref, later_ref, last_ref, weights, scaled = refs
    later_ref[...] = pair_ref[:, : 2 * cols]
    last_ref[...] = pair_ref[:, 2 * cols : 3 * cols]
    here, c = at_ref[0], at_ref[1]
    whole = blocks[0].shape[0]
    for ref, offset, start in zip(blocks, (0, ys - 1, 1, 2, 2), (0, 0, 0, 0, whole // 2)):
        where = lax.rem(here + offset, ys) * deep
        for k in range(ref.shape[0] // deep):
            at = (start // deep + k) * ys * deep
            rows = pl.ds(pl.multiple_of(at + where, deep), deep)
            weights[rows, :] = ref[k * deep : (k + 1) * deep, : 2 * cols]
            send_ref[rows, :] = ref[k * deep : (k + 1) * deep, 2 * cols :]
    normed(rows_ref, gain_ref, scaled)
    gated = gate_of(scaled[...], weights, cols)
    count = keep_ref.shape[0]
    low, high = gated[:count], gated[rows_ref.shape[0] - count :]
    keep_ref[...] = jnp.where(c == 0, low, high)
    at = whole * ys
    send_ref[at : at + count, :] = jnp.where(c == 0, high, low)
    send_ref[at + count :, :] = small_ref[...]


def second_kernel(cols, rows_ref, gain_ref, mine_ref, other_ref, gated_ref, tail_ref, scaled):
    normed(rows_ref, gain_ref, scaled)
    for k, w_ref in enumerate((mine_ref, other_ref)):
        part = gate_of(scaled[...], w_ref, cols)
        gated_ref[:, k * cols : (k + 1) * cols] = part
        tail_ref[:, (1 - k) * cols : (2 - k) * cols] = part[-HALO:]


def meet_kernel(keep_ref, got_ref, padded_ref, other_ref):
    rows, cols = keep_ref.shape
    deep = other_ref.shape[0]
    at = got_ref.shape[0] - 3 * deep
    parts = [got_ref[at + k * deep : at + (k + 1) * deep, :].astype(F32) for k in range(3)]
    other_ref[...] = parts[0] + parts[1] + parts[2]
    padded_ref[:, :cols] = keep_ref[...].astype(F32)
    padded_ref[:, cols:] = got_ref[at - rows : at, :].astype(F32)


def body(stream_in, norm_gain, value_weight, gate_weight, conv_taps, channel_gain, out_weight):
    y, x, c = (lax.axis_index(a) for a in ("y", "x", "c"))
    width = stream_in.shape[1]
    half = stream_in.shape[0] // 2
    kernel = conv_taps.shape[1]
    cols = value_weight.shape[2]
    xs = lax.axis_size("x")
    share = half // xs

    raw = jnp.concatenate([value_weight, gate_weight, jnp.swapaxes(out_weight, 1, 2)], axis=2)
    deep, wide = raw.shape[1:]
    padded, first = lax.optimization_barrier((jnp.pad(raw[1], ((0, 0), (0, cols))), raw[0]))
    later = lax.all_gather(padded, "z", axis=0, tiled=True)
    block = lax.all_gather(first, "z", axis=0, tiled=True)
    block, edge = lax.optimization_barrier((block, stream_in[-HALO:]))
    before = passed_on(edge, SP)
    middle = block.shape[0] // 2
    up, down = shifted(block, "y", 1), shifted(block, "y", -1)
    blocks = (block, up, down, shifted(up[:middle], "y", 1), shifted(down[middle:], "y", -1))
    rows = jnp.concatenate([before, stream_in], axis=0)
    table = jnp.concatenate([conv_taps, channel_gain[:, None]], axis=1)
    small = in_parts(table).reshape(-1, cols)

    keep, send, later, last = call(
        functools.partial(first_kernel, cols, deep, lax.axis_size("y")),
        [
            ((half + HALO, cols), BF16),
            ((width + half + HALO + small.shape[0], cols), BF16),
            ((later.shape[0], 2 * cols), BF16),
            ((later.shape[0], cols), BF16),
        ],
        jnp.stack([y, c]),
        rows,
        norm_gain[:1],
        small,
        *blocks,
        later,
        scratch=[((width, 2 * cols), BF16), (rows.shape, BF16)],
        scalars=1,
    )
    later, last = (
        lax.all_gather(p.reshape(-1, 1, deep, p.shape[1]), "y", axis=1, tiled=True)
        for p in (later, last)
    )
    got = shifted(send, "c", 1)
    out_t = jnp.concatenate([send[:width], got[:width]], axis=1)
    padded, other_table = call(
        meet_kernel,
        [((half + HALO, 2 * cols), F32), ((2 * table.shape[1], cols), F32)],
        keep,
        got,
    )
    tables = jnp.concatenate([table, other_table.reshape(table.shape)], axis=2)

    stream = lax.dynamic_slice_in_dim(stream_in, c * half, half, 0)
    for layer in range(2):
        if layer:
            gated, tail = call(
                functools.partial(second_kernel, cols),
                [((half, 2 * cols), BF16), ((HALO, 2 * cols), BF16)],
                stream,
                norm_gain[1:],
                mine,
                other,
                scratch=[(stream.shape, BF16)],
            )
            padded = jnp.concatenate([passed_on(tail, (*SP, "c")), gated], axis=0).astype(F32)
        filtered = jnp.zeros((half, 2 * cols), F32)
        for tap in range(kernel):
            at = HALO - kernel + 1 + tap
            filtered = filtered + tables[layer, tap] * padded[at : at + half]
        sums = jnp.stack([jnp.sum(filtered, axis=1), jnp.sum(filtered * filtered, axis=1)])
        if layer:
            last, sums = lax.optimization_barrier((last, sums))
            last = last.reshape(width, cols)
            out_t = jnp.concatenate([last, shifted(last, "c", 1)], axis=1)
        sums = jnp.sum(lax.all_gather(sums.reshape(1, -1), "x", axis=0), axis=0).reshape(2, half, 1)
        mean = sums[0] / width
        variance = sums[1] / width - mean * mean
        gain = tables[layer, kernel]
        activated = jax.nn.silu((filtered - mean) * lax.rsqrt(variance + epsilon) * gain).astype(BF16)
        branch = lax.dot_general(
            activated, out_t, (((1,), (1,)), ((), ())), preferred_element_type=F32
        ).astype(BF16)
        parts = lax.all_to_all(branch.reshape(xs, share, width), "x", 0, 0, tiled=True)
        own = lax.dynamic_slice_in_dim(stream, x * share, share, 0).astype(F32)
        own = (own + jnp.sum(parts.astype(F32), axis=0)).astype(BF16)
        if not layer:
            later, own = lax.optimization_barrier((later, own))
            mine = later.reshape(width, 2 * cols)
            other = shifted(mine, "c", 1)
        stream = lax.all_gather(own, "x", axis=0, tiled=True)
    sibling = shifted(stream, "c", 1)
    return jnp.where(
        c == 0,
        jnp.concatenate([stream, sibling], axis=0),
        jnp.concatenate([sibling, stream], axis=0),
    )


def solution(mesh):
    finer = Mesh(mesh.devices.reshape(16, 4, 4, 2), (*SP, *TP))
    placed = (
        P(SP, None),
        P(),
        P(None, SP, TP),
        P(None, SP, TP),
        P(None, None, TP),
        P(None, TP),
        P(None, TP, SP),
    )
    return jax.shard_map(body, mesh=finer, in_specs=placed, out_specs=P(SP, None), check_vma=False)
```

time: 235 us -> 214 us (0.911)
  the two profiles are of different devices: /device:TPU:33 before, /device:TPU:1 now
where the time goes in v2:
time: 214 us; the launch traced here: 213 us
  blocking collectives  81.8 us (38%)
  starting transfers between devices  51.3 us (24%)
  waiting for transfers between devices  28.6 us (13%)
  between operations  13.4 us (6%)
  local copies, waits for them, and re-layouts  11.6 us (5%)
  other arithmetic  11.4 us (5%)
  Pallas kernels  11.2 us (5%)
  matrix products  3.64 us (2%)
    ppermute x8, starting transfers between devices, shifted(): lax.ppermute(value, axis, [(i, (i + steps) % count) for i in range(count)])  40.5 us
    all_gather x1, blocking collectives, body(): block = lax.all_gather(first, 'z', axis=0, tiled=True)  35.3 us
    all_gather x2, blocking collectives, body(): stream = lax.all_gather(own, 'x', axis=0, tiled=True)  21.4 us
    all_gather x2, blocking collectives, body(): lax.all_gather(sums.reshape(1, -1), 'x', axis=0)  15.5 us
    pallas_call x3, Pallas kernels, call(): pl.pallas_call(kernel, out_shape=[jax.ShapeDtypeStruct(s, d) for s, d in...  11.2 us
    all_to_all x1, blocking collectives, body(): lax.all_to_all(branch.reshape(xs, share, width), 'x', 0, 0, tiled=True)  9.64 us
    ppermute x8, waiting for transfers between devices, shifted(): lax.ppermute(value, axis, [(i, (i + steps) % count) for i in range(count)])  9.25 us
    all_gather x2, waiting for transfers between devices, body(): lax.all_gather(p.reshape(-1, 1, deep, p.shape[1]), 'y', axis=1, tiled=True)  9.11 us
  transfers between devices with their start and end apart: 14, of which 10 were waited for; matrix products, arithmetic and copies ran while one was open for 8% of the time, Pallas kernels for 3%

profile of v2, /device:TPU:1, one launch (start us, length us, event | category | flops | bytes accessed | tf_op | source)
XLA Modules:
  0.0 212.9 jit_solution(10691287736993794050)
XLA Ops:
  8.2 1.6 slice.423
  9.7 35.3 %all_gather.24.refs_0_ = bf16[512,768]{1,0:T(8,128)(2,1)S(1)} all-gather(bf16[32,768]{1,0:T(8,128)(2,1)S(1)} %get-tuple-element.21), channel_id=1, replica_groups=mesh['z'=16,'y'=4,'x'=4,'c'=2] {'z'}, dimensions={0}, use_global_device_ids=true | all-gather | bytes 835584 | tf_op jit(solution)/shard_map/all_gather | solution.py:121
  45.0 3.1 %collective-permute-start.1 = (bf16[512,768]{1,0:T(8,128)(2,1)S(1)}, bf16[512,768]{1,0:T(8,128)(2,1)S(1)}, u32[]{:S(2)}, u32[]{:S(2)}) collective-permute-start(bf16[512,768]{1,0:T(8,128)(2,1)S(1)} %all_gather.24.refs_0_), channel_id=1, source_target_pairs={{0,8},{8,16},{16,24},{24,0},{1,9},{9,17},{17,25},{25,1},{2,10},{10... | collective-permute-start | bytes 2359304 | tf_op jit(solution)/shard_map/ppermute | solution.py:21
  48.2 3.3 %collective-permute-start.2 = (bf16[512,768]{1,0:T(8,128)(2,1)S(1)}, bf16[512,768]{1,0:T(8,128)(2,1)S(1)}, u32[]{:S(2)}, u32[]{:S(2)}) collective-permute-start(bf16[512,768]{1,0:T(8,128)(2,1)S(1)} %all_gather.24.refs_0_), channel_id=1, source_target_pairs={{0,24},{8,0},{16,8},{24,16},{1,25},{9,1},{17,9},{25,17},{2,26},{10... | collective-permute-start | bytes 2359304 | tf_op jit(solution)/shard_map/ppermute | solution.py:21
  51.5 2.6 %collective-permute-start = (bf16[32,2048]{1,0:T(8,128)(2,1)}, bf16[32,2048]{1,0:T(8,128)(2,1)}, u32[]{:S(2)}, u32[]{:S(2)}) collective-permute-start(bf16[32,2048]{1,0:T(8,128)(2,1)} %slice.423), channel_id=1, source_target_pairs={{0,8},{8,16},{16,24},{24,32},{32,40},{40,48},{48,56},{56,64},{64,7... | collective-permute-start | bytes 393224 | tf_op jit(solution)/shard_map/ppermute | solution.py:26
  57.1 2.3 %collective-permute-done.1.refs_1_ = bf16[512,768]{1,0:T(8,128)(2,1)S(1)} collective-permute-done((bf16[512,768]{1,0:T(8,128)(2,1)S(1)}, bf16[512,768]{1,0:T(8,128)(2,1)S(1)}, u32[]{:S(2)}, u32[]{:S(2)}) %collective-permute-start.1) | collective-permute-done | bytes 786464 | tf_op jit(solution)/shard_map/ppermute | solution.py:21
  59.4 1.9 collective-permute-start.3
  61.4 4.6 %collective-permute-start.4 = (bf16[256,768]{1,0:T(8,128)(2,1)S(1)}, bf16[256,768]{1,0:T(8,128)(2,1)}, u32[]{:S(2)}, u32[]{:S(2)}) collective-permute-start(bf16[256,768]{1,0:T(8,128)(2,1)S(1)} %slice.563), channel_id=1, source_target_pairs={{0,24},{8,0},{16,8},{24,16},{1,25},{9,1},{17,9},{25,17},{2,26},{10... | collective-permute-start | bytes 1179656 | tf_op jit(solution)/shard_map/ppermute | solution.py:21
  67.2 2.0 pad_maximum_fusion.rows_ref
  69.3 2.6 %collective-permute-done.3.refs_3_ = bf16[256,768]{1,0:T(8,128)(2,1)S(1)} collective-permute-done((bf16[256,768]{1,0:T(8,128)(2,1)S(1)}, bf16[256,768]{1,0:T(8,128)(2,1)S(1)}, u32[]{:S(2)}, u32[]{:S(2)}) %collective-permute-start.3) | collective-permute-done | bytes 393248 | tf_op jit(solution)/shard_map/ppermute | solution.py:21
  74.0 2.0 all-gather.4.cloned.1.call-done.refs_5_
  76.0 5.1 %shard_map.73 = (bf16[160,256]{1,0:T(8,128)(2,1)}, bf16[2400,256]{1,0:T(8,128)(2,1)}, bf16[512,512]{1,0:T(8,128)(2,1)}, bf16[512,256]{1,0:T(8,128)(2,1)}) custom-call(s32[2]{0:T(128)} %pad_add_fusion.at_ref, bf16[288,2048]{1,0:T(8,128)(2,1)} %pad_maximum_fusion.rows_ref, f32[1,2048]{1,0:T(1,128)} %get-tuple-element.113.gain_ref, bf16[192,256]{1,0:T(8,128)(2,1)} %bitcast.120, ...), custom_call_target="tpu_custom_call" | custom-call | tf_op jit(solution)/shard_map/pallas_call | solution.py:44
  81.1 12.1 %collective-permute-start.5 = (bf16[2400,256]{1,0:T(8,128)(2,1)}, bf16[2400,256]{1,0:T(8,128)(2,1)S(1)}, u32[]{:S(2)}, u32[]{:S(2)}) collective-permute-start(bf16[2400,256]{1,0:T(8,128)(2,1)} %get-tuple-element.27), channel_id=1, source_target_pairs={{0,1},{1,0},{2,3},{3,2},{4,5},{5,4},{6,7},{7,6},{8,9},{9,8},{10,11... | collective-permute-start | bytes 3686408 | tf_op jit(solution)/shard_map/ppermute | solution.py:21
  97.1 2.1 shard_map.74
  101.1 1.8 fusion.55
  103.0 7.8 %all_gather.27 = f32[4,1,256]{2,1,0:T(1,128)S(1)} all-gather(f32[1,1,256]{2,1,0:T(1,128)S(1)} %bitcast.189), channel_id=1, replica_groups=mesh['z'=16,'y'=4,'x'=4,'c'=2] {'x'}, dimensions={0}, use_global_device_ids=true | all-gather | bytes 5120 | tf_op jit(solution)/shard_map/all_gather | solution.py:184
  111.7 1.6 convolution_convert_fusion.1
  113.4 3.5 %all-to-all-start = ((bf16[4,32,2048]{2,1,0:T(8,128)(2,1)}), bf16[4,32,2048]{2,1,0:T(8,128)(2,1)S(1)}, u32[]{:S(2)}, u32[]{:S(2)}) async-start(bf16[4,32,2048]{2,1,0:T(8,128)(2,1)} %bitcast.118), calls=%async_computation | async-start | bytes 1048576 | tf_op jit(solution)/shard_map/all_to_all | solution.py:192
  116.9 6.9 %all-to-all-done = bf16[4,32,2048]{2,1,0:T(8,128)(2,1)S(1)} async-done(((bf16[4,32,2048]{2,1,0:T(8,128)(2,1)}), bf16[4,32,2048]{2,1,0:T(8,128)(2,1)S(1)}, u32[]{:S(2)}, u32[]{:S(2)}) %all-to-all-start) | async-done | bytes 524320 | tf_op jit(solution)/shard_map/all_to_all | solution.py:192
  123.9 4.5 %all-gather.6.cloned.1.call-done = bf16[16,4,32,512]{3,2,1,0:T(8,128)(2,1)} async-done(((bf16[16,1,32,512]{3,2,1,0:T(8,128)(2,1)}), bf16[16,4,32,512]{3,2,1,0:T(8,128)(2,1)}) %all-gather.6.cloned.1.call-update) | async-done | bytes 2097168 | tf_op jit(solution)/shard_map/all_gather | solution.py:149
  128.4 2.7 %collective-permute-start.6 = (bf16[2048,512]{1,0:T(8,128)(2,1)}, bf16[2048,512]{1,0:T(8,128)(2,1)S(1)}, u32[]{:S(2)}, u32[]{:S(2)}) collective-permute-start(bf16[2048,512]{1,0:T(8,128)(2,1)} %bitcast.115), channel_id=1, source_target_pairs={{0,1},{1,0},{2,3},{3,2},{4,5},{5,4},{6,7},{7,6},{8,9},{9,8},{10,11... | collective-permute-start | bytes 6291464 | tf_op jit(solution)/shard_map/ppermute | solution.py:21
  131.2 11.5 %all_gather.28.rows_ref = bf16[128,2048]{1,0:T(8,128)(2,1)} all-gather(bf16[32,2048]{1,0:T(8,128)(2,1)S(1)} %add_convert_fusion.1), channel_id=1, replica_groups=mesh['z'=16,'y'=4,'x'=4,'c'=2] {'x'}, dimensions={0}, use_global_device_ids=true | all-gather | bytes 655360 | tf_op jit(solution)/shard_map/all_gather | solution.py:199
  144.0 3.9 %shard_map.75 = (bf16[128,512]{1,0:T(8,128)(2,1)}, bf16[32,512]{1,0:T(8,128)(2,1)}) custom-call(bf16[128,2048]{1,0:T(8,128)(2,1)} %all_gather.28.rows_ref, f32[1,2048]{1,0:T(1,128)} %get-tuple-element.112.gain_ref, bf16[2048,512]{1,0:T(8,128)(2,1)} %bitcast.116, bf16[2048,512]{1,0:T(8,128)(2,1)} %copy-done.3), custom_call_target="tpu_custom_call" | custom-call | tf_op jit(solution)/shard_map/pallas_call | solution.py:44
  147.9 4.6 %collective-permute-start.7 = (bf16[32,512]{1,0:T(8,128)(2,1)}, bf16[32,512]{1,0:T(8,128)(2,1)S(1)}, u32[]{:S(2)}, u32[]{:S(2)}) collective-permute-start(bf16[32,512]{1,0:T(8,128)(2,1)} %get-tuple-element.32), channel_id=1, source_target_pairs={{0,1},{1,8},{8,9},{9,16},{16,17},{17,24},{24,25},{25,32},{32,33},{... | collective-permute-start | bytes 98312 | tf_op jit(solution)/shard_map/ppermute | solution.py:26
  156.0 4.6 %all-gather.8.cloned.1.call-done = bf16[16,4,32,256]{3,2,1,0:T(8,128)(2,1)} async-done(((bf16[16,1,32,256]{3,2,1,0:T(8,128)(2,1)}), bf16[16,4,32,256]{3,2,1,0:T(8,128)(2,1)}) %all-gather.8.cloned.1.call-update) | async-done | bytes 1048592 | tf_op jit(solution)/shard_map/all_gather | solution.py:149
  160.6 4.6 %collective-permute-start.8 = (bf16[2048,256]{1,0:T(8,128)(2,1)}, bf16[2048,256]{1,0:T(8,128)(2,1)S(1)}, u32[]{:S(2)}, u32[]{:S(2)}) collective-permute-start(bf16[2048,256]{1,0:T(8,128)(2,1)} %bitcast.200), channel_id=1, source_target_pairs={{0,1},{1,0},{2,3},{3,2},{4,5},{5,4},{6,7},{7,6},{8,9},{9,8},{10,11... | collective-permute-start | bytes 3145736 | tf_op jit(solution)/shard_map/ppermute | solution.py:21
  165.3 7.6 %all_gather.30 = f32[4,1,256]{2,1,0:T(1,128)S(1)} all-gather(f32[1,1,256]{2,1,0:T(1,128)S(1)} %bitcast.188), channel_id=1, replica_groups=mesh['z'=16,'y'=4,'x'=4,'c'=2] {'x'}, dimensions={0}, use_global_device_ids=true | all-gather | bytes 5120 | tf_op jit(solution)/shard_map/all_gather | solution.py:184
  173.0 2.0 convolution_convert_fusion
  175.0 9.6 %all_to_all.10 = bf16[4,32,2048]{2,1,0:T(8,128)(2,1)S(1)} all-to-all(bf16[4,32,2048]{2,1,0:T(8,128)(2,1)S(1)} %bitcast.119), channel_id=1, replica_groups=mesh['z'=16,'y'=4,'x'=4,'c'=2] {'x'}, dimensions={0} | all-to-all | bytes 1048576 | tf_op jit(solution)/shard_map/all_to_all | solution.py:192
  185.7 9.9 %all_gather.31 = bf16[128,2048]{1,0:T(8,128)(2,1)S(1)} all-gather(bf16[32,2048]{1,0:T(8,128)(2,1)S(1)} %add_convert_fusion), channel_id=1, replica_groups=mesh['z'=16,'y'=4,'x'=4,'c'=2] {'x'}, dimensions={0}, use_global_device_ids=true | all-gather | bytes 655360 | tf_op jit(solution)/shard_map/all_gather | solution.py:199
  195.6 8.0 %collective-permute-start.9 = (bf16[128,2048]{1,0:T(8,128)(2,1)S(1)}, bf16[128,2048]{1,0:T(8,128)(2,1)S(1)}, u32[]{:S(2)}, u32[]{:S(2)}) collective-permute-start(bf16[128,2048]{1,0:T(8,128)(2,1)S(1)} %all_gather.31), channel_id=1, source_target_pairs={{0,1},{1,0},{2,3},{3,2},{4,5},{5,4},{6,7},{7,6},{8,9},{9,8},{10,11... | collective-permute-start | bytes 1572872 | tf_op jit(solution)/shard_map/ppermute | solution.py:21
  203.6 1.5 collective-permute-done.9
  (68 shorter events, 21.9 us)
Async XLA Ops:
  6.5 60.7 %copy-start.6 = (bf16[256,2048]{1,0:T(8,128)(2,1)S(1)}, bf16[256,2048]{1,0:T(8,128)(2,1)}, u32[]{:S(2)}) copy-start(bf16[256,2048]{1,0:T(8,128)(2,1)} %param.7) | copy-start | bytes 3145732
  6.5 69.5 %all-gather.4.cloned.1.call-start = ((), (), s32[]{:S(2)}) async-start(), calls=%async_computation.2 | async-start | bytes 1114112 | tf_op jit(solution)/shard_map/all_gather | solution.py:120
  8.1 120.3 %all-gather.6.cloned.1.call-start = ((), (), s32[]{:S(2)}) async-start(), calls=%async_computation.3 | async-start | bytes 2621440 | tf_op jit(solution)/shard_map/all_gather | solution.py:149
  45.0 24.2 %copy-start.2 = (bf16[512,768]{1,0:T(8,128)(2,1)}, bf16[512,768]{1,0:T(8,128)(2,1)S(1)}, u32[]{:S(2)}) copy-start(bf16[512,768]{1,0:T(8,128)(2,1)S(1)} %all_gather.24.refs_0_) | copy-start | bytes 2359300
  45.0 14.4 %collective-permute-start.1 = (bf16[512,768]{1,0:T(8,128)(2,1)S(1)}, bf16[512,768]{1,0:T(8,128)(2,1)S(1)}, u32[]{:S(2)}, u32[]{:S(2)}) collective-permute-start(bf16[512,768]{1,0:T(8,128)(2,1)S(1)} %all_gather.24.refs_0_), channel_id=1, source_target_pairs={{0,8},{8,16},{16,24},{24,0},{1,9},{9,17},{17,25},{25,1},{2,10},{10... | collective-permute-start | bytes 2359304 | tf_op jit(solution)/shard_map/ppermute | solution.py:21
  48.2 13.2 %collective-permute-start.2 = (bf16[512,768]{1,0:T(8,128)(2,1)S(1)}, bf16[512,768]{1,0:T(8,128)(2,1)S(1)}, u32[]{:S(2)}, u32[]{:S(2)}) collective-permute-start(bf16[512,768]{1,0:T(8,128)(2,1)S(1)} %all_gather.24.refs_0_), channel_id=1, source_target_pairs={{0,24},{8,0},{16,8},{24,16},{1,25},{9,1},{17,9},{25,17},{2,26},{10... | collective-permute-start | bytes 2359304 | tf_op jit(solution)/shard_map/ppermute | solution.py:21
  51.5 15.7 %collective-permute-start = (bf16[32,2048]{1,0:T(8,128)(2,1)}, bf16[32,2048]{1,0:T(8,128)(2,1)}, u32[]{:S(2)}, u32[]{:S(2)}) collective-permute-start(bf16[32,2048]{1,0:T(8,128)(2,1)} %slice.423), channel_id=1, source_target_pairs={{0,8},{8,16},{16,24},{24,32},{32,40},{40,48},{48,56},{56,64},{64,7... | collective-permute-start | bytes 393224 | tf_op jit(solution)/shard_map/ppermute | solution.py:26
  59.4 16.6 %copy-start.4 = (bf16[512,768]{1,0:T(8,128)(2,1)}, bf16[512,768]{1,0:T(8,128)(2,1)S(1)}, u32[]{:S(2)}) copy-start(bf16[512,768]{1,0:T(8,128)(2,1)S(1)} %collective-permute-done.1.refs_1_) | copy-start | bytes 2359300
  59.4 12.4 %collective-permute-start.3 = (bf16[256,768]{1,0:T(8,128)(2,1)S(1)}, bf16[256,768]{1,0:T(8,128)(2,1)S(1)}, u32[]{:S(2)}, u32[]{:S(2)}) collective-permute-start(bf16[256,768]{1,0:T(8,128)(2,1)S(1)} %slice.562), channel_id=1, source_target_pairs={{0,8},{8,16},{16,24},{24,0},{1,9},{9,17},{17,25},{25,1},{2,10},{10... | collective-permute-start | bytes 1179656 | tf_op jit(solution)/shard_map/ppermute | solution.py:21
  61.4 14.6 %copy-start.5 = (bf16[512,768]{1,0:T(8,128)(2,1)}, bf16[512,768]{1,0:T(8,128)(2,1)S(1)}, u32[]{:S(2)}) copy-start(bf16[512,768]{1,0:T(8,128)(2,1)S(1)} %collective-permute-done.2.refs_2_) | copy-start | bytes 2359300
  61.4 12.6 %collective-permute-start.4 = (bf16[256,768]{1,0:T(8,128)(2,1)S(1)}, bf16[256,768]{1,0:T(8,128)(2,1)}, u32[]{:S(2)}, u32[]{:S(2)}) collective-permute-start(bf16[256,768]{1,0:T(8,128)(2,1)S(1)} %slice.563), channel_id=1, source_target_pairs={{0,24},{8,0},{16,8},{24,16},{1,25},{9,1},{17,9},{25,17},{2,26},{10... | collective-permute-start | bytes 1179656 | tf_op jit(solution)/shard_map/ppermute | solution.py:21
  71.9 0.7 copy-start.7
  81.1 19.0 %copy-start.9 = (f32[2,256]{1,0:T(2,128)S(1)}, f32[2,256]{1,0:T(2,128)}, u32[]{:S(2)}) copy-start(f32[2,256]{1,0:T(2,128)} %param.12) | copy-start | bytes 6148
  81.1 14.9 %collective-permute-start.5 = (bf16[2400,256]{1,0:T(8,128)(2,1)}, bf16[2400,256]{1,0:T(8,128)(2,1)S(1)}, u32[]{:S(2)}, u32[]{:S(2)}) collective-permute-start(bf16[2400,256]{1,0:T(8,128)(2,1)} %get-tuple-element.27), channel_id=1, source_target_pairs={{0,1},{1,0},{2,3},{3,2},{4,5},{5,4},{6,7},{7,6},{8,9},{9,8},{10,11... | collective-permute-start | bytes 3686408 | tf_op jit(solution)/shard_map/ppermute | solution.py:21
  96.0 1.0 copy-start.1
  99.2 2.0 copy-start
  102.9 7.9 %slice-start = ((bf16[2400,256]{1,0:T(8,128)(2,1)}), bf16[2048,256]{1,0:T(8,128)(2,1)S(1)}, s32[]{:S(2)}) async-start(bf16[2400,256]{1,0:T(8,128)(2,1)} %copy-done.1), calls=%async_computation.5 | async-start | bytes 2097152 | tf_op jit(solution)/shard_map/slice | solution.py:153
  110.8 1.0 copy-start.8
  113.4 10.4 %all-to-all-start = ((bf16[4,32,2048]{2,1,0:T(8,128)(2,1)}), bf16[4,32,2048]{2,1,0:T(8,128)(2,1)S(1)}, u32[]{:S(2)}, u32[]{:S(2)}) async-start(bf16[4,32,2048]{2,1,0:T(8,128)(2,1)} %bitcast.118), calls=%async_computation | async-start | bytes 1048576 | tf_op jit(solution)/shard_map/all_to_all | solution.py:192
  116.8 43.8 %all-gather.8.cloned.1.call-start = ((), (), s32[]{:S(2)}) async-start(), calls=%async_computation.4 | async-start | bytes 1310720 | tf_op jit(solution)/shard_map/all_gather | solution.py:149
  128.4 14.2 %collective-permute-start.6 = (bf16[2048,512]{1,0:T(8,128)(2,1)}, bf16[2048,512]{1,0:T(8,128)(2,1)S(1)}, u32[]{:S(2)}, u32[]{:S(2)}) collective-permute-start(bf16[2048,512]{1,0:T(8,128)(2,1)} %bitcast.115), channel_id=1, source_target_pairs={{0,1},{1,0},{2,3},{3,2},{4,5},{5,4},{6,7},{7,6},{8,9},{9,8},{10,11... | collective-permute-start | bytes 6291464 | tf_op jit(solution)/shard_map/ppermute | solution.py:21
  142.7 1.3 copy-start.3
  147.9 6.0 %collective-permute-start.7 = (bf16[32,512]{1,0:T(8,128)(2,1)}, bf16[32,512]{1,0:T(8,128)(2,1)S(1)}, u32[]{:S(2)}, u32[]{:S(2)}) collective-permute-start(bf16[32,512]{1,0:T(8,128)(2,1)} %get-tuple-element.32), channel_id=1, source_target_pairs={{0,1},{1,8},{8,9},{9,16},{16,17},{17,24},{24,25},{25,32},{32,33},{... | collective-permute-start | bytes 98312 | tf_op jit(solution)/shard_map/ppermute | solution.py:26
  160.6 12.4 %collective-permute-start.8 = (bf16[2048,256]{1,0:T(8,128)(2,1)}, bf16[2048,256]{1,0:T(8,128)(2,1)S(1)}, u32[]{:S(2)}, u32[]{:S(2)}) collective-permute-start(bf16[2048,256]{1,0:T(8,128)(2,1)} %bitcast.200), channel_id=1, source_target_pairs={{0,1},{1,0},{2,3},{3,2},{4,5},{5,4},{6,7},{7,6},{8,9},{9,8},{10,11... | collective-permute-start | bytes 3145736 | tf_op jit(solution)/shard_map/ppermute | solution.py:21
  195.6 9.5 %collective-permute-start.9 = (bf16[128,2048]{1,0:T(8,128)(2,1)S(1)}, bf16[128,2048]{1,0:T(8,128)(2,1)S(1)}, u32[]{:S(2)}, u32[]{:S(2)}) collective-permute-start(bf16[128,2048]{1,0:T(8,128)(2,1)S(1)} %all_gather.31), channel_id=1, source_target_pairs={{0,1},{1,0},{2,3},{3,2},{4,5},{5,4},{6,7},{7,6},{8,9},{9,8},{10,11... | collective-permute-start | bytes 1572872 | tf_op jit(solution)/shard_map/ppermute | solution.py:21
Sparse Core Ops, SparseCore 0:
  9.4 66.5 all-gather.3
  93.4 34.9 all-gather.5
  131.3 29.2 all-gather.7

commit v3 on v2

--- a/solution.py
+++ b/solution.py
@@ -64,8 +64,8 @@
     return (value * jax.nn.sigmoid(gate)).astype(BF16)
 
 
-def first_kernel(cols, deep, ys, at_ref, rows_ref, gain_ref, small_ref, *refs):
-    *blocks, pair_ref, keep_ref, send_ref, later_ref, last_ref, weights, scaled = refs
+def first_kernel(cols, deep, ys, at_ref, rows_ref, small_ref, *refs):
+    *blocks, pair_ref, keep_ref, send_ref, later_ref, last_ref, weights = refs
     later_ref[...] = pair_ref[:, : 2 * cols]
     last_ref[...] = pair_ref[:, 2 * cols : 3 * cols]
     here, c = at_ref[0], at_ref[1]
@@ -77,8 +77,7 @@
             rows = pl.ds(pl.multiple_of(at + where, deep), deep)
             weights[rows, :] = ref[k * deep : (k + 1) * deep, : 2 * cols]
             send_ref[rows, :] = ref[k * deep : (k + 1) * deep, 2 * cols :]
-    normed(rows_ref, gain_ref, scaled)
-    gated = gate_of(scaled[...], weights, cols)
+    gated = gate_of(rows_ref[...], weights, cols)
     count = keep_ref.shape[0]
     low, high = gated[:count], gated[rows_ref.shape[0] - count :]
     keep_ref[...] = jnp.where(c == 0, low, high)
@@ -87,12 +86,15 @@
     send_ref[at + count :, :] = small_ref[...]
 
 
-def second_kernel(cols, rows_ref, gain_ref, mine_ref, other_ref, gated_ref, tail_ref, scaled):
+def second_kernel(cols, rows_ref, gain_ref, later_ref, gated_ref, tail_ref, scaled, weights):
     normed(rows_ref, gain_ref, scaled)
-    for k, w_ref in enumerate((mine_ref, other_ref)):
-        part = gate_of(scaled[...], w_ref, cols)
-        gated_ref[:, k * cols : (k + 1) * cols] = part
-        tail_ref[:, (1 - k) * cols : (2 - k) * cols] = part[-HALO:]
+    zs, cores, deep, _ = later_ref.shape
+    for core in range(cores):
+        for k in range(zs):
+            weights[k * deep : (k + 1) * deep, :] = later_ref[k, core]
+        part = gate_of(scaled[...], weights, cols)
+        gated_ref[:, core * cols : (core + 1) * cols] = part
+        tail_ref[:, core * cols : (core + 1) * cols] = part[-HALO:]
 
 
 def meet_kernel(keep_ref, got_ref, padded_ref, other_ref):
@@ -114,17 +116,24 @@
     xs = lax.axis_size("x")
     share = half // xs
 
-    raw = jnp.concatenate([value_weight, gate_weight, jnp.swapaxes(out_weight, 1, 2)], axis=2)
-    deep, wide = raw.shape[1:]
-    padded, first = lax.optimization_barrier((jnp.pad(raw[1], ((0, 0), (0, cols))), raw[0]))
+    turned = jnp.swapaxes(out_weight, 1, 2)
+    first, padded = (
+        jnp.concatenate([value_weight[k], gate_weight[k]] + [turned[k]] * (k + 1), axis=1)
+        for k in range(2)
+    )
+    padded, first = lax.optimization_barrier((padded, first))
+    deep = first.shape[0]
     later = lax.all_gather(padded, "z", axis=0, tiled=True)
     block = lax.all_gather(first, "z", axis=0, tiled=True)
-    block, edge = lax.optimization_barrier((block, stream_in[-HALO:]))
-    before = passed_on(edge, SP)
+    block, source = lax.optimization_barrier((block, stream_in))
+    before = passed_on(source[-HALO:], SP)
     middle = block.shape[0] // 2
     up, down = shifted(block, "y", 1), shifted(block, "y", -1)
+    up, down, before = lax.optimization_barrier((up, down, before))
     blocks = (block, up, down, shifted(up[:middle], "y", 1), shifted(down[middle:], "y", -1))
-    rows = jnp.concatenate([before, stream_in], axis=0)
+    rows = jnp.concatenate([before, stream_in], axis=0).astype(F32)
+    rows = rows * lax.rsqrt(jnp.mean(rows * rows, axis=1, keepdims=True) + epsilon) * norm_gain[0]
+    rows = rows.astype(BF16)
     table = jnp.concatenate([conv_taps, channel_gain[:, None]], axis=1)
     small = in_parts(table).reshape(-1, cols)
 
@@ -138,15 +147,14 @@
         ],
         jnp.stack([y, c]),
         rows,
-        norm_gain[:1],
         small,
         *blocks,
         later,
-        scratch=[((width, 2 * cols), BF16), (rows.shape, BF16)],
+        scratch=[((width, 2 * cols), BF16)],
         scalars=1,
     )
     later, last = (
-        lax.all_gather(p.reshape(-1, 1, deep, p.shape[1]), "y", axis=1, tiled=True)
+        lax.all_gather(p.reshape(-1, 1, deep, p.shape[1]), ("c", "y"), axis=1, tiled=True)
         for p in (later, last)
     )
     got = shifted(send, "c", 1)
@@ -157,7 +165,9 @@
         keep,
         got,
     )
-    tables = jnp.concatenate([table, other_table.reshape(table.shape)], axis=2)
+    pair = (table, other_table.reshape(table.shape))
+    ordered = jnp.where(c == 0, jnp.concatenate(pair, 2)[1], jnp.concatenate(pair[::-1], 2)[1])
+    tables = (jnp.concatenate(pair, 2)[0], ordered)
 
     stream = lax.dynamic_slice_in_dim(stream_in, c * half, half, 0)
     for layer in range(2):
@@ -167,24 +177,23 @@
                 [((half, 2 * cols), BF16), ((HALO, 2 * cols), BF16)],
                 stream,
                 norm_gain[1:],
-                mine,
-                other,
-                scratch=[(stream.shape, BF16)],
+                later.reshape(lax.axis_size("z"), 2, -1, 2 * cols),
+                scratch=[(stream.shape, BF16), ((width, 2 * cols), BF16)],
             )
             padded = jnp.concatenate([passed_on(tail, (*SP, "c")), gated], axis=0).astype(F32)
         filtered = jnp.zeros((half, 2 * cols), F32)
         for tap in range(kernel):
             at = HALO - kernel + 1 + tap
-            filtered = filtered + tables[layer, tap] * padded[at : at + half]
+            filtered = filtered + tables[layer][tap] * padded[at : at + half]
         sums = jnp.stack([jnp.sum(filtered, axis=1), jnp.sum(filtered * filtered, axis=1)])
+        sums = jnp.sum(lax.all_gather(sums.reshape(1, -1), "x", axis=0), axis=0).reshape(2, half, 1)
         if layer:
             last, sums = lax.optimization_barrier((last, sums))
-            last = last.reshape(width, cols)
-            out_t = jnp.concatenate([last, shifted(last, "c", 1)], axis=1)
-        sums = jnp.sum(lax.all_gather(sums.reshape(1, -1), "x", axis=0), axis=0).reshape(2, half, 1)
+            last = last.reshape(lax.axis_size("z"), 2, -1, cols)
+            out_t = jnp.concatenate([last[:, k].reshape(width, cols) for k in range(2)], axis=1)
         mean = sums[0] / width
         variance = sums[1] / width - mean * mean
-        gain = tables[layer, kernel]
+        gain = tables[layer][kernel]
         activated = jax.nn.silu((filtered - mean) * lax.rsqrt(variance + epsilon) * gain).astype(BF16)
         branch = lax.dot_general(
             activated, out_t, (((1,), (1,)), ((), ())), preferred_element_type=F32
@@ -192,10 +201,6 @@
         parts = lax.all_to_all(branch.reshape(xs, share, width), "x", 0, 0, tiled=True)
         own = lax.dynamic_slice_in_dim(stream, x * share, share, 0).astype(F32)
         own = (own + jnp.sum(parts.astype(F32), axis=0)).astype(BF16)
-        if not layer:
-            later, own = lax.optimization_barrier((later, own))
-            mine = later.reshape(width, 2 * cols)
-            other = shifted(mine, "c", 1)
         stream = lax.all_gather(own, "x", axis=0, tiled=True)
     sibling = shifted(stream, "c", 1)
     return jnp.where(

time: 214 us -> 206 us (0.963)
  starting transfers between devices: 51.3 us -> 46.4 us
  waiting for transfers between devices: 28.6 us -> 23.9 us
  blocking collectives: 81.8 us -> 84 us
    ppermute x8 -> x6, starting transfers between devices: 40.5 us -> 31.6 us  [shifted(): lax.ppermute(value, axis, [(i, (i + steps) % count) for i in range(count)])]
    ppermute x2, starting transfers between devices: 7.26 us -> 11.2 us  [passed_on(): return lax.ppermute(value, axes, [(i, i + 1) for i in range(count - 1)])]
    concatenate x3 -> x2, other arithmetic: 3.8 us -> 0.63 us  [body(): jnp.concatenate([value_weight[k], gate_weight[k]] + [turned[k]] * (k + 1)...]
    all_to_all x1, blocking collectives: 9.64 us -> 12.8 us  [body(): lax.all_to_all(branch.reshape(xs, share, width), 'x', 0, 0, tiled=True)]
    ppermute x8 -> x6, waiting for transfers between devices: 9.25 us -> 6.26 us  [shifted(): lax.ppermute(value, axis, [(i, (i + steps) % count) for i in range(count)])]
    all_gather x2, waiting for transfers between devices: 9.11 us -> 6.18 us  [body(): lax.all_gather(p.reshape(-1, 1, deep, p.shape[1]), ('c', 'y'), axis=1, ti...]
  transfers between devices with their start and end apart: 14 -> 12, of which waited for: 10 -> 10; matrix products, arithmetic and copies ran while one was open for 8% -> 8% of each run, Pallas kernels for 3% -> 3%
where the time goes in v3:
time: 206 us; the launch traced here: 205 us
  blocking collectives  84 us (41%)
  starting transfers between devices  46.4 us (23%)
  waiting for transfers between devices  23.9 us (12%)
  local copies, waits for them, and re-layouts  13.4 us (7%)
  between operations  13.4 us (7%)
  other arithmetic  11 us (5%)
  Pallas kernels  10.8 us (5%)
  matrix products  2.42 us (1%)
    all_gather x1, blocking collectives, body(): block = lax.all_gather(first, 'z', axis=0, tiled=True)  35.4 us
    ppermute x6, starting transfers between devices, shifted(): lax.ppermute(value, axis, [(i, (i + steps) % count) for i in range(count)])  31.6 us
    all_gather x2, blocking collectives, body(): stream = lax.all_gather(own, 'x', axis=0, tiled=True)  21.2 us
    all_gather x2, blocking collectives, body(): lax.all_gather(sums.reshape(1, -1), 'x', axis=0)  14.6 us
    all_to_all x1, blocking collectives, body(): lax.all_to_all(branch.reshape(xs, share, width), 'x', 0, 0, tiled=True)  12.8 us
    ppermute x2, starting transfers between devices, passed_on(): return lax.ppermute(value, axes, [(i, i + 1) for i in range(count - 1)])  11.2 us
    pallas_call x3, Pallas kernels, call(): pl.pallas_call(kernel, out_shape=[jax.ShapeDtypeStruct(s, d) for s, d in...  10.8 us
    all_to_all x1, waiting for transfers between devices, body(): lax.all_to_all(branch.reshape(xs, share, width), 'x', 0, 0, tiled=True)  6.76 us
  transfers between devices with their start and end apart: 12, of which 10 were waited for; matrix products, arithmetic and copies ran while one was open for 8% of the time, Pallas kernels for 3%

profile of v3, /device:TPU:1, one launch (start us, length us, event | category | flops | bytes accessed | tf_op | source)
XLA Modules:
  0.0 205.5 jit_solution(2921686807695562064)
XLA Ops:
  8.8 35.4 %all_gather.24.refs_0_ = bf16[512,768]{1,0:T(8,128)(2,1)S(1)} all-gather(bf16[32,768]{1,0:T(8,128)(2,1)S(1)} %pad_maximum_fusion.8), channel_id=1, replica_groups=mesh['z'=16,'y'=4,'x'=4,'c'=2] {'z'}, dimensions={0}, use_global_device_ids=true | all-gather | bytes 835584 | tf_op jit(solution)/shard_map/all_gather | solution.py:127
  44.3 3.0 %collective-permute-start = (bf16[512,768]{1,0:T(8,128)(2,1)S(1)}, bf16[512,768]{1,0:T(8,128)(2,1)S(1)}, u32[]{:S(2)}, u32[]{:S(2)}) collective-permute-start(bf16[512,768]{1,0:T(8,128)(2,1)S(1)} %all_gather.24.refs_0_), channel_id=1, source_target_pairs={{0,8},{8,16},{16,24},{24,0},{1,9},{9,17},{17,25},{25,1},{2,10},{10... | collective-permute-start | bytes 2359304 | tf_op jit(solution)/shard_map/ppermute | solution.py:21
  47.3 3.4 %collective-permute-start.1 = (bf16[512,768]{1,0:T(8,128)(2,1)S(1)}, bf16[512,768]{1,0:T(8,128)(2,1)S(1)}, u32[]{:S(2)}, u32[]{:S(2)}) collective-permute-start(bf16[512,768]{1,0:T(8,128)(2,1)S(1)} %all_gather.24.refs_0_), channel_id=1, source_target_pairs={{0,24},{8,0},{16,8},{24,16},{1,25},{9,1},{17,9},{25,17},{2,26},{10... | collective-permute-start | bytes 2359304 | tf_op jit(solution)/shard_map/ppermute | solution.py:21
  50.8 1.6 slice.546
  52.3 1.8 collective-permute-start.2
  54.2 1.5 copy.28
  57.2 1.4 fusion.62
  61.0 3.1 %collective-permute-start.3 = (bf16[256,768]{1,0:T(8,128)(2,1)S(1)}, bf16[256,768]{1,0:T(8,128)(2,1)S(1)}, u32[]{:S(2)}, u32[]{:S(2)}) collective-permute-start(bf16[256,768]{1,0:T(8,128)(2,1)S(1)} %slice.548), channel_id=1, source_target_pairs={{0,8},{8,16},{16,24},{24,0},{1,9},{9,17},{17,25},{25,1},{2,10},{10... | collective-permute-start | bytes 1179656 | tf_op jit(solution)/shard_map/ppermute | solution.py:21
  64.1 4.0 %collective-permute-start.4 = (bf16[256,768]{1,0:T(8,128)(2,1)S(1)}, bf16[256,768]{1,0:T(8,128)(2,1)}, u32[]{:S(2)}, u32[]{:S(2)}) collective-permute-start(bf16[256,768]{1,0:T(8,128)(2,1)S(1)} %slice.549), channel_id=1, source_target_pairs={{0,24},{8,0},{16,8},{24,16},{1,25},{9,1},{17,9},{25,17},{2,26},{10... | collective-permute-start | bytes 1179656 | tf_op jit(solution)/shard_map/ppermute | solution.py:21
  68.5 1.4 fusion.2.rows_ref
  69.8 1.8 collective-permute-done.3.refs_3_
  72.9 3.3 %all-gather.4.cloned.1.call-done.refs_5_ = bf16[512,1024]{1,0:T(8,128)(2,1)} async-done(((bf16[32,1024]{1,0:T(8,128)(2,1)}), bf16[512,1024]{1,0:T(8,128)(2,1)}) %all-gather.4.cloned.1.call-update) | async-done | bytes 1048592 | tf_op jit(solution)/shard_map/all_gather | solution.py:126
  76.2 4.8 %shard_map.73 = (bf16[160,256]{1,0:T(8,128)(2,1)}, bf16[2400,256]{1,0:T(8,128)(2,1)}, bf16[512,512]{1,0:T(8,128)(2,1)}, bf16[512,256]{1,0:T(8,128)(2,1)}) custom-call(s32[2]{0:T(128)} %pad_add_fusion.at_ref, bf16[288,2048]{1,0:T(8,128)(2,1)} %fusion.2.rows_ref, bf16[192,256]{1,0:T(8,128)(2,1)} %bitcast.133, bf16[512,768]{1,0:T(8,128)(2,1)} %copy-done.4, ...), custom_call_target="tpu_custom_call" | custom-call | tf_op jit(solution)/shard_map/pallas_call | solution.py:44
  81.2 11.9 %collective-permute-start.5 = (bf16[2400,256]{1,0:T(8,128)(2,1)}, bf16[2400,256]{1,0:T(8,128)(2,1)S(1)}, u32[]{:S(2)}, u32[]{:S(2)}) collective-permute-start(bf16[2400,256]{1,0:T(8,128)(2,1)} %get-tuple-element.30), channel_id=1, source_target_pairs={{0,1},{1,0},{2,3},{3,2},{4,5},{5,4},{6,7},{7,6},{8,9},{9,8},{10,11... | collective-permute-start | bytes 3686408 | tf_op jit(solution)/shard_map/ppermute | solution.py:21
  94.4 1.4 collective-permute-done.5.got_ref
  96.8 2.1 %shard_map.74 = (f32[160,512]{1,0:T(8,128)}, f32[64,256]{1,0:T(8,128)}) custom-call(bf16[160,256]{1,0:T(8,128)(2,1)} %get-tuple-element.29.keep_ref, bf16[2400,256]{1,0:T(8,128)(2,1)} %copy-done.2), custom_call_target="tpu_custom_call" | custom-call | tf_op jit(solution)/shard_map/pallas_call | solution.py:44
  100.0 1.8 fusion.57
  101.9 7.6 %all_gather.26 = f32[4,1,256]{2,1,0:T(1,128)S(1)} all-gather(f32[1,1,256]{2,1,0:T(1,128)S(1)} %bitcast.208), channel_id=1, replica_groups=mesh['z'=16,'y'=4,'x'=4,'c'=2] {'x'}, dimensions={0}, use_global_device_ids=true | all-gather | bytes 5120 | tf_op jit(solution)/shard_map/all_gather | solution.py:189
  110.5 1.6 convolution_convert_fusion.1
  112.1 3.5 %all-to-all-start = ((bf16[4,32,2048]{2,1,0:T(8,128)(2,1)}), bf16[4,32,2048]{2,1,0:T(8,128)(2,1)S(1)}, u32[]{:S(2)}, u32[]{:S(2)}) async-start(bf16[4,32,2048]{2,1,0:T(8,128)(2,1)} %bitcast.131), calls=%async_computation | async-start | bytes 1048576 | tf_op jit(solution)/shard_map/all_to_all | solution.py:201
  115.7 6.8 %all-to-all-done = bf16[4,32,2048]{2,1,0:T(8,128)(2,1)S(1)} async-done(((bf16[4,32,2048]{2,1,0:T(8,128)(2,1)}), bf16[4,32,2048]{2,1,0:T(8,128)(2,1)S(1)}, u32[]{:S(2)}, u32[]{:S(2)}) %all-to-all-start) | async-done | bytes 524320 | tf_op jit(solution)/shard_map/all_to_all | solution.py:201
  122.6 10.6 %all_gather.27.rows_ref = bf16[128,2048]{1,0:T(8,128)(2,1)} all-gather(bf16[32,2048]{1,0:T(8,128)(2,1)S(1)} %add_convert_fusion.1), channel_id=1, replica_groups=mesh['z'=16,'y'=4,'x'=4,'c'=2] {'x'}, dimensions={0}, use_global_device_ids=true | all-gather | bytes 655360 | tf_op jit(solution)/shard_map/all_gather | solution.py:204
  133.3 3.9 %shard_map.75 = (bf16[128,512]{1,0:T(8,128)(2,1)}, bf16[32,512]{1,0:T(8,128)(2,1)}) custom-call(bf16[128,2048]{1,0:T(8,128)(2,1)} %all_gather.27.rows_ref, f32[1,2048]{1,0:T(1,128)} %get-tuple-element.120.gain_ref, bf16[16,2,128,512]{3,2,1,0:T(8,128)(2,1)} %bitcast.126), custom_call_target="tpu_custom_call" | custom-call | tf_op jit(solution)/shard_map/pallas_call | solution.py:44
  137.2 9.4 %collective-permute-start.6 = (bf16[32,512]{1,0:T(8,128)(2,1)}, bf16[32,512]{1,0:T(8,128)(2,1)S(1)}, u32[]{:S(2)}, u32[]{:S(2)}) collective-permute-start(bf16[32,512]{1,0:T(8,128)(2,1)} %get-tuple-element.34), channel_id=1, source_target_pairs={{0,1},{1,8},{8,9},{9,16},{16,17},{17,24},{24,25},{25,32},{32,33},{... | collective-permute-start | bytes 98312 | tf_op jit(solution)/shard_map/ppermute | solution.py:26
  146.6 1.3 collective-permute-done.6
  150.0 7.0 %all_gather.30 = f32[4,1,256]{2,1,0:T(1,128)S(1)} all-gather(f32[1,1,256]{2,1,0:T(1,128)S(1)} %bitcast.209), channel_id=1, replica_groups=mesh['z'=16,'y'=4,'x'=4,'c'=2] {'x'}, dimensions={0}, use_global_device_ids=true | all-gather | bytes 5120 | tf_op jit(solution)/shard_map/all_gather | solution.py:189
  157.0 6.2 %all-gather.8.cloned.1.call-done = bf16[16,8,32,256]{3,2,1,0:T(8,128)(2,1)} async-done(((bf16[16,1,32,256]{3,2,1,0:T(8,128)(2,1)}), bf16[16,8,32,256]{3,2,1,0:T(8,128)(2,1)}) %all-gather.8.cloned.1.call-update) | async-done | bytes 2097168 | tf_op jit(solution)/shard_map/all_gather | solution.py:157
  163.2 1.7 fusion.59
  165.7 12.8 %all_to_all.10 = bf16[4,32,2048]{2,1,0:T(8,128)(2,1)S(1)} all-to-all(bf16[4,32,2048]{2,1,0:T(8,128)(2,1)S(1)} %bitcast.132), channel_id=1, replica_groups=mesh['z'=16,'y'=4,'x'=4,'c'=2] {'x'}, dimensions={0} | all-to-all | bytes 1048576 | tf_op jit(solution)/shard_map/all_to_all | solution.py:201
  179.5 10.6 %all_gather.31 = bf16[128,2048]{1,0:T(8,128)(2,1)S(1)} all-gather(bf16[32,2048]{1,0:T(8,128)(2,1)S(1)} %add_convert_fusion), channel_id=1, replica_groups=mesh['z'=16,'y'=4,'x'=4,'c'=2] {'x'}, dimensions={0}, use_global_device_ids=true | all-gather | bytes 655360 | tf_op jit(solution)/shard_map/all_gather | solution.py:204
  190.1 6.1 %collective-permute-start.7 = (bf16[128,2048]{1,0:T(8,128)(2,1)S(1)}, bf16[128,2048]{1,0:T(8,128)(2,1)S(1)}, u32[]{:S(2)}, u32[]{:S(2)}) collective-permute-start(bf16[128,2048]{1,0:T(8,128)(2,1)S(1)} %all_gather.31), channel_id=1, source_target_pairs={{0,1},{1,0},{2,3},{3,2},{4,5},{5,4},{6,7},{7,6},{8,9},{9,8},{10,11... | collective-permute-start | bytes 1572872 | tf_op jit(solution)/shard_map/ppermute | solution.py:21
  196.2 1.5 collective-permute-done.7
  (72 shorter events, 17.7 us)
Async XLA Ops:
  6.5 61.6 %copy-start.1 = (bf16[256,2048]{1,0:T(8,128)(2,1)S(1)}, bf16[256,2048]{1,0:T(8,128)(2,1)}, u32[]{:S(2)}) copy-start(bf16[256,2048]{1,0:T(8,128)(2,1)} %param.7) | copy-start | bytes 3145732
  6.5 69.7 %all-gather.4.cloned.1.call-start = ((), (), s32[]{:S(2)}) async-start(), calls=%async_computation.2 | async-start | bytes 1114112 | tf_op jit(solution)/shard_map/all_gather | solution.py:126
  8.8 124.5 %all-gather.6.cloned.1.call-start = ((), (), s32[]{:S(2)}) async-start(), calls=%async_computation.3 | async-start | bytes 4718592 | tf_op jit(solution)/shard_map/all_gather | solution.py:157
  44.3 25.6 %copy-start.4 = (bf16[512,768]{1,0:T(8,128)(2,1)}, bf16[512,768]{1,0:T(8,128)(2,1)S(1)}, u32[]{:S(2)}) copy-start(bf16[512,768]{1,0:T(8,128)(2,1)S(1)} %all_gather.24.refs_0_) | copy-start | bytes 2359300
  44.3 15.6 %collective-permute-start = (bf16[512,768]{1,0:T(8,128)(2,1)S(1)}, bf16[512,768]{1,0:T(8,128)(2,1)S(1)}, u32[]{:S(2)}, u32[]{:S(2)}) collective-permute-start(bf16[512,768]{1,0:T(8,128)(2,1)S(1)} %all_gather.24.refs_0_), channel_id=1, source_target_pairs={{0,8},{8,16},{16,24},{24,0},{1,9},{9,17},{17,25},{25,1},{2,10},{10... | collective-permute-start | bytes 2359304 | tf_op jit(solution)/shard_map/ppermute | solution.py:21
  47.3 13.6 %collective-permute-start.1 = (bf16[512,768]{1,0:T(8,128)(2,1)S(1)}, bf16[512,768]{1,0:T(8,128)(2,1)S(1)}, u32[]{:S(2)}, u32[]{:S(2)}) collective-permute-start(bf16[512,768]{1,0:T(8,128)(2,1)S(1)} %all_gather.24.refs_0_), channel_id=1, source_target_pairs={{0,24},{8,0},{16,8},{24,16},{1,25},{9,1},{17,9},{25,17},{2,26},{10... | collective-permute-start | bytes 2359304 | tf_op jit(solution)/shard_map/ppermute | solution.py:21
  52.3 7.6 %collective-permute-start.2 = (bf16[32,2048]{1,0:T(8,128)(2,1)}, bf16[32,2048]{1,0:T(8,128)(2,1)S(1)}, u32[]{:S(2)}, u32[]{:S(2)}) collective-permute-start(bf16[32,2048]{1,0:T(8,128)(2,1)} %slice.546), channel_id=1, source_target_pairs={{0,8},{8,16},{16,24},{24,32},{32,40},{40,48},{48,56},{56,64},{64,7... | collective-permute-start | bytes 393224 | tf_op jit(solution)/shard_map/ppermute | solution.py:26
  59.9 10.0 %copy-start.5 = (bf16[512,768]{1,0:T(8,128)(2,1)}, bf16[512,768]{1,0:T(8,128)(2,1)S(1)}, u32[]{:S(2)}) copy-start(bf16[512,768]{1,0:T(8,128)(2,1)S(1)} %collective-permute-done.refs_1_) | copy-start | bytes 2359300
  60.9 8.9 %copy-start.6 = (bf16[512,768]{1,0:T(8,128)(2,1)}, bf16[512,768]{1,0:T(8,128)(2,1)S(1)}, u32[]{:S(2)}) copy-start(bf16[512,768]{1,0:T(8,128)(2,1)S(1)} %collective-permute-done.1.refs_2_) | copy-start | bytes 2359300
  61.0 10.7 %collective-permute-start.3 = (bf16[256,768]{1,0:T(8,128)(2,1)S(1)}, bf16[256,768]{1,0:T(8,128)(2,1)S(1)}, u32[]{:S(2)}, u32[]{:S(2)}) collective-permute-start(bf16[256,768]{1,0:T(8,128)(2,1)S(1)} %slice.548), channel_id=1, source_target_pairs={{0,8},{8,16},{16,24},{24,0},{1,9},{9,17},{17,25},{25,1},{2,10},{10... | collective-permute-start | bytes 1179656 | tf_op jit(solution)/shard_map/ppermute | solution.py:21
  64.1 8.8 %collective-permute-start.4 = (bf16[256,768]{1,0:T(8,128)(2,1)S(1)}, bf16[256,768]{1,0:T(8,128)(2,1)}, u32[]{:S(2)}, u32[]{:S(2)}) collective-permute-start(bf16[256,768]{1,0:T(8,128)(2,1)S(1)} %slice.549), channel_id=1, source_target_pairs={{0,24},{8,0},{16,8},{24,16},{1,25},{9,1},{17,9},{25,17},{2,26},{10... | collective-permute-start | bytes 1179656 | tf_op jit(solution)/shard_map/ppermute | solution.py:21
  71.7 0.8 copy-start.7
  81.1 18.8 %copy-start.3 = (f32[2,31,256]{2,0,1:T(2,128)S(1)}, f32[2,31,256]{2,0,1:T(2,128)}, u32[]{:S(2)}) copy-start(f32[2,31,256]{2,0,1:T(2,128)} %param.11) | copy-start | bytes 190468
  81.1 18.8 %copy-start.9 = (f32[2,256]{1,0:T(2,128)S(1)}, f32[2,256]{1,0:T(2,128)}, u32[]{:S(2)}) copy-start(f32[2,256]{1,0:T(2,128)} %param.12) | copy-start | bytes 6148
  81.1 82.1 %all-gather.8.cloned.1.call-start = ((), (), s32[]{:S(2)}) async-start(), calls=%async_computation.4 | async-start | bytes 2359296 | tf_op jit(solution)/shard_map/all_gather | solution.py:157
  81.2 14.6 %collective-permute-start.5 = (bf16[2400,256]{1,0:T(8,128)(2,1)}, bf16[2400,256]{1,0:T(8,128)(2,1)S(1)}, u32[]{:S(2)}, u32[]{:S(2)}) collective-permute-start(bf16[2400,256]{1,0:T(8,128)(2,1)} %get-tuple-element.30), channel_id=1, source_target_pairs={{0,1},{1,0},{2,3},{3,2},{4,5},{5,4},{6,7},{7,6},{8,9},{9,8},{10,11... | collective-permute-start | bytes 3686408 | tf_op jit(solution)/shard_map/ppermute | solution.py:21
  95.8 1.0 copy-start.2
  98.9 1.1 copy-start
  101.8 7.7 %slice-start = ((bf16[2400,256]{1,0:T(8,128)(2,1)}), bf16[2048,256]{1,0:T(8,128)(2,1)S(1)}, s32[]{:S(2)}) async-start(bf16[2400,256]{1,0:T(8,128)(2,1)} %copy-done.2), calls=%async_computation.5 | async-start | bytes 2097152 | tf_op jit(solution)/shard_map/slice | solution.py:161
  109.5 1.0 copy-start.8
  112.1 10.4 %all-to-all-start = ((bf16[4,32,2048]{2,1,0:T(8,128)(2,1)}), bf16[4,32,2048]{2,1,0:T(8,128)(2,1)S(1)}, u32[]{:S(2)}, u32[]{:S(2)}) async-start(bf16[4,32,2048]{2,1,0:T(8,128)(2,1)} %bitcast.131), calls=%async_computation | async-start | bytes 1048576 | tf_op jit(solution)/shard_map/all_to_all | solution.py:201
  137.2 10.7 %collective-permute-start.6 = (bf16[32,512]{1,0:T(8,128)(2,1)}, bf16[32,512]{1,0:T(8,128)(2,1)S(1)}, u32[]{:S(2)}, u32[]{:S(2)}) collective-permute-start(bf16[32,512]{1,0:T(8,128)(2,1)} %get-tuple-element.34), channel_id=1, source_target_pairs={{0,1},{1,8},{8,9},{9,16},{16,17},{17,24},{24,25},{25,32},{32,33},{... | collective-permute-start | bytes 98312 | tf_op jit(solution)/shard_map/ppermute | solution.py:26
  190.1 7.6 %collective-permute-start.7 = (bf16[128,2048]{1,0:T(8,128)(2,1)S(1)}, bf16[128,2048]{1,0:T(8,128)(2,1)S(1)}, u32[]{:S(2)}, u32[]{:S(2)}) collective-permute-start(bf16[128,2048]{1,0:T(8,128)(2,1)S(1)} %all_gather.31), channel_id=1, source_target_pairs={{0,1},{1,0},{2,3},{3,2},{4,5},{5,4},{6,7},{7,6},{8,9},{9,8},{10,11... | collective-permute-start | bytes 1572872 | tf_op jit(solution)/shard_map/ppermute | solution.py:21
Sparse Core Ops, SparseCore 0:
  9.4 66.7 all-gather.3
  81.2 46.7 all-gather.5
  130.1 32.9 all-gather.7

commit v4 on v3

--- a/solution.py
+++ b/solution.py
@@ -39,12 +39,13 @@
     return jnp.stack(parts)
 
 
-def call(kernel, out, *args, scratch=(), scalars=0):
+def call(kernel, out, *args, scratch=(), scalars=0, last=None):
     smem, vmem = pl.BlockSpec(memory_space=pltpu.SMEM), pl.BlockSpec(memory_space=pltpu.VMEM)
     return pl.pallas_call(
         kernel,
         out_shape=[jax.ShapeDtypeStruct(s, d) for s, d in out],
-        in_specs=[smem] * scalars + [vmem] * (len(args) - scalars),
+        grid=(1,) if last else (),
+        in_specs=[smem] * scalars + [vmem] * (len(args) - scalars - 1) + [last or vmem],
         out_specs=[vmem] * len(out),
         scratch_shapes=[pltpu.VMEM(s, d) for s, d in scratch],
     )(*args)
@@ -65,9 +66,8 @@
 
 
 def first_kernel(cols, deep, ys, at_ref, rows_ref, small_ref, *refs):
-    *blocks, pair_ref, keep_ref, send_ref, later_ref, last_ref, weights = refs
-    later_ref[...] = pair_ref[:, : 2 * cols]
-    last_ref[...] = pair_ref[:, 2 * cols : 3 * cols]
+    *blocks, pair_ref, keep_ref, send_ref, later_ref, weights = refs
+    later_ref[...] = pair_ref[:, : 3 * cols]
     here, c = at_ref[0], at_ref[1]
     whole = blocks[0].shape[0]
     for ref, offset, start in zip(blocks, (0, ys - 1, 1, 2, 2), (0, 0, 0, 0, whole // 2)):
@@ -137,13 +137,12 @@
     table = jnp.concatenate([conv_taps, channel_gain[:, None]], axis=1)
     small = in_parts(table).reshape(-1, cols)
 
-    keep, send, later, last = call(
+    keep, send, later = call(
         functools.partial(first_kernel, cols, deep, lax.axis_size("y")),
         [
             ((half + HALO, cols), BF16),
             ((width + half + HALO + small.shape[0], cols), BF16),
-            ((later.shape[0], 2 * cols), BF16),
-            ((later.shape[0], cols), BF16),
+            ((later.shape[0], 3 * cols), BF16),
         ],
         jnp.stack([y, c]),
         rows,
@@ -153,10 +152,9 @@
         scratch=[((width, 2 * cols), BF16)],
         scalars=1,
     )
-    later, last = (
-        lax.all_gather(p.reshape(-1, 1, deep, p.shape[1]), ("c", "y"), axis=1, tiled=True)
-        for p in (later, last)
-    )
+    later = lax.all_gather(
+        later.reshape(-1, 1, deep, later.shape[1]), ("c", "y"), axis=1, tiled=True
+    ).reshape(lax.axis_size("z"), 2, -1, later.shape[1])
     got = shifted(send, "c", 1)
     out_t = jnp.concatenate([send[:width], got[:width]], axis=1)
     padded, other_table = call(
@@ -177,9 +175,13 @@
                 [((half, 2 * cols), BF16), ((HALO, 2 * cols), BF16)],
                 stream,
                 norm_gain[1:],
-                later.reshape(lax.axis_size("z"), 2, -1, 2 * cols),
+                later,
                 scratch=[(stream.shape, BF16), ((width, 2 * cols), BF16)],
+                last=pl.BlockSpec((*later.shape[:3], 2 * cols), lambda _: (0, 0, 0, 0)),
             )
+            columns, tail = lax.optimization_barrier((later, tail))
+            columns = columns[..., 2 * cols :]
+            out_t = jnp.concatenate([columns[:, k].reshape(width, cols) for k in range(2)], axis=1)
             padded = jnp.concatenate([passed_on(tail, (*SP, "c")), gated], axis=0).astype(F32)
         filtered = jnp.zeros((half, 2 * cols), F32)
         for tap in range(kernel):
@@ -187,10 +189,6 @@
             filtered = filtered + tables[layer][tap] * padded[at : at + half]
         sums = jnp.stack([jnp.sum(filtered, axis=1), jnp.sum(filtered * filtered, axis=1)])
         sums = jnp.sum(lax.all_gather(sums.reshape(1, -1), "x", axis=0), axis=0).reshape(2, half, 1)
-        if layer:
-            last, sums = lax.optimization_barrier((last, sums))
-            last = last.reshape(lax.axis_size("z"), 2, -1, cols)
-            out_t = jnp.concatenate([last[:, k].reshape(width, cols) for k in range(2)], axis=1)
         mean = sums[0] / width
         variance = sums[1] / width - mean * mean
         gain = tables[layer][kernel]

time: 206 us -> 198 us (0.961)
  waiting for transfers between devices: 23.9 us -> 18.8 us
  starting transfers between devices: 46.4 us -> 43.1 us
    all_gather x2 -> x1, waiting for transfers between devices: 6.18 us -> 2.37 us  [body(): lax.all_gather(later.reshape(-1, 1, deep, later.shape[1]), ('c', 'y'), ax...]
    ppermute x2, starting transfers between devices: 11.2 us -> 7.74 us  [passed_on(): return lax.ppermute(value, axes, [(i, i + 1) for i in range(count - 1)])]
    unnamed x21 -> x23, local copies, waits for them, and re-layouts: 4.19 us -> 4.18 us
  transfers between devices with their start and end apart: 12 -> 11, of which waited for: 10 -> 8; matrix products, arithmetic and copies ran while one was open for 8% -> 9% of each run, Pallas kernels for 3% -> 1%
where the time goes in v4:
time: 198 us; the launch traced here: 196 us
  blocking collectives  83.1 us (42%)
  starting transfers between devices  43.1 us (22%)
  waiting for transfers between devices  18.8 us (9%)
  between operations  13.7 us (7%)
  local copies, waits for them, and re-layouts  13.5 us (7%)
  Pallas kernels  10.8 us (5%)
  other arithmetic  10.2 us (5%)
  matrix products  2.42 us (1%)
    all_gather x1, blocking collectives, body(): block = lax.all_gather(first, 'z', axis=0, tiled=True)  35.4 us
    ppermute x6, starting transfers between devices, shifted(): lax.ppermute(value, axis, [(i, (i + steps) % count) for i in range(count)])  31.8 us
    all_gather x2, blocking collectives, body(): stream = lax.all_gather(own, 'x', axis=0, tiled=True)  22.1 us
    all_gather x2, blocking collectives, body(): lax.all_gather(sums.reshape(1, -1), 'x', axis=0)  14 us
    all_to_all x1, blocking collectives, body(): lax.all_to_all(branch.reshape(xs, share, width), 'x', 0, 0, tiled=True)  11.6 us
    pallas_call x3, Pallas kernels, call(): pl.pallas_call(kernel, out_shape=[jax.ShapeDtypeStruct(s, d) for s, d in...  10.8 us
    ppermute x2, starting transfers between devices, passed_on(): return lax.ppermute(value, axes, [(i, i + 1) for i in range(count - 1)])  7.74 us
    all_to_all x1, waiting for transfers between devices, body(): lax.all_to_all(branch.reshape(xs, share, width), 'x', 0, 0, tiled=True)  6.76 us
  transfers between devices with their start and end apart: 11, of which 8 were waited for; matrix products, arithmetic and copies ran while one was open for 9% of the time, Pallas kernels for 1%

profile of v4, /device:TPU:1, one launch (start us, length us, event | category | flops | bytes accessed | tf_op | source)
XLA Modules:
  0.0 195.7 jit_solution(11955718380188062974)
XLA Ops:
  8.9 35.4 %all_gather.21.refs_0_ = bf16[512,768]{1,0:T(8,128)(2,1)S(1)} all-gather(bf16[32,768]{1,0:T(8,128)(2,1)S(1)} %pad_maximum_fusion.8), channel_id=1, replica_groups=mesh['z'=16,'y'=4,'x'=4,'c'=2] {'z'}, dimensions={0}, use_global_device_ids=true | all-gather | bytes 835584 | tf_op jit(solution)/shard_map/all_gather | solution.py:127
  44.2 3.0 %collective-permute-start = (bf16[512,768]{1,0:T(8,128)(2,1)S(1)}, bf16[512,768]{1,0:T(8,128)(2,1)S(1)}, u32[]{:S(2)}, u32[]{:S(2)}) collective-permute-start(bf16[512,768]{1,0:T(8,128)(2,1)S(1)} %all_gather.21.refs_0_), channel_id=1, source_target_pairs={{0,8},{8,16},{16,24},{24,0},{1,9},{9,17},{17,25},{25,1},{2,10},{10... | collective-permute-start | bytes 2359304 | tf_op jit(solution)/shard_map/ppermute | solution.py:21
  47.3 3.4 %collective-permute-start.1 = (bf16[512,768]{1,0:T(8,128)(2,1)S(1)}, bf16[512,768]{1,0:T(8,128)(2,1)S(1)}, u32[]{:S(2)}, u32[]{:S(2)}) collective-permute-start(bf16[512,768]{1,0:T(8,128)(2,1)S(1)} %all_gather.21.refs_0_), channel_id=1, source_target_pairs={{0,24},{8,0},{16,8},{24,16},{1,25},{9,1},{17,9},{25,17},{2,26},{10... | collective-permute-start | bytes 2359304 | tf_op jit(solution)/shard_map/ppermute | solution.py:21
  50.7 1.6 slice.551
  52.3 1.8 collective-permute-start.2
  54.2 1.5 copy.21
  57.2 1.4 fusion.63
  60.9 3.2 %collective-permute-start.3 = (bf16[256,768]{1,0:T(8,128)(2,1)S(1)}, bf16[256,768]{1,0:T(8,128)(2,1)S(1)}, u32[]{:S(2)}, u32[]{:S(2)}) collective-permute-start(bf16[256,768]{1,0:T(8,128)(2,1)S(1)} %slice.553), channel_id=1, source_target_pairs={{0,8},{8,16},{16,24},{24,0},{1,9},{9,17},{17,25},{25,1},{2,10},{10... | collective-permute-start | bytes 1179656 | tf_op jit(solution)/shard_map/ppermute | solution.py:21
  64.1 3.8 %collective-permute-start.4 = (bf16[256,768]{1,0:T(8,128)(2,1)S(1)}, bf16[256,768]{1,0:T(8,128)(2,1)}, u32[]{:S(2)}, u32[]{:S(2)}) collective-permute-start(bf16[256,768]{1,0:T(8,128)(2,1)S(1)} %slice.554), channel_id=1, source_target_pairs={{0,24},{8,0},{16,8},{24,16},{1,25},{9,1},{17,9},{25,17},{2,26},{10... | collective-permute-start | bytes 1179656 | tf_op jit(solution)/shard_map/ppermute | solution.py:21
  68.2 1.4 fusion.2.rows_ref
  69.6 2.1 %collective-permute-done.3.refs_3_ = bf16[256,768]{1,0:T(8,128)(2,1)S(1)} collective-permute-done((bf16[256,768]{1,0:T(8,128)(2,1)S(1)}, bf16[256,768]{1,0:T(8,128)(2,1)S(1)}, u32[]{:S(2)}, u32[]{:S(2)}) %collective-permute-start.3) | collective-permute-done | bytes 393248 | tf_op jit(solution)/shard_map/ppermute | solution.py:21
  72.9 3.2 %all-gather.3.cloned.1.call-done.refs_5_ = bf16[512,1024]{1,0:T(8,128)(2,1)} async-done(((bf16[32,1024]{1,0:T(8,128)(2,1)}), bf16[512,1024]{1,0:T(8,128)(2,1)}) %all-gather.3.cloned.1.call-update) | async-done | bytes 1048592 | tf_op jit(solution)/shard_map/all_gather | solution.py:126
  76.1 4.8 %shard_map.73 = (bf16[160,256]{1,0:T(8,128)(2,1)}, bf16[2400,256]{1,0:T(8,128)(2,1)}, bf16[512,768]{1,0:T(8,128)(2,1)}) custom-call(s32[2]{0:T(128)} %pad_add_fusion.at_ref, bf16[288,2048]{1,0:T(8,128)(2,1)} %fusion.2.rows_ref, bf16[192,256]{1,0:T(8,128)(2,1)} %bitcast.129, bf16[512,768]{1,0:T(8,128)(2,1)} %copy-done.4, bf16[512,768]{1,0:T(8,128)(2,1)} %copy-done.5, ...), custom_call_target="tpu_custom_call" | custom-call | tf_op jit(solution)/shard_map/pallas_call | solution.py:44
  81.0 12.1 %collective-permute-start.5 = (bf16[2400,256]{1,0:T(8,128)(2,1)}, bf16[2400,256]{1,0:T(8,128)(2,1)S(1)}, u32[]{:S(2)}, u32[]{:S(2)}) collective-permute-start(bf16[2400,256]{1,0:T(8,128)(2,1)} %get-tuple-element.29), channel_id=1, source_target_pairs={{0,1},{1,0},{2,3},{3,2},{4,5},{5,4},{6,7},{7,6},{8,9},{9,8},{10,11... | collective-permute-start | bytes 3686408 | tf_op jit(solution)/shard_map/ppermute | solution.py:21
  93.1 1.3 slice.620
  94.4 1.4 collective-permute-done.5.got_ref
  96.9 2.1 %shard_map.74 = (f32[160,512]{1,0:T(8,128)}, f32[64,256]{1,0:T(8,128)}) custom-call(bf16[160,256]{1,0:T(8,128)(2,1)} %get-tuple-element.28.keep_ref, bf16[2400,256]{1,0:T(8,128)(2,1)} %copy-done.2), custom_call_target="tpu_custom_call" | custom-call | tf_op jit(solution)/shard_map/pallas_call | solution.py:44
  100.1 1.8 fusion.58
  101.9 7.7 %all_gather.23 = f32[4,1,256]{2,1,0:T(1,128)S(1)} all-gather(f32[1,1,256]{2,1,0:T(1,128)S(1)} %bitcast.203), channel_id=1, replica_groups=mesh['z'=16,'y'=4,'x'=4,'c'=2] {'x'}, dimensions={0}, use_global_device_ids=true | all-gather | bytes 5120 | tf_op jit(solution)/shard_map/all_gather | solution.py:191
  110.6 1.6 convolution_convert_fusion.1
  112.2 3.5 %all-to-all-start = ((bf16[4,32,2048]{2,1,0:T(8,128)(2,1)}), bf16[4,32,2048]{2,1,0:T(8,128)(2,1)S(1)}, u32[]{:S(2)}, u32[]{:S(2)}) async-start(bf16[4,32,2048]{2,1,0:T(8,128)(2,1)} %bitcast.127), calls=%async_computation | async-start | bytes 1048576 | tf_op jit(solution)/shard_map/all_to_all | solution.py:199
  115.9 6.8 %all-to-all-done = bf16[4,32,2048]{2,1,0:T(8,128)(2,1)S(1)} async-done(((bf16[4,32,2048]{2,1,0:T(8,128)(2,1)}), bf16[4,32,2048]{2,1,0:T(8,128)(2,1)S(1)}, u32[]{:S(2)}, u32[]{:S(2)}) %all-to-all-start) | async-done | bytes 524320 | tf_op jit(solution)/shard_map/all_to_all | solution.py:199
  122.8 11.8 %all_gather.24.rows_ref = bf16[128,2048]{1,0:T(8,128)(2,1)} all-gather(bf16[32,2048]{1,0:T(8,128)(2,1)S(1)} %add_convert_fusion.1), channel_id=1, replica_groups=mesh['z'=16,'y'=4,'x'=4,'c'=2] {'x'}, dimensions={0}, use_global_device_ids=true | all-gather | bytes 655360 | tf_op jit(solution)/shard_map/all_gather | solution.py:202
  134.6 2.4 %all-gather.5.cloned.1.call-done = bf16[16,8,32,768]{3,2,1,0:T(8,128)(2,1)} async-done(((bf16[16,1,32,768]{3,2,1,0:T(8,128)(2,1)}), bf16[16,8,32,768]{3,2,1,0:T(8,128)(2,1)}) %all-gather.5.cloned.1.call-update) | async-done | bytes 6291472 | tf_op jit(solution)/shard_map/all_gather | solution.py:155
  137.0 3.9 %shard_map.75 = (bf16[128,512]{1,0:T(8,128)(2,1)}, bf16[32,512]{1,0:T(8,128)(2,1)}) custom-call(bf16[128,2048]{1,0:T(8,128)(2,1)} %all_gather.24.rows_ref, f32[1,2048]{1,0:T(1,128)} %get-tuple-element.118.gain_ref, bf16[16,2,128,768]{3,2,1,0:T(8,128)(2,1)} %bitcast.122), custom_call_target="tpu_custom_call" | custom-call | tf_op jit(solution)/shard_map/pallas_call | solution.py:44
  140.9 5.9 %collective-permute-start.6 = (bf16[32,512]{1,0:T(8,128)(2,1)}, bf16[32,512]{1,0:T(8,128)(2,1)S(1)}, u32[]{:S(2)}, u32[]{:S(2)}) collective-permute-start(bf16[32,512]{1,0:T(8,128)(2,1)} %get-tuple-element.34), channel_id=1, source_target_pairs={{0,1},{1,8},{8,9},{9,16},{16,17},{17,24},{24,25},{25,32},{32,33},{... | collective-permute-start | bytes 98312 | tf_op jit(solution)/shard_map/ppermute | solution.py:26
  146.8 1.7 fusion.60
  149.7 6.4 %all_gather.26 = f32[4,1,256]{2,1,0:T(1,128)S(1)} all-gather(f32[1,1,256]{2,1,0:T(1,128)S(1)} %bitcast.204), channel_id=1, replica_groups=mesh['z'=16,'y'=4,'x'=4,'c'=2] {'x'}, dimensions={0}, use_global_device_ids=true | all-gather | bytes 5120 | tf_op jit(solution)/shard_map/all_gather | solution.py:191
  157.0 11.6 %all_to_all.10 = bf16[4,32,2048]{2,1,0:T(8,128)(2,1)S(1)} all-to-all(bf16[4,32,2048]{2,1,0:T(8,128)(2,1)S(1)} %bitcast.128), channel_id=1, replica_groups=mesh['z'=16,'y'=4,'x'=4,'c'=2] {'x'}, dimensions={0} | all-to-all | bytes 1048576 | tf_op jit(solution)/shard_map/all_to_all | solution.py:199
  169.6 10.3 %all_gather.27 = bf16[128,2048]{1,0:T(8,128)(2,1)S(1)} all-gather(bf16[32,2048]{1,0:T(8,128)(2,1)S(1)} %add_convert_fusion), channel_id=1, replica_groups=mesh['z'=16,'y'=4,'x'=4,'c'=2] {'x'}, dimensions={0}, use_global_device_ids=true | all-gather | bytes 655360 | tf_op jit(solution)/shard_map/all_gather | solution.py:202
  179.8 6.3 %collective-permute-start.7 = (bf16[128,2048]{1,0:T(8,128)(2,1)S(1)}, bf16[128,2048]{1,0:T(8,128)(2,1)S(1)}, u32[]{:S(2)}, u32[]{:S(2)}) collective-permute-start(bf16[128,2048]{1,0:T(8,128)(2,1)S(1)} %all_gather.27), channel_id=1, source_target_pairs={{0,1},{1,0},{2,3},{3,2},{4,5},{5,4},{6,7},{7,6},{8,9},{9,8},{10,11... | collective-permute-start | bytes 1572872 | tf_op jit(solution)/shard_map/ppermute | solution.py:21
  186.1 1.5 collective-permute-done.7
  (71 shorter events, 15.4 us)
Async XLA Ops:
  6.5 61.3 %copy-start.1 = (bf16[256,2048]{1,0:T(8,128)(2,1)S(1)}, bf16[256,2048]{1,0:T(8,128)(2,1)}, u32[]{:S(2)}) copy-start(bf16[256,2048]{1,0:T(8,128)(2,1)} %param.7) | copy-start | bytes 3145732
  6.5 69.6 %all-gather.3.cloned.1.call-start = ((), (), s32[]{:S(2)}) async-start(), calls=%async_computation.2 | async-start | bytes 1114112 | tf_op jit(solution)/shard_map/all_gather | solution.py:126
  8.8 128.2 %all-gather.5.cloned.1.call-start = ((), (), s32[]{:S(2)}) async-start(), calls=%async_computation.3 | async-start | bytes 7077888 | tf_op jit(solution)/shard_map/all_gather | solution.py:155
  44.2 25.3 %copy-start.4 = (bf16[512,768]{1,0:T(8,128)(2,1)}, bf16[512,768]{1,0:T(8,128)(2,1)S(1)}, u32[]{:S(2)}) copy-start(bf16[512,768]{1,0:T(8,128)(2,1)S(1)} %all_gather.21.refs_0_) | copy-start | bytes 2359300
  44.2 15.6 %collective-permute-start = (bf16[512,768]{1,0:T(8,128)(2,1)S(1)}, bf16[512,768]{1,0:T(8,128)(2,1)S(1)}, u32[]{:S(2)}, u32[]{:S(2)}) collective-permute-start(bf16[512,768]{1,0:T(8,128)(2,1)S(1)} %all_gather.21.refs_0_), channel_id=1, source_target_pairs={{0,8},{8,16},{16,24},{24,0},{1,9},{9,17},{17,25},{25,1},{2,10},{10... | collective-permute-start | bytes 2359304 | tf_op jit(solution)/shard_map/ppermute | solution.py:21
  47.3 13.5 %collective-permute-start.1 = (bf16[512,768]{1,0:T(8,128)(2,1)S(1)}, bf16[512,768]{1,0:T(8,128)(2,1)S(1)}, u32[]{:S(2)}, u32[]{:S(2)}) collective-permute-start(bf16[512,768]{1,0:T(8,128)(2,1)S(1)} %all_gather.21.refs_0_), channel_id=1, source_target_pairs={{0,24},{8,0},{16,8},{24,16},{1,25},{9,1},{17,9},{25,17},{2,26},{10... | collective-permute-start | bytes 2359304 | tf_op jit(solution)/shard_map/ppermute | solution.py:21
  52.3 7.6 %collective-permute-start.2 = (bf16[32,2048]{1,0:T(8,128)(2,1)}, bf16[32,2048]{1,0:T(8,128)(2,1)S(1)}, u32[]{:S(2)}, u32[]{:S(2)}) collective-permute-start(bf16[32,2048]{1,0:T(8,128)(2,1)} %slice.551), channel_id=1, source_target_pairs={{0,8},{8,16},{16,24},{24,32},{32,40},{40,48},{48,56},{56,64},{64,7... | collective-permute-start | bytes 393224 | tf_op jit(solution)/shard_map/ppermute | solution.py:26
  59.9 9.7 %copy-start.5 = (bf16[512,768]{1,0:T(8,128)(2,1)}, bf16[512,768]{1,0:T(8,128)(2,1)S(1)}, u32[]{:S(2)}) copy-start(bf16[512,768]{1,0:T(8,128)(2,1)S(1)} %collective-permute-done.refs_1_) | copy-start | bytes 2359300
  60.8 8.8 %copy-start.6 = (bf16[512,768]{1,0:T(8,128)(2,1)}, bf16[512,768]{1,0:T(8,128)(2,1)S(1)}, u32[]{:S(2)}) copy-start(bf16[512,768]{1,0:T(8,128)(2,1)S(1)} %collective-permute-done.1.refs_2_) | copy-start | bytes 2359300
  60.9 10.8 %collective-permute-start.3 = (bf16[256,768]{1,0:T(8,128)(2,1)S(1)}, bf16[256,768]{1,0:T(8,128)(2,1)S(1)}, u32[]{:S(2)}, u32[]{:S(2)}) collective-permute-start(bf16[256,768]{1,0:T(8,128)(2,1)S(1)} %slice.553), channel_id=1, source_target_pairs={{0,8},{8,16},{16,24},{24,0},{1,9},{9,17},{17,25},{25,1},{2,10},{10... | collective-permute-start | bytes 1179656 | tf_op jit(solution)/shard_map/ppermute | solution.py:21
  64.1 8.8 %collective-permute-start.4 = (bf16[256,768]{1,0:T(8,128)(2,1)S(1)}, bf16[256,768]{1,0:T(8,128)(2,1)}, u32[]{:S(2)}, u32[]{:S(2)}) collective-permute-start(bf16[256,768]{1,0:T(8,128)(2,1)S(1)} %slice.554), channel_id=1, source_target_pairs={{0,24},{8,0},{16,8},{24,16},{1,25},{9,1},{17,9},{25,17},{2,26},{10... | collective-permute-start | bytes 1179656 | tf_op jit(solution)/shard_map/ppermute | solution.py:21
  71.7 0.8 copy-start.7
  81.0 19.0 %copy-start.3 = (f32[2,31,256]{2,0,1:T(2,128)S(1)}, f32[2,31,256]{2,0,1:T(2,128)}, u32[]{:S(2)}) copy-start(f32[2,31,256]{2,0,1:T(2,128)} %param.11) | copy-start | bytes 190468
  81.0 19.0 %copy-start.9 = (f32[2,256]{1,0:T(2,128)S(1)}, f32[2,256]{1,0:T(2,128)}, u32[]{:S(2)}) copy-start(f32[2,256]{1,0:T(2,128)} %param.12) | copy-start | bytes 6148
  81.0 14.9 %collective-permute-start.5 = (bf16[2400,256]{1,0:T(8,128)(2,1)}, bf16[2400,256]{1,0:T(8,128)(2,1)S(1)}, u32[]{:S(2)}, u32[]{:S(2)}) collective-permute-start(bf16[2400,256]{1,0:T(8,128)(2,1)} %get-tuple-element.29), channel_id=1, source_target_pairs={{0,1},{1,0},{2,3},{3,2},{4,5},{5,4},{6,7},{7,6},{8,9},{9,8},{10,11... | collective-permute-start | bytes 3686408 | tf_op jit(solution)/shard_map/ppermute | solution.py:21
  95.9 1.0 copy-start.2
  99.0 1.1 copy-start
  101.9 7.7 %slice-start = ((bf16[2400,256]{1,0:T(8,128)(2,1)}), bf16[2048,256]{1,0:T(8,128)(2,1)S(1)}, s32[]{:S(2)}) async-start(bf16[2400,256]{1,0:T(8,128)(2,1)} %copy-done.2), calls=%async_computation.4 | async-start | bytes 2097152 | tf_op jit(solution)/shard_map/slice | solution.py:159
  109.6 1.0 copy-start.8
  112.2 10.5 %all-to-all-start = ((bf16[4,32,2048]{2,1,0:T(8,128)(2,1)}), bf16[4,32,2048]{2,1,0:T(8,128)(2,1)S(1)}, u32[]{:S(2)}, u32[]{:S(2)}) async-start(bf16[4,32,2048]{2,1,0:T(8,128)(2,1)} %bitcast.127), calls=%async_computation | async-start | bytes 1048576 | tf_op jit(solution)/shard_map/all_to_all | solution.py:199
  140.8 7.7 %copy-start.10 = (bf16[128,512]{1,0:T(8,128)(2,1)S(1)}, bf16[128,512]{1,0:T(8,128)(2,1)}, u32[]{:S(2)}) copy-start(bf16[128,512]{1,0:T(8,128)(2,1)} %get-tuple-element.35) | copy-start | bytes 393220
  140.9 7.7 %collective-permute-start.6 = (bf16[32,512]{1,0:T(8,128)(2,1)}, bf16[32,512]{1,0:T(8,128)(2,1)S(1)}, u32[]{:S(2)}, u32[]{:S(2)}) collective-permute-start(bf16[32,512]{1,0:T(8,128)(2,1)} %get-tuple-element.34), channel_id=1, source_target_pairs={{0,1},{1,8},{8,9},{9,16},{16,17},{17,24},{24,25},{25,32},{32,33},{... | collective-permute-start | bytes 98312 | tf_op jit(solution)/shard_map/ppermute | solution.py:26
  179.8 7.8 %collective-permute-start.7 = (bf16[128,2048]{1,0:T(8,128)(2,1)S(1)}, bf16[128,2048]{1,0:T(8,128)(2,1)S(1)}, u32[]{:S(2)}, u32[]{:S(2)}) collective-permute-start(bf16[128,2048]{1,0:T(8,128)(2,1)S(1)} %all_gather.27), channel_id=1, source_target_pairs={{0,1},{1,0},{2,3},{3,2},{4,5},{5,4},{6,7},{7,6},{8,9},{9,8},{10,11... | collective-permute-start | bytes 1572872 | tf_op jit(solution)/shard_map/ppermute | solution.py:21
Sparse Core Ops, SparseCore 0:
  9.4 66.6 all-gather.2
  81.1 55.7 all-gather.4

commit v5 on v4

--- a/solution.py
+++ b/solution.py
@@ -199,7 +199,7 @@
         parts = lax.all_to_all(branch.reshape(xs, share, width), "x", 0, 0, tiled=True)
         own = lax.dynamic_slice_in_dim(stream, x * share, share, 0).astype(F32)
         own = (own + jnp.sum(parts.astype(F32), axis=0)).astype(BF16)
-        stream = lax.all_gather(own, "x", axis=0, tiled=True)
+        stream = sent_to_all(own, "x").reshape(half, width)
     sibling = shifted(stream, "c", 1)
     return jnp.where(
         c == 0,

time: 198 us -> 195 us (0.985)
  blocking collectives: 83.1 us -> 71.7 us
  waiting for transfers between devices: 18.8 us -> 26.1 us
    all_gather x2 -> x0, blocking collectives: 22.1 us -> none  [body(): stream = lax.all_gather(own, 'x', axis=0, tiled=True)]
    all_to_all x0 -> x1, blocking collectives: none -> 10.8 us  [sent_to_all(): return lax.all_to_all(copies, axis, split_axis=0, concat_axis=0, tiled=True)]
    all_to_all x0 -> x1, waiting for transfers between devices: none -> 6.92 us  [sent_to_all(): return lax.all_to_all(copies, axis, split_axis=0, concat_axis=0, tiled=True)]
    all_to_all x0 -> x1, starting transfers between devices: none -> 3.47 us  [sent_to_all(): return lax.all_to_all(copies, axis, split_axis=0, concat_axis=0, tiled=True)]
    ppermute x6, starting transfers between devices: 31.8 us -> 29.6 us  [shifted(): lax.ppermute(value, axis, [(i, (i + steps) % count) for i in range(count)])]
    unnamed x23 -> x25, local copies, waits for them, and re-layouts: 4.18 us -> 4.17 us
  transfers between devices with their start and end apart: 11 -> 12, of which waited for: 8 -> 10; matrix products, arithmetic and copies ran while one was open for 9% -> 9% of each run, Pallas kernels for 1% -> 1%
where the time goes in v5:
time: 195 us; the launch traced here: 194 us
  blocking collectives  71.7 us (37%)
  starting transfers between devices  44.2 us (23%)
  waiting for transfers between devices  26.1 us (13%)
  local copies, waits for them, and re-layouts  14.4 us (7%)
  between operations  13.7 us (7%)
  Pallas kernels  10.8 us (6%)
  other arithmetic  10.2 us (5%)
  matrix products  2.42 us (1%)
    all_gather x1, blocking collectives, body(): block = lax.all_gather(first, 'z', axis=0, tiled=True)  35.4 us
    ppermute x6, starting transfers between devices, shifted(): lax.ppermute(value, axis, [(i, (i + steps) % count) for i in range(count)])  29.6 us
    all_gather x2, blocking collectives, body(): lax.all_gather(sums.reshape(1, -1), 'x', axis=0)  13.7 us
    all_to_all x1, blocking collectives, body(): lax.all_to_all(branch.reshape(xs, share, width), 'x', 0, 0, tiled=True)  11.7 us
    all_to_all x1, blocking collectives, sent_to_all(): return lax.all_to_all(copies, axis, split_axis=0, concat_axis=0, tiled=True)  10.8 us
    pallas_call x3, Pallas kernels, call(): pl.pallas_call(kernel, out_shape=[jax.ShapeDtypeStruct(s, d) for s, d in...  10.8 us
    ppermute x2, starting transfers between devices, passed_on(): return lax.ppermute(value, axes, [(i, i + 1) for i in range(count - 1)])  7.63 us
    all_to_all x1, waiting for transfers between devices, sent_to_all(): return lax.all_to_all(copies, axis, split_axis=0, concat_axis=0, tiled=True)  6.92 us
  transfers between devices with their start and end apart: 12, of which 10 were waited for; matrix products, arithmetic and copies ran while one was open for 9% of the time, Pallas kernels for 1%

profile of v5, /device:TPU:1, one launch (start us, length us, event | category | flops | bytes accessed | tf_op | source)
XLA Modules:
  0.0 193.6 jit_solution(4601053240686586732)
XLA Ops:
  8.8 35.4 %all_gather.15.refs_0_ = bf16[512,768]{1,0:T(8,128)(2,1)S(1)} all-gather(bf16[32,768]{1,0:T(8,128)(2,1)S(1)} %pad_maximum_fusion.8), channel_id=1, replica_groups=mesh['z'=16,'y'=4,'x'=4,'c'=2] {'z'}, dimensions={0}, use_global_device_ids=true | all-gather | bytes 835584 | tf_op jit(solution)/shard_map/all_gather | solution.py:127
  44.3 3.0 %collective-permute-start = (bf16[512,768]{1,0:T(8,128)(2,1)S(1)}, bf16[512,768]{1,0:T(8,128)(2,1)S(1)}, u32[]{:S(2)}, u32[]{:S(2)}) collective-permute-start(bf16[512,768]{1,0:T(8,128)(2,1)S(1)} %all_gather.15.refs_0_), channel_id=1, source_target_pairs={{0,8},{8,16},{16,24},{24,0},{1,9},{9,17},{17,25},{25,1},{2,10},{10... | collective-permute-start | bytes 2359304 | tf_op jit(solution)/shard_map/ppermute | solution.py:21
  47.3 3.4 %collective-permute-start.1 = (bf16[512,768]{1,0:T(8,128)(2,1)S(1)}, bf16[512,768]{1,0:T(8,128)(2,1)S(1)}, u32[]{:S(2)}, u32[]{:S(2)}) collective-permute-start(bf16[512,768]{1,0:T(8,128)(2,1)S(1)} %all_gather.15.refs_0_), channel_id=1, source_target_pairs={{0,24},{8,0},{16,8},{24,16},{1,25},{9,1},{17,9},{25,17},{2,26},{10... | collective-permute-start | bytes 2359304 | tf_op jit(solution)/shard_map/ppermute | solution.py:21
  50.8 1.6 slice.551
  52.3 1.8 collective-permute-start.2
  54.2 1.5 copy.21
  57.2 1.4 fusion.63
  61.0 3.1 %collective-permute-start.3 = (bf16[256,768]{1,0:T(8,128)(2,1)S(1)}, bf16[256,768]{1,0:T(8,128)(2,1)S(1)}, u32[]{:S(2)}, u32[]{:S(2)}) collective-permute-start(bf16[256,768]{1,0:T(8,128)(2,1)S(1)} %slice.553), channel_id=1, source_target_pairs={{0,8},{8,16},{16,24},{24,0},{1,9},{9,17},{17,25},{25,1},{2,10},{10... | collective-permute-start | bytes 1179656 | tf_op jit(solution)/shard_map/ppermute | solution.py:21
  64.1 4.0 %collective-permute-start.4 = (bf16[256,768]{1,0:T(8,128)(2,1)S(1)}, bf16[256,768]{1,0:T(8,128)(2,1)}, u32[]{:S(2)}, u32[]{:S(2)}) collective-permute-start(bf16[256,768]{1,0:T(8,128)(2,1)S(1)} %slice.554), channel_id=1, source_target_pairs={{0,24},{8,0},{16,8},{24,16},{1,25},{9,1},{17,9},{25,17},{2,26},{10... | collective-permute-start | bytes 1179656 | tf_op jit(solution)/shard_map/ppermute | solution.py:21
  68.5 1.4 fusion.2.rows_ref
  69.8 1.8 collective-permute-done.3.refs_3_
  72.9 3.2 %all-gather.3.cloned.1.call-done.refs_5_ = bf16[512,1024]{1,0:T(8,128)(2,1)} async-done(((bf16[32,1024]{1,0:T(8,128)(2,1)}), bf16[512,1024]{1,0:T(8,128)(2,1)}) %all-gather.3.cloned.1.call-update) | async-done | bytes 1048592 | tf_op jit(solution)/shard_map/all_gather | solution.py:126
  76.1 4.8 %shard_map.73 = (bf16[160,256]{1,0:T(8,128)(2,1)}, bf16[2400,256]{1,0:T(8,128)(2,1)}, bf16[512,768]{1,0:T(8,128)(2,1)}) custom-call(s32[2]{0:T(128)} %pad_add_fusion.at_ref, bf16[288,2048]{1,0:T(8,128)(2,1)} %fusion.2.rows_ref, bf16[192,256]{1,0:T(8,128)(2,1)} %bitcast.135, bf16[512,768]{1,0:T(8,128)(2,1)} %copy-done.4, bf16[512,768]{1,0:T(8,128)(2,1)} %copy-done.6, ...), custom_call_target="tpu_custom_call" | custom-call | tf_op jit(solution)/shard_map/pallas_call | solution.py:44
  81.0 12.1 %collective-permute-start.5 = (bf16[2400,256]{1,0:T(8,128)(2,1)}, bf16[2400,256]{1,0:T(8,128)(2,1)S(1)}, u32[]{:S(2)}, u32[]{:S(2)}) collective-permute-start(bf16[2400,256]{1,0:T(8,128)(2,1)} %get-tuple-element.29), channel_id=1, source_target_pairs={{0,1},{1,0},{2,3},{3,2},{4,5},{5,4},{6,7},{7,6},{8,9},{9,8},{10,11... | collective-permute-start | bytes 3686408 | tf_op jit(solution)/shard_map/ppermute | solution.py:21
  94.4 1.4 collective-permute-done.5.got_ref
  96.9 2.1 %shard_map.74 = (f32[160,512]{1,0:T(8,128)}, f32[64,256]{1,0:T(8,128)}) custom-call(bf16[160,256]{1,0:T(8,128)(2,1)} %get-tuple-element.28.keep_ref, bf16[2400,256]{1,0:T(8,128)(2,1)} %copy-done.2), custom_call_target="tpu_custom_call" | custom-call | tf_op jit(solution)/shard_map/pallas_call | solution.py:44
  100.1 1.8 fusion.58
  101.9 7.6 %all_gather.17 = f32[4,1,256]{2,1,0:T(1,128)S(1)} all-gather(f32[1,1,256]{2,1,0:T(1,128)S(1)} %bitcast.209), channel_id=1, replica_groups=mesh['z'=16,'y'=4,'x'=4,'c'=2] {'x'}, dimensions={0}, use_global_device_ids=true | all-gather | bytes 5120 | tf_op jit(solution)/shard_map/all_gather | solution.py:191
  110.5 1.6 convolution_convert_fusion.1
  112.1 3.5 %all-to-all-start = ((bf16[4,32,2048]{2,1,0:T(8,128)(2,1)}), bf16[4,32,2048]{2,1,0:T(8,128)(2,1)S(1)}, u32[]{:S(2)}, u32[]{:S(2)}) async-start(bf16[4,32,2048]{2,1,0:T(8,128)(2,1)} %bitcast.133), calls=%async_computation | async-start | bytes 1048576 | tf_op jit(solution)/shard_map/all_to_all | solution.py:199
  115.8 6.8 %all-to-all-done = bf16[4,32,2048]{2,1,0:T(8,128)(2,1)S(1)} async-done(((bf16[4,32,2048]{2,1,0:T(8,128)(2,1)}), bf16[4,32,2048]{2,1,0:T(8,128)(2,1)S(1)}, u32[]{:S(2)}, u32[]{:S(2)}) %all-to-all-start) | async-done | bytes 524320 | tf_op jit(solution)/shard_map/all_to_all | solution.py:199
  123.6 3.5 %all-to-all-start.1 = ((bf16[4,32,2048]{2,1,0:T(8,128)(2,1)}), bf16[4,32,2048]{2,1,0:T(8,128)(2,1)S(1)}, u32[]{:S(2)}, u32[]{:S(2)}) async-start(bf16[4,32,2048]{2,1,0:T(8,128)(2,1)} %broadcast_in_dim.11), calls=%async_computation.1 | async-start | bytes 1048576 | tf_op jit(solution)/shard_map/all_to_all | solution.py:31
  127.1 6.9 %all-to-all-done.1 = bf16[4,32,2048]{2,1,0:T(8,128)(2,1)S(1)} async-done(((bf16[4,32,2048]{2,1,0:T(8,128)(2,1)}), bf16[4,32,2048]{2,1,0:T(8,128)(2,1)S(1)}, u32[]{:S(2)}, u32[]{:S(2)}) %all-to-all-start.1) | async-done | bytes 524320 | tf_op jit(solution)/shard_map/all_to_all | solution.py:31
  134.0 2.8 %all-gather.5.cloned.1.call-done = bf16[16,8,32,768]{3,2,1,0:T(8,128)(2,1)} async-done(((bf16[16,1,32,768]{3,2,1,0:T(8,128)(2,1)}), bf16[16,8,32,768]{3,2,1,0:T(8,128)(2,1)}) %all-gather.5.cloned.1.call-update) | async-done | bytes 6291472 | tf_op jit(solution)/shard_map/all_gather | solution.py:155
  136.8 3.9 %shard_map.75 = (bf16[128,512]{1,0:T(8,128)(2,1)}, bf16[32,512]{1,0:T(8,128)(2,1)}) custom-call(bf16[128,2048]{1,0:T(8,128)(2,1)} %bitcast.126, f32[1,2048]{1,0:T(1,128)} %get-tuple-element.118.gain_ref, bf16[16,2,128,768]{3,2,1,0:T(8,128)(2,1)} %bitcast.124), custom_call_target="tpu_custom_call" | custom-call | tf_op jit(solution)/shard_map/pallas_call | solution.py:44
  140.7 5.8 %collective-permute-start.6 = (bf16[32,512]{1,0:T(8,128)(2,1)}, bf16[32,512]{1,0:T(8,128)(2,1)S(1)}, u32[]{:S(2)}, u32[]{:S(2)}) collective-permute-start(bf16[32,512]{1,0:T(8,128)(2,1)} %get-tuple-element.34), channel_id=1, source_target_pairs={{0,1},{1,8},{8,9},{9,16},{16,17},{17,24},{24,25},{25,32},{32,33},{... | collective-permute-start | bytes 98312 | tf_op jit(solution)/shard_map/ppermute | solution.py:26
  146.5 1.7 fusion.60
  149.5 6.1 %all_gather.19 = f32[4,1,256]{2,1,0:T(1,128)S(1)} all-gather(f32[1,1,256]{2,1,0:T(1,128)S(1)} %bitcast.210), channel_id=1, replica_groups=mesh['z'=16,'y'=4,'x'=4,'c'=2] {'x'}, dimensions={0}, use_global_device_ids=true | all-gather | bytes 5120 | tf_op jit(solution)/shard_map/all_gather | solution.py:191
  156.5 11.7 %all_to_all.20 = bf16[4,32,2048]{2,1,0:T(8,128)(2,1)S(1)} all-to-all(bf16[4,32,2048]{2,1,0:T(8,128)(2,1)S(1)} %bitcast.134), channel_id=1, replica_groups=mesh['z'=16,'y'=4,'x'=4,'c'=2] {'x'}, dimensions={0} | all-to-all | bytes 1048576 | tf_op jit(solution)/shard_map/all_to_all | solution.py:199
  169.2 10.8 %all_to_all.21 = bf16[4,32,2048]{2,1,0:T(8,128)(2,1)S(1)} all-to-all(bf16[4,32,2048]{2,1,0:T(8,128)(2,1)S(1)} %broadcast_in_dim.12), channel_id=1, replica_groups=mesh['z'=16,'y'=4,'x'=4,'c'=2] {'x'}, dimensions={0} | all-to-all | bytes 1048576 | tf_op jit(solution)/shard_map/all_to_all | solution.py:31
  180.1 3.9 %collective-permute-start.7 = (bf16[128,2048]{1,0:T(8,128)(2,1)S(1)}, bf16[128,2048]{1,0:T(8,128)(2,1)S(1)}, u32[]{:S(2)}, u32[]{:S(2)}) collective-permute-start(bf16[128,2048]{1,0:T(8,128)(2,1)S(1)} %bitcast.128), channel_id=1, source_target_pairs={{0,1},{1,0},{2,3},{3,2},{4,5},{5,4},{6,7},{7,6},{8,9},{9,8},{10,11... | collective-permute-start | bytes 1572872 | tf_op jit(solution)/shard_map/ppermute | solution.py:21
  184.0 1.5 collective-permute-done.7
  (76 shorter events, 17.6 us)
Async XLA Ops:
  6.5 61.6 %copy-start.1 = (bf16[256,2048]{1,0:T(8,128)(2,1)S(1)}, bf16[256,2048]{1,0:T(8,128)(2,1)}, u32[]{:S(2)}) copy-start(bf16[256,2048]{1,0:T(8,128)(2,1)} %param.7) | copy-start | bytes 3145732
  6.5 69.6 %all-gather.3.cloned.1.call-start = ((), (), s32[]{:S(2)}) async-start(), calls=%async_computation.4 | async-start | bytes 1114112 | tf_op jit(solution)/shard_map/all_gather | solution.py:126
  8.8 128.0 %all-gather.5.cloned.1.call-start = ((), (), s32[]{:S(2)}) async-start(), calls=%async_computation.5 | async-start | bytes 7077888 | tf_op jit(solution)/shard_map/all_gather | solution.py:155
  44.3 25.6 %copy-start.4 = (bf16[512,768]{1,0:T(8,128)(2,1)}, bf16[512,768]{1,0:T(8,128)(2,1)S(1)}, u32[]{:S(2)}) copy-start(bf16[512,768]{1,0:T(8,128)(2,1)S(1)} %all_gather.15.refs_0_) | copy-start | bytes 2359300
  44.3 15.6 %collective-permute-start = (bf16[512,768]{1,0:T(8,128)(2,1)S(1)}, bf16[512,768]{1,0:T(8,128)(2,1)S(1)}, u32[]{:S(2)}, u32[]{:S(2)}) collective-permute-start(bf16[512,768]{1,0:T(8,128)(2,1)S(1)} %all_gather.15.refs_0_), channel_id=1, source_target_pairs={{0,8},{8,16},{16,24},{24,0},{1,9},{9,17},{17,25},{25,1},{2,10},{10... | collective-permute-start | bytes 2359304 | tf_op jit(solution)/shard_map/ppermute | solution.py:21
  47.3 13.6 %collective-permute-start.1 = (bf16[512,768]{1,0:T(8,128)(2,1)S(1)}, bf16[512,768]{1,0:T(8,128)(2,1)S(1)}, u32[]{:S(2)}, u32[]{:S(2)}) collective-permute-start(bf16[512,768]{1,0:T(8,128)(2,1)S(1)} %all_gather.15.refs_0_), channel_id=1, source_target_pairs={{0,24},{8,0},{16,8},{24,16},{1,25},{9,1},{17,9},{25,17},{2,26},{10... | collective-permute-start | bytes 2359304 | tf_op jit(solution)/shard_map/ppermute | solution.py:21
  52.3 7.6 %collective-permute-start.2 = (bf16[32,2048]{1,0:T(8,128)(2,1)}, bf16[32,2048]{1,0:T(8,128)(2,1)S(1)}, u32[]{:S(2)}, u32[]{:S(2)}) collective-permute-start(bf16[32,2048]{1,0:T(8,128)(2,1)} %slice.551), channel_id=1, source_target_pairs={{0,8},{8,16},{16,24},{24,32},{32,40},{40,48},{48,56},{56,64},{64,7... | collective-permute-start | bytes 393224 | tf_op jit(solution)/shard_map/ppermute | solution.py:26
  59.9 9.9 %copy-start.6 = (bf16[512,768]{1,0:T(8,128)(2,1)}, bf16[512,768]{1,0:T(8,128)(2,1)S(1)}, u32[]{:S(2)}) copy-start(bf16[512,768]{1,0:T(8,128)(2,1)S(1)} %collective-permute-done.refs_1_) | copy-start | bytes 2359300
  60.9 8.9 %copy-start.7 = (bf16[512,768]{1,0:T(8,128)(2,1)}, bf16[512,768]{1,0:T(8,128)(2,1)S(1)}, u32[]{:S(2)}) copy-start(bf16[512,768]{1,0:T(8,128)(2,1)S(1)} %collective-permute-done.1.refs_2_) | copy-start | bytes 2359300
  61.0 10.7 %collective-permute-start.3 = (bf16[256,768]{1,0:T(8,128)(2,1)S(1)}, bf16[256,768]{1,0:T(8,128)(2,1)S(1)}, u32[]{:S(2)}, u32[]{:S(2)}) collective-permute-start(bf16[256,768]{1,0:T(8,128)(2,1)S(1)} %slice.553), channel_id=1, source_target_pairs={{0,8},{8,16},{16,24},{24,0},{1,9},{9,17},{17,25},{25,1},{2,10},{10... | collective-permute-start | bytes 1179656 | tf_op jit(solution)/shard_map/ppermute | solution.py:21
  64.1 8.8 %collective-permute-start.4 = (bf16[256,768]{1,0:T(8,128)(2,1)S(1)}, bf16[256,768]{1,0:T(8,128)(2,1)}, u32[]{:S(2)}, u32[]{:S(2)}) collective-permute-start(bf16[256,768]{1,0:T(8,128)(2,1)S(1)} %slice.554), channel_id=1, source_target_pairs={{0,24},{8,0},{16,8},{24,16},{1,25},{9,1},{17,9},{25,17},{2,26},{10... | collective-permute-start | bytes 1179656 | tf_op jit(solution)/shard_map/ppermute | solution.py:21
  71.7 0.8 copy-start.8
  81.0 18.9 %copy-start.3 = (f32[2,31,256]{2,0,1:T(2,128)S(1)}, f32[2,31,256]{2,0,1:T(2,128)}, u32[]{:S(2)}) copy-start(f32[2,31,256]{2,0,1:T(2,128)} %param.11) | copy-start | bytes 190468
  81.0 19.0 %copy-start.10 = (f32[2,256]{1,0:T(2,128)S(1)}, f32[2,256]{1,0:T(2,128)}, u32[]{:S(2)}) copy-start(f32[2,256]{1,0:T(2,128)} %param.12) | copy-start | bytes 6148
  81.0 14.9 %collective-permute-start.5 = (bf16[2400,256]{1,0:T(8,128)(2,1)}, bf16[2400,256]{1,0:T(8,128)(2,1)S(1)}, u32[]{:S(2)}, u32[]{:S(2)}) collective-permute-start(bf16[2400,256]{1,0:T(8,128)(2,1)} %get-tuple-element.29), channel_id=1, source_target_pairs={{0,1},{1,0},{2,3},{3,2},{4,5},{5,4},{6,7},{7,6},{8,9},{9,8},{10,11... | collective-permute-start | bytes 3686408 | tf_op jit(solution)/shard_map/ppermute | solution.py:21
  95.9 1.0 copy-start.2
  99.0 1.1 copy-start
  101.9 7.7 %slice-start = ((bf16[2400,256]{1,0:T(8,128)(2,1)}), bf16[2048,256]{1,0:T(8,128)(2,1)S(1)}, s32[]{:S(2)}) async-start(bf16[2400,256]{1,0:T(8,128)(2,1)} %copy-done.2), calls=%async_computation.6 | async-start | bytes 2097152 | tf_op jit(solution)/shard_map/slice | solution.py:159
  109.6 1.0 copy-start.9
  112.1 10.4 %all-to-all-start = ((bf16[4,32,2048]{2,1,0:T(8,128)(2,1)}), bf16[4,32,2048]{2,1,0:T(8,128)(2,1)S(1)}, u32[]{:S(2)}, u32[]{:S(2)}) async-start(bf16[4,32,2048]{2,1,0:T(8,128)(2,1)} %bitcast.133), calls=%async_computation | async-start | bytes 1048576 | tf_op jit(solution)/shard_map/all_to_all | solution.py:199
  123.6 10.4 %all-to-all-start.1 = ((bf16[4,32,2048]{2,1,0:T(8,128)(2,1)}), bf16[4,32,2048]{2,1,0:T(8,128)(2,1)S(1)}, u32[]{:S(2)}, u32[]{:S(2)}) async-start(bf16[4,32,2048]{2,1,0:T(8,128)(2,1)} %broadcast_in_dim.11), calls=%async_computation.1 | async-start | bytes 1048576 | tf_op jit(solution)/shard_map/all_to_all | solution.py:31
  134.0 2.8 %copy-start.5 = (bf16[4,32,2048]{2,1,0:T(8,128)(2,1)}, bf16[4,32,2048]{2,1,0:T(8,128)(2,1)S(1)}, u32[]{:S(2)}) copy-start(bf16[4,32,2048]{2,1,0:T(8,128)(2,1)S(1)} %all-to-all-done.1) | copy-start | bytes 1572868
  140.7 7.6 %copy-start.11 = (bf16[128,512]{1,0:T(8,128)(2,1)S(1)}, bf16[128,512]{1,0:T(8,128)(2,1)}, u32[]{:S(2)}) copy-start(bf16[128,512]{1,0:T(8,128)(2,1)} %get-tuple-element.35) | copy-start | bytes 393220
  140.7 7.6 %collective-permute-start.6 = (bf16[32,512]{1,0:T(8,128)(2,1)}, bf16[32,512]{1,0:T(8,128)(2,1)S(1)}, u32[]{:S(2)}, u32[]{:S(2)}) collective-permute-start(bf16[32,512]{1,0:T(8,128)(2,1)} %get-tuple-element.34), channel_id=1, source_target_pairs={{0,1},{1,8},{8,9},{9,16},{16,17},{17,24},{24,25},{25,32},{32,33},{... | collective-permute-start | bytes 98312 | tf_op jit(solution)/shard_map/ppermute | solution.py:26
  180.1 5.4 %collective-permute-start.7 = (bf16[128,2048]{1,0:T(8,128)(2,1)S(1)}, bf16[128,2048]{1,0:T(8,128)(2,1)S(1)}, u32[]{:S(2)}, u32[]{:S(2)}) collective-permute-start(bf16[128,2048]{1,0:T(8,128)(2,1)S(1)} %bitcast.128), channel_id=1, source_target_pairs={{0,1},{1,0},{2,3},{3,2},{4,5},{5,4},{6,7},{7,6},{8,9},{9,8},{10,11... | collective-permute-start | bytes 1572872 | tf_op jit(solution)/shard_map/ppermute | solution.py:21
Sparse Core Ops, SparseCore 0:
  9.4 66.6 all-gather.2
  81.1 55.6 all-gather.4

commit v6 on v5

--- a/solution.py
+++ b/solution.py
@@ -86,13 +86,11 @@
     send_ref[at + count :, :] = small_ref[...]
 
 
-def second_kernel(cols, rows_ref, gain_ref, later_ref, gated_ref, tail_ref, scaled, weights):
+def second_kernel(cols, rows_ref, gain_ref, later_ref, gated_ref, tail_ref, scaled):
     normed(rows_ref, gain_ref, scaled)
-    zs, cores, deep, _ = later_ref.shape
+    zs, cores, deep, wide = later_ref.shape
     for core in range(cores):
-        for k in range(zs):
-            weights[k * deep : (k + 1) * deep, :] = later_ref[k, core]
-        part = gate_of(scaled[...], weights, cols)
+        part = gate_of(scaled[...], later_ref[:, core].reshape(zs * deep, wide), cols)
         gated_ref[:, core * cols : (core + 1) * cols] = part
         tail_ref[:, core * cols : (core + 1) * cols] = part[-HALO:]
 
@@ -176,7 +174,7 @@
                 stream,
                 norm_gain[1:],
                 later,
-                scratch=[(stream.shape, BF16), ((width, 2 * cols), BF16)],
+                scratch=[(stream.shape, BF16)],
                 last=pl.BlockSpec((*later.shape[:3], 2 * cols), lambda _: (0, 0, 0, 0)),
             )
             columns, tail = lax.optimization_barrier((later, tail))

time: 195 us -> 195 us (level)
  no operation moved by 1% of the time
where the time goes in v6:
time: 195 us; the launch traced here: 194 us
  blocking collectives  71.7 us (37%)
  starting transfers between devices  44.2 us (23%)
  waiting for transfers between devices  26.1 us (13%)
  local copies, waits for them, and re-layouts  14.4 us (7%)
  between operations  13.7 us (7%)
  Pallas kernels  10.8 us (6%)
  other arithmetic  10.2 us (5%)
  matrix products  2.42 us (1%)
    all_gather x1, blocking collectives, body(): block = lax.all_gather(first, 'z', axis=0, tiled=True)  35.4 us
    ppermute x6, starting transfers between devices, shifted(): lax.ppermute(value, axis, [(i, (i + steps) % count) for i in range(count)])  29.6 us
    all_gather x2, blocking collectives, body(): lax.all_gather(sums.reshape(1, -1), 'x', axis=0)  13.7 us
    all_to_all x1, blocking collectives, body(): lax.all_to_all(branch.reshape(xs, share, width), 'x', 0, 0, tiled=True)  11.7 us
    all_to_all x1, blocking collectives, sent_to_all(): return lax.all_to_all(copies, axis, split_axis=0, concat_axis=0, tiled=True)  10.8 us
    pallas_call x3, Pallas kernels, call(): pl.pallas_call(kernel, out_shape=[jax.ShapeDtypeStruct(s, d) for s, d in...  10.8 us
    ppermute x2, starting transfers between devices, passed_on(): return lax.ppermute(value, axes, [(i, i + 1) for i in range(count - 1)])  7.63 us
    all_to_all x1, waiting for transfers between devices, sent_to_all(): return lax.all_to_all(copies, axis, split_axis=0, concat_axis=0, tiled=True)  6.92 us
  transfers between devices with their start and end apart: 12, of which 10 were waited for; matrix products, arithmetic and copies ran while one was open for 9% of the time, Pallas kernels for 1%

profile of v6, /device:TPU:1, one launch (start us, length us, event | category | flops | bytes accessed | tf_op | source)
XLA Modules:
  0.0 193.6 jit_solution(4601053240686586732)
XLA Ops:
  8.8 35.4 %all_gather.15.refs_0_ = bf16[512,768]{1,0:T(8,128)(2,1)S(1)} all-gather(bf16[32,768]{1,0:T(8,128)(2,1)S(1)} %pad_maximum_fusion.8), channel_id=1, replica_groups=mesh['z'=16,'y'=4,'x'=4,'c'=2] {'z'}, dimensions={0}, use_global_device_ids=true | all-gather | bytes 835584 | tf_op jit(solution)/shard_map/all_gather | solution.py:125
  44.3 3.0 %collective-permute-start = (bf16[512,768]{1,0:T(8,128)(2,1)S(1)}, bf16[512,768]{1,0:T(8,128)(2,1)S(1)}, u32[]{:S(2)}, u32[]{:S(2)}) collective-permute-start(bf16[512,768]{1,0:T(8,128)(2,1)S(1)} %all_gather.15.refs_0_), channel_id=1, source_target_pairs={{0,8},{8,16},{16,24},{24,0},{1,9},{9,17},{17,25},{25,1},{2,10},{10... | collective-permute-start | bytes 2359304 | tf_op jit(solution)/shard_map/ppermute | solution.py:21
  47.3 3.4 %collective-permute-start.1 = (bf16[512,768]{1,0:T(8,128)(2,1)S(1)}, bf16[512,768]{1,0:T(8,128)(2,1)S(1)}, u32[]{:S(2)}, u32[]{:S(2)}) collective-permute-start(bf16[512,768]{1,0:T(8,128)(2,1)S(1)} %all_gather.15.refs_0_), channel_id=1, source_target_pairs={{0,24},{8,0},{16,8},{24,16},{1,25},{9,1},{17,9},{25,17},{2,26},{10... | collective-permute-start | bytes 2359304 | tf_op jit(solution)/shard_map/ppermute | solution.py:21
  50.8 1.6 slice.551
  52.3 1.8 collective-permute-start.2
  54.2 1.5 copy.21
  57.2 1.4 fusion.63
  61.0 3.1 %collective-permute-start.3 = (bf16[256,768]{1,0:T(8,128)(2,1)S(1)}, bf16[256,768]{1,0:T(8,128)(2,1)S(1)}, u32[]{:S(2)}, u32[]{:S(2)}) collective-permute-start(bf16[256,768]{1,0:T(8,128)(2,1)S(1)} %slice.553), channel_id=1, source_target_pairs={{0,8},{8,16},{16,24},{24,0},{1,9},{9,17},{17,25},{25,1},{2,10},{10... | collective-permute-start | bytes 1179656 | tf_op jit(solution)/shard_map/ppermute | solution.py:21
  64.1 4.0 %collective-permute-start.4 = (bf16[256,768]{1,0:T(8,128)(2,1)S(1)}, bf16[256,768]{1,0:T(8,128)(2,1)}, u32[]{:S(2)}, u32[]{:S(2)}) collective-permute-start(bf16[256,768]{1,0:T(8,128)(2,1)S(1)} %slice.554), channel_id=1, source_target_pairs={{0,24},{8,0},{16,8},{24,16},{1,25},{9,1},{17,9},{25,17},{2,26},{10... | collective-permute-start | bytes 1179656 | tf_op jit(solution)/shard_map/ppermute | solution.py:21
  68.5 1.4 fusion.2.rows_ref
  69.8 1.8 collective-permute-done.3.refs_3_
  72.9 3.2 %all-gather.3.cloned.1.call-done.refs_5_ = bf16[512,1024]{1,0:T(8,128)(2,1)} async-done(((bf16[32,1024]{1,0:T(8,128)(2,1)}), bf16[512,1024]{1,0:T(8,128)(2,1)}) %all-gather.3.cloned.1.call-update) | async-done | bytes 1048592 | tf_op jit(solution)/shard_map/all_gather | solution.py:124
  76.1 4.8 %shard_map.73 = (bf16[160,256]{1,0:T(8,128)(2,1)}, bf16[2400,256]{1,0:T(8,128)(2,1)}, bf16[512,768]{1,0:T(8,128)(2,1)}) custom-call(s32[2]{0:T(128)} %pad_add_fusion.at_ref, bf16[288,2048]{1,0:T(8,128)(2,1)} %fusion.2.rows_ref, bf16[192,256]{1,0:T(8,128)(2,1)} %bitcast.135, bf16[512,768]{1,0:T(8,128)(2,1)} %copy-done.4, bf16[512,768]{1,0:T(8,128)(2,1)} %copy-done.6, ...), custom_call_target="tpu_custom_call" | custom-call | tf_op jit(solution)/shard_map/pallas_call | solution.py:44
  81.0 12.1 %collective-permute-start.5 = (bf16[2400,256]{1,0:T(8,128)(2,1)}, bf16[2400,256]{1,0:T(8,128)(2,1)S(1)}, u32[]{:S(2)}, u32[]{:S(2)}) collective-permute-start(bf16[2400,256]{1,0:T(8,128)(2,1)} %get-tuple-element.29), channel_id=1, source_target_pairs={{0,1},{1,0},{2,3},{3,2},{4,5},{5,4},{6,7},{7,6},{8,9},{9,8},{10,11... | collective-permute-start | bytes 3686408 | tf_op jit(solution)/shard_map/ppermute | solution.py:21
  94.4 1.4 collective-permute-done.5.got_ref
  96.9 2.1 %shard_map.74 = (f32[160,512]{1,0:T(8,128)}, f32[64,256]{1,0:T(8,128)}) custom-call(bf16[160,256]{1,0:T(8,128)(2,1)} %get-tuple-element.28.keep_ref, bf16[2400,256]{1,0:T(8,128)(2,1)} %copy-done.2), custom_call_target="tpu_custom_call" | custom-call | tf_op jit(solution)/shard_map/pallas_call | solution.py:44
  100.1 1.8 fusion.58
  101.9 7.6 %all_gather.17 = f32[4,1,256]{2,1,0:T(1,128)S(1)} all-gather(f32[1,1,256]{2,1,0:T(1,128)S(1)} %bitcast.209), channel_id=1, replica_groups=mesh['z'=16,'y'=4,'x'=4,'c'=2] {'x'}, dimensions={0}, use_global_device_ids=true | all-gather | bytes 5120 | tf_op jit(solution)/shard_map/all_gather | solution.py:189
  110.5 1.6 convolution_convert_fusion.1
  112.1 3.5 %all-to-all-start = ((bf16[4,32,2048]{2,1,0:T(8,128)(2,1)}), bf16[4,32,2048]{2,1,0:T(8,128)(2,1)S(1)}, u32[]{:S(2)}, u32[]{:S(2)}) async-start(bf16[4,32,2048]{2,1,0:T(8,128)(2,1)} %bitcast.133), calls=%async_computation | async-start | bytes 1048576 | tf_op jit(solution)/shard_map/all_to_all | solution.py:197
  115.8 6.8 %all-to-all-done = bf16[4,32,2048]{2,1,0:T(8,128)(2,1)S(1)} async-done(((bf16[4,32,2048]{2,1,0:T(8,128)(2,1)}), bf16[4,32,2048]{2,1,0:T(8,128)(2,1)S(1)}, u32[]{:S(2)}, u32[]{:S(2)}) %all-to-all-start) | async-done | bytes 524320 | tf_op jit(solution)/shard_map/all_to_all | solution.py:197
  123.6 3.5 %all-to-all-start.1 = ((bf16[4,32,2048]{2,1,0:T(8,128)(2,1)}), bf16[4,32,2048]{2,1,0:T(8,128)(2,1)S(1)}, u32[]{:S(2)}, u32[]{:S(2)}) async-start(bf16[4,32,2048]{2,1,0:T(8,128)(2,1)} %broadcast_in_dim.11), calls=%async_computation.1 | async-start | bytes 1048576 | tf_op jit(solution)/shard_map/all_to_all | solution.py:31
  127.1 6.9 %all-to-all-done.1 = bf16[4,32,2048]{2,1,0:T(8,128)(2,1)S(1)} async-done(((bf16[4,32,2048]{2,1,0:T(8,128)(2,1)}), bf16[4,32,2048]{2,1,0:T(8,128)(2,1)S(1)}, u32[]{:S(2)}, u32[]{:S(2)}) %all-to-all-start.1) | async-done | bytes 524320 | tf_op jit(solution)/shard_map/all_to_all | solution.py:31
  134.0 2.8 %all-gather.5.cloned.1.call-done = bf16[16,8,32,768]{3,2,1,0:T(8,128)(2,1)} async-done(((bf16[16,1,32,768]{3,2,1,0:T(8,128)(2,1)}), bf16[16,8,32,768]{3,2,1,0:T(8,128)(2,1)}) %all-gather.5.cloned.1.call-update) | async-done | bytes 6291472 | tf_op jit(solution)/shard_map/all_gather | solution.py:153
  136.8 3.9 %shard_map.75 = (bf16[128,512]{1,0:T(8,128)(2,1)}, bf16[32,512]{1,0:T(8,128)(2,1)}) custom-call(bf16[128,2048]{1,0:T(8,128)(2,1)} %bitcast.126, f32[1,2048]{1,0:T(1,128)} %get-tuple-element.118.gain_ref, bf16[16,2,128,768]{3,2,1,0:T(8,128)(2,1)} %bitcast.124), custom_call_target="tpu_custom_call" | custom-call | tf_op jit(solution)/shard_map/pallas_call | solution.py:44
  140.7 5.8 %collective-permute-start.6 = (bf16[32,512]{1,0:T(8,128)(2,1)}, bf16[32,512]{1,0:T(8,128)(2,1)S(1)}, u32[]{:S(2)}, u32[]{:S(2)}) collective-permute-start(bf16[32,512]{1,0:T(8,128)(2,1)} %get-tuple-element.34), channel_id=1, source_target_pairs={{0,1},{1,8},{8,9},{9,16},{16,17},{17,24},{24,25},{25,32},{32,33},{... | collective-permute-start | bytes 98312 | tf_op jit(solution)/shard_map/ppermute | solution.py:26
  146.5 1.7 fusion.60
  149.5 6.1 %all_gather.19 = f32[4,1,256]{2,1,0:T(1,128)S(1)} all-gather(f32[1,1,256]{2,1,0:T(1,128)S(1)} %bitcast.210), channel_id=1, replica_groups=mesh['z'=16,'y'=4,'x'=4,'c'=2] {'x'}, dimensions={0}, use_global_device_ids=true | all-gather | bytes 5120 | tf_op jit(solution)/shard_map/all_gather | solution.py:189
  156.5 11.7 %all_to_all.20 = bf16[4,32,2048]{2,1,0:T(8,128)(2,1)S(1)} all-to-all(bf16[4,32,2048]{2,1,0:T(8,128)(2,1)S(1)} %bitcast.134), channel_id=1, replica_groups=mesh['z'=16,'y'=4,'x'=4,'c'=2] {'x'}, dimensions={0} | all-to-all | bytes 1048576 | tf_op jit(solution)/shard_map/all_to_all | solution.py:197
  169.2 10.8 %all_to_all.21 = bf16[4,32,2048]{2,1,0:T(8,128)(2,1)S(1)} all-to-all(bf16[4,32,2048]{2,1,0:T(8,128)(2,1)S(1)} %broadcast_in_dim.12), channel_id=1, replica_groups=mesh['z'=16,'y'=4,'x'=4,'c'=2] {'x'}, dimensions={0} | all-to-all | bytes 1048576 | tf_op jit(solution)/shard_map/all_to_all | solution.py:31
  180.1 3.9 %collective-permute-start.7 = (bf16[128,2048]{1,0:T(8,128)(2,1)S(1)}, bf16[128,2048]{1,0:T(8,128)(2,1)S(1)}, u32[]{:S(2)}, u32[]{:S(2)}) collective-permute-start(bf16[128,2048]{1,0:T(8,128)(2,1)S(1)} %bitcast.128), channel_id=1, source_target_pairs={{0,1},{1,0},{2,3},{3,2},{4,5},{5,4},{6,7},{7,6},{8,9},{9,8},{10,11... | collective-permute-start | bytes 1572872 | tf_op jit(solution)/shard_map/ppermute | solution.py:21
  184.0 1.5 collective-permute-done.7
  (76 shorter events, 17.6 us)
Async XLA Ops:
  6.5 61.6 %copy-start.1 = (bf16[256,2048]{1,0:T(8,128)(2,1)S(1)}, bf16[256,2048]{1,0:T(8,128)(2,1)}, u32[]{:S(2)}) copy-start(bf16[256,2048]{1,0:T(8,128)(2,1)} %param.7) | copy-start | bytes 3145732
  6.5 69.6 %all-gather.3.cloned.1.call-start = ((), (), s32[]{:S(2)}) async-start(), calls=%async_computation.4 | async-start | bytes 1114112 | tf_op jit(solution)/shard_map/all_gather | solution.py:124
  8.8 128.0 %all-gather.5.cloned.1.call-start = ((), (), s32[]{:S(2)}) async-start(), calls=%async_computation.5 | async-start | bytes 7077888 | tf_op jit(solution)/shard_map/all_gather | solution.py:153
  44.3 25.6 %copy-start.4 = (bf16[512,768]{1,0:T(8,128)(2,1)}, bf16[512,768]{1,0:T(8,128)(2,1)S(1)}, u32[]{:S(2)}) copy-start(bf16[512,768]{1,0:T(8,128)(2,1)S(1)} %all_gather.15.refs_0_) | copy-start | bytes 2359300
  44.3 15.6 %collective-permute-start = (bf16[512,768]{1,0:T(8,128)(2,1)S(1)}, bf16[512,768]{1,0:T(8,128)(2,1)S(1)}, u32[]{:S(2)}, u32[]{:S(2)}) collective-permute-start(bf16[512,768]{1,0:T(8,128)(2,1)S(1)} %all_gather.15.refs_0_), channel_id=1, source_target_pairs={{0,8},{8,16},{16,24},{24,0},{1,9},{9,17},{17,25},{25,1},{2,10},{10... | collective-permute-start | bytes 2359304 | tf_op jit(solution)/shard_map/ppermute | solution.py:21
  47.3 13.6 %collective-permute-start.1 = (bf16[512,768]{1,0:T(8,128)(2,1)S(1)}, bf16[512,768]{1,0:T(8,128)(2,1)S(1)}, u32[]{:S(2)}, u32[]{:S(2)}) collective-permute-start(bf16[512,768]{1,0:T(8,128)(2,1)S(1)} %all_gather.15.refs_0_), channel_id=1, source_target_pairs={{0,24},{8,0},{16,8},{24,16},{1,25},{9,1},{17,9},{25,17},{2,26},{10... | collective-permute-start | bytes 2359304 | tf_op jit(solution)/shard_map/ppermute | solution.py:21
  52.3 7.6 %collective-permute-start.2 = (bf16[32,2048]{1,0:T(8,128)(2,1)}, bf16[32,2048]{1,0:T(8,128)(2,1)S(1)}, u32[]{:S(2)}, u32[]{:S(2)}) collective-permute-start(bf16[32,2048]{1,0:T(8,128)(2,1)} %slice.551), channel_id=1, source_target_pairs={{0,8},{8,16},{16,24},{24,32},{32,40},{40,48},{48,56},{56,64},{64,7... | collective-permute-start | bytes 393224 | tf_op jit(solution)/shard_map/ppermute | solution.py:26
  59.9 9.9 %copy-start.6 = (bf16[512,768]{1,0:T(8,128)(2,1)}, bf16[512,768]{1,0:T(8,128)(2,1)S(1)}, u32[]{:S(2)}) copy-start(bf16[512,768]{1,0:T(8,128)(2,1)S(1)} %collective-permute-done.refs_1_) | copy-start | bytes 2359300
  60.9 8.9 %copy-start.7 = (bf16[512,768]{1,0:T(8,128)(2,1)}, bf16[512,768]{1,0:T(8,128)(2,1)S(1)}, u32[]{:S(2)}) copy-start(bf16[512,768]{1,0:T(8,128)(2,1)S(1)} %collective-permute-done.1.refs_2_) | copy-start | bytes 2359300
  61.0 10.7 %collective-permute-start.3 = (bf16[256,768]{1,0:T(8,128)(2,1)S(1)}, bf16[256,768]{1,0:T(8,128)(2,1)S(1)}, u32[]{:S(2)}, u32[]{:S(2)}) collective-permute-start(bf16[256,768]{1,0:T(8,128)(2,1)S(1)} %slice.553), channel_id=1, source_target_pairs={{0,8},{8,16},{16,24},{24,0},{1,9},{9,17},{17,25},{25,1},{2,10},{10... | collective-permute-start | bytes 1179656 | tf_op jit(solution)/shard_map/ppermute | solution.py:21
  64.1 8.8 %collective-permute-start.4 = (bf16[256,768]{1,0:T(8,128)(2,1)S(1)}, bf16[256,768]{1,0:T(8,128)(2,1)}, u32[]{:S(2)}, u32[]{:S(2)}) collective-permute-start(bf16[256,768]{1,0:T(8,128)(2,1)S(1)} %slice.554), channel_id=1, source_target_pairs={{0,24},{8,0},{16,8},{24,16},{1,25},{9,1},{17,9},{25,17},{2,26},{10... | collective-permute-start | bytes 1179656 | tf_op jit(solution)/shard_map/ppermute | solution.py:21
  71.7 0.8 copy-start.8
  81.0 18.9 %copy-start.3 = (f32[2,31,256]{2,0,1:T(2,128)S(1)}, f32[2,31,256]{2,0,1:T(2,128)}, u32[]{:S(2)}) copy-start(f32[2,31,256]{2,0,1:T(2,128)} %param.11) | copy-start | bytes 190468
  81.0 19.0 %copy-start.10 = (f32[2,256]{1,0:T(2,128)S(1)}, f32[2,256]{1,0:T(2,128)}, u32[]{:S(2)}) copy-start(f32[2,256]{1,0:T(2,128)} %param.12) | copy-start | bytes 6148
  81.0 14.9 %collective-permute-start.5 = (bf16[2400,256]{1,0:T(8,128)(2,1)}, bf16[2400,256]{1,0:T(8,128)(2,1)S(1)}, u32[]{:S(2)}, u32[]{:S(2)}) collective-permute-start(bf16[2400,256]{1,0:T(8,128)(2,1)} %get-tuple-element.29), channel_id=1, source_target_pairs={{0,1},{1,0},{2,3},{3,2},{4,5},{5,4},{6,7},{7,6},{8,9},{9,8},{10,11... | collective-permute-start | bytes 3686408 | tf_op jit(solution)/shard_map/ppermute | solution.py:21
  95.9 1.0 copy-start.2
  99.0 1.1 copy-start
  101.9 7.7 %slice-start = ((bf16[2400,256]{1,0:T(8,128)(2,1)}), bf16[2048,256]{1,0:T(8,128)(2,1)S(1)}, s32[]{:S(2)}) async-start(bf16[2400,256]{1,0:T(8,128)(2,1)} %copy-done.2), calls=%async_computation.6 | async-start | bytes 2097152 | tf_op jit(solution)/shard_map/slice | solution.py:157
  109.6 1.0 copy-start.9
  112.1 10.4 %all-to-all-start = ((bf16[4,32,2048]{2,1,0:T(8,128)(2,1)}), bf16[4,32,2048]{2,1,0:T(8,128)(2,1)S(1)}, u32[]{:S(2)}, u32[]{:S(2)}) async-start(bf16[4,32,2048]{2,1,0:T(8,128)(2,1)} %bitcast.133), calls=%async_computation | async-start | bytes 1048576 | tf_op jit(solution)/shard_map/all_to_all | solution.py:197
  123.6 10.4 %all-to-all-start.1 = ((bf16[4,32,2048]{2,1,0:T(8,128)(2,1)}), bf16[4,32,2048]{2,1,0:T(8,128)(2,1)S(1)}, u32[]{:S(2)}, u32[]{:S(2)}) async-start(bf16[4,32,2048]{2,1,0:T(8,128)(2,1)} %broadcast_in_dim.11), calls=%async_computation.1 | async-start | bytes 1048576 | tf_op jit(solution)/shard_map/all_to_all | solution.py:31
  134.0 2.8 %copy-start.5 = (bf16[4,32,2048]{2,1,0:T(8,128)(2,1)}, bf16[4,32,2048]{2,1,0:T(8,128)(2,1)S(1)}, u32[]{:S(2)}) copy-start(bf16[4,32,2048]{2,1,0:T(8,128)(2,1)S(1)} %all-to-all-done.1) | copy-start | bytes 1572868
  140.7 7.6 %copy-start.11 = (bf16[128,512]{1,0:T(8,128)(2,1)S(1)}, bf16[128,512]{1,0:T(8,128)(2,1)}, u32[]{:S(2)}) copy-start(bf16[128,512]{1,0:T(8,128)(2,1)} %get-tuple-element.35) | copy-start | bytes 393220
  140.7 7.6 %collective-permute-start.6 = (bf16[32,512]{1,0:T(8,128)(2,1)}, bf16[32,512]{1,0:T(8,128)(2,1)S(1)}, u32[]{:S(2)}, u32[]{:S(2)}) collective-permute-start(bf16[32,512]{1,0:T(8,128)(2,1)} %get-tuple-element.34), channel_id=1, source_target_pairs={{0,1},{1,8},{8,9},{9,16},{16,17},{17,24},{24,25},{25,32},{32,33},{... | collective-permute-start | bytes 98312 | tf_op jit(solution)/shard_map/ppermute | solution.py:26
  180.1 5.4 %collective-permute-start.7 = (bf16[128,2048]{1,0:T(8,128)(2,1)S(1)}, bf16[128,2048]{1,0:T(8,128)(2,1)S(1)}, u32[]{:S(2)}, u32[]{:S(2)}) collective-permute-start(bf16[128,2048]{1,0:T(8,128)(2,1)S(1)} %bitcast.128), channel_id=1, source_target_pairs={{0,1},{1,0},{2,3},{3,2},{4,5},{5,4},{6,7},{7,6},{8,9},{9,8},{10,11... | collective-permute-start | bytes 1572872 | tf_op jit(solution)/shard_map/ppermute | solution.py:21
Sparse Core Ops, SparseCore 0:
  9.4 66.6 all-gather.2
  81.1 55.6 all-gather.4
